TPU v7x, 256 devices: a whole 4x4x8 slice. The times are simulated.
256 devices in a mesh: ra: 32 (over z, x), cb: 4 (over y), dp: 2 (over core).
Axes of the slice: x: 4, y: 4, z: 8, core: 2. Of those that a mesh axis runs over, the one named last changes fastest.
Arguments:
- tokens: bfloat16 [256, 4096], P('dp', 'ra'), may hold values from -24 to 24
- first_gain: float32 [4096], P('ra'), may hold values from 0.1 to 1.9
- first_gate: float32 [4096, 11264], P('ra', 'cb'), may hold values from -0.1875 to 0.1875
- first_gate_scale: float32 [11264], P('cb'), may hold values from 0.5 to 2
- first_up: float32 [4096, 11264], P('ra', 'cb'), may hold values from -0.1875 to 0.1875
- first_up_scale: float32 [11264], P('cb'), may hold values from 0.5 to 2
- first_down: float32 [11264, 4096], P('cb', 'ra'), may hold values from -0.0546875 to 0.0546875
- first_down_scale: float32 [4096], P('ra'), may hold values from 0.5 to 2
- second_gain: float32 [4096], P('ra'), may hold values from 0.1 to 1.9
- second_gate: float32 [4096, 11264], P('ra', 'cb'), may hold values from -0.1875 to 0.1875
- second_gate_scale: float32 [11264], P('cb'), may hold values from 0.5 to 2
- second_up: float32 [4096, 11264], P('ra', 'cb'), may hold values from -0.1875 to 0.1875
- second_up_scale: float32 [11264], P('cb'), may hold values from 0.5 to 2
- second_down: float32 [11264, 4096], P('cb', 'ra'), may hold values from -0.0546875 to 0.0546875
- second_down_scale: float32 [4096], P('ra'), may hold values from 0.5 to 2
Outputs:
- mixed: float32 [256, 4096], P('dp', 'ra')
All inputs are finite; a program needn't handle non-finite values.
Results may differ from a plain program's by a relative error of at most 0.0083.
Values may be sent and summed in bfloat16 or wider, within the bound.
No kernel may reach another device: no remote copies, remote signals or barrier semaphores. Data moves between devices by JAX's collectives and lax.ppermute only.
A program may use at most 64 MiB of HBM per device.

v0:
```python
import jax
import jax.numpy as jnp
from jax import lax
from jax.sharding import Mesh
from jax.sharding import PartitionSpec as P

RA = ("ra_0", "ra_1")


def sent_to_all(shard, axis):
    size = lax.axis_size(axis)
    return lax.all_to_all(
        jnp.broadcast_to(shard[None], (size, *shard.shape)), axis, 0, 0, tiled=True
    )


def of_everyone(shard, axis):
    return sent_to_all(shard, axis).sum(axis=0)


def sum_by_axis(shard, axes, dim):
    for axis in axes:
        shard = lax.psum_scatter(shard, axis, scatter_dimension=dim, tiled=True)
    return shard


def laid_out(blocks, dim):
    lengths = list(blocks.shape[1:])
    lengths[dim] *= blocks.shape[0]
    return jnp.moveaxis(blocks, 0, dim).reshape(lengths)


def gather_directly(shard, axis, dim):
    blocks = sent_to_all(shard, axis)
    return laid_out(blocks, dim)


def half_step(stream, gain, gate_w, gate_scale, up_w, up_scale, down_w, down_scale):
    squares = jnp.sum(stream * stream, axis=1)
    width = stream.shape[1] * lax.axis_size(RA)
    scaled = (stream * gain).astype(jnp.bfloat16)
    gate_part = jnp.dot(scaled, gate_w.astype(jnp.bfloat16), preferred_element_type=jnp.float32)
    up_part = jnp.dot(scaled, up_w.astype(jnp.bfloat16), preferred_element_type=jnp.float32)
    down_bf = down_w.astype(jnp.bfloat16)
    total = of_everyone(squares, RA)
    inverse = lax.rsqrt(total / width + 1e-06)[:, None]
    gate_sum, up_sum = (sum_by_axis(gate_part, RA, 1), sum_by_axis(up_part, RA, 1))
    columns = gate_sum.shape[1]
    offset = lax.axis_index(RA) * columns
    gate_own = lax.dynamic_slice_in_dim(gate_scale, offset, columns, 0)
    up_own = lax.dynamic_slice_in_dim(up_scale, offset, columns, 0)
    hidden = (jax.nn.silu(gate_sum * inverse * gate_own) * (up_sum * inverse * up_own)).astype(
        jnp.bfloat16
    )
    partial_value = jnp.dot(
        gather_directly(hidden, RA, 1), down_bf, preferred_element_type=jnp.float32
    )
    branch = of_everyone(partial_value, "cb")
    return 0.5 * stream + 0.5 * branch * down_scale


def local(
    tokens,
    first_gain,
    first_gate,
    first_gate_scale,
    first_up,
    first_up_scale,
    first_down,
    first_down_scale,
    second_gain,
    second_gate,
    second_gate_scale,
    second_up,
    second_up_scale,
    second_down,
    second_down_scale,
):
    stream = tokens.astype(jnp.float32)
    stream = half_step(
        stream,
        first_gain,
        first_gate,
        first_gate_scale,
        first_up,
        first_up_scale,
        first_down,
        first_down_scale,
    )
    stream = half_step(
        stream,
        second_gain,
        second_gate,
        second_gate_scale,
        second_up,
        second_up_scale,
        second_down,
        second_down_scale,
    )
    return stream


def solution(mesh):
    torus = Mesh(
        mesh.devices.reshape(8, 4, mesh.shape["cb"], mesh.shape["dp"]), ("ra_0", "ra_1", "cb", "dp")
    )
    in_specs = (
        P("dp", RA),
        P(RA),
        P(RA, "cb"),
        P("cb"),
        P(RA, "cb"),
        P("cb"),
        P("cb", RA),
        P(RA),
        P(RA),
        P(RA, "cb"),
        P("cb"),
        P(RA, "cb"),
        P("cb"),
        P("cb", RA),
        P(RA),
    )
    out_specs = P("dp", RA)
    return jax.shard_map(local, mesh=torus, in_specs=in_specs, out_specs=out_specs, check_vma=False)
```

profile of v0, /device:TPU:2, one launch (start us, length us, event | category | flops | bytes accessed | tf_op | source)
XLA Modules:
  0.0 360.3 jit_solution(14948034705384698733)
XLA Ops:
  6.5 3.0 fusion.10
  9.6 0.0 reduce-scatter.19.cloned.1.call-start
  9.7 0.7 copy-done
  10.3 1.5 fusion.8
  11.9 0.0 reduce-scatter.19.cloned.1.call-update
  11.9 0.0 reduce-scatter.25.cloned.1.call-start
  12.0 41.0 %reduce-scatter.17.cloned.1.call-done = f32[128,352]{0,1:T(8,128)} async-done(((f32[128,2816]{0,1:T(8,128)}), f32[128,352]{0,1:T(8,128)}) %reduce-scatter.17.cloned.1.call-update) | async-done | bytes 180240 | tf_op jit(solution)/shard_map/reduce_scatter | solution.py:23
  53.0 0.0 reduce-scatter.27.cloned.1.call-start
  53.1 41.3 %reduce-scatter.19.cloned.1.call-done = f32[128,352]{0,1:T(8,128)} async-done(((f32[128,2816]{0,1:T(8,128)}), f32[128,352]{0,1:T(8,128)}) %reduce-scatter.19.cloned.1.call-update) | async-done | bytes 180240 | tf_op jit(solution)/shard_map/reduce_scatter | solution.py:23
  94.4 0.1 fusion.14
  94.5 0.6 broadcast_in_dim.12
  95.1 7.5 %all-to-all-start = ((f32[32,1,128]{2,1,0:T(1,128)}), f32[32,1,128]{2,1,0:T(1,128)S(1)}, u32[]{:S(2)}, u32[]{:S(2)}) async-start(f32[32,1,128]{2,1,0:T(1,128)} %broadcast_in_dim.12), calls=%async_computation.1 | async-start | bytes 32768 | tf_op jit(solution)/shard_map/all_to_all | solution.py:12
  102.7 0.8 dynamic_slice.12
  103.4 0.8 dynamic_slice.13
  104.2 6.9 %all-to-all-done = f32[32,1,128]{2,1,0:T(1,128)S(1)} async-done(((f32[32,1,128]{2,1,0:T(1,128)}), f32[32,1,128]{2,1,0:T(1,128)S(1)}, u32[]{:S(2)}, u32[]{:S(2)}) %all-to-all-start) | async-done | bytes 16416 | tf_op jit(solution)/shard_map/all_to_all | solution.py:12
  111.2 5.8 %reduce-scatter.25.cloned.1.call-done = f32[128,88]{0,1:T(8,128)} async-done(((f32[128,352]{0,1:T(8,128)}), f32[128,88]{0,1:T(8,128)}) %reduce-scatter.25.cloned.1.call-update) | async-done | bytes 45072
  117.0 25.4 %reduce-scatter.27.cloned.1.call-done = f32[128,88]{0,1:T(8,128)} async-done(((f32[128,352]{0,1:T(8,128)}), f32[128,88]{0,1:T(8,128)}) %reduce-scatter.27.cloned.1.call-update) | async-done | bytes 45072
  142.4 0.9 multiply_convert_fusion.2
  143.3 0.1 broadcast_in_dim.13
  143.4 29.0 %all_to_all.32 = bf16[32,128,88]{1,2,0:T(8,128)(2,1)S(1)} all-to-all(bf16[32,128,88]{1,2,0:T(8,128)(2,1)S(1)} %broadcast_in_dim.13), channel_id=1, replica_groups=mesh['ra_0'=8,'ra_1'=4,'cb'=4,'dp'=2] {'ra_0','ra_1'}, dimensions={0} | all-to-all | bytes 1441792 | tf_op jit(solution)/shard_map/all_to_all | solution.py:12
  172.5 0.4 fusion.6
  172.9 0.7 broadcast_in_dim.14
  173.6 4.3 %all-to-all-start.2 = ((f32[4,128,128]{2,1,0:T(8,128)}), f32[4,128,128]{2,1,0:T(8,128)S(1)}, u32[]{:S(2)}, u32[]{:S(2)}) async-start(f32[4,128,128]{2,1,0:T(8,128)} %broadcast_in_dim.14), calls=%async_computation.4 | async-start | bytes 524288 | tf_op jit(solution)/shard_map/all_to_all | solution.py:12
  177.8 6.7 %all-to-all-done.2 = f32[4,128,128]{2,1,0:T(8,128)S(1)} async-done(((f32[4,128,128]{2,1,0:T(8,128)}), f32[4,128,128]{2,1,0:T(8,128)S(1)}, u32[]{:S(2)}, u32[]{:S(2)}) %all-to-all-start.2) | async-done | bytes 262176 | tf_op jit(solution)/shard_map/all_to_all | solution.py:12
  184.6 1.5 fusion.4
  186.1 0.0 reduce-scatter.23.cloned.1.call-start
  186.2 1.3 copy-done.4
  187.5 1.5 fusion.2
  189.0 0.0 reduce-scatter.29.cloned.1.call-start
  189.1 32.2 %reduce-scatter.21.cloned.1.call-done = f32[128,352]{0,1:T(8,128)} async-done(((f32[128,2816]{0,1:T(8,128)}), f32[128,352]{0,1:T(8,128)}) %reduce-scatter.21.cloned.1.call-update) | async-done | bytes 180240 | tf_op jit(solution)/shard_map/reduce_scatter | solution.py:23
  221.3 0.0 reduce-scatter.31.cloned.1.call-start
  221.3 41.2 %reduce-scatter.23.cloned.1.call-done = f32[128,352]{0,1:T(8,128)} async-done(((f32[128,2816]{0,1:T(8,128)}), f32[128,352]{0,1:T(8,128)}) %reduce-scatter.23.cloned.1.call-update) | async-done | bytes 180240 | tf_op jit(solution)/shard_map/reduce_scatter | solution.py:23
  262.5 0.1 multiply_reduce_fusion
  262.6 0.6 broadcast_in_dim.15
  263.3 7.5 %all-to-all-start.3 = ((f32[32,1,128]{2,1,0:T(1,128)}), f32[32,1,128]{2,1,0:T(1,128)S(1)}, u32[]{:S(2)}, u32[]{:S(2)}) async-start(f32[32,1,128]{2,1,0:T(1,128)} %broadcast_in_dim.15), calls=%async_computation.6 | async-start | bytes 32768 | tf_op jit(solution)/shard_map/all_to_all | solution.py:12
  270.8 0.8 dynamic_slice.14
  271.6 0.8 dynamic_slice.15
  272.3 6.9 %all-to-all-done.3 = f32[32,1,128]{2,1,0:T(1,128)S(1)} async-done(((f32[32,1,128]{2,1,0:T(1,128)}), f32[32,1,128]{2,1,0:T(1,128)S(1)}, u32[]{:S(2)}, u32[]{:S(2)}) %all-to-all-start.3) | async-done | bytes 16416 | tf_op jit(solution)/shard_map/all_to_all | solution.py:12
  279.3 5.8 %reduce-scatter.29.cloned.1.call-done = f32[128,88]{0,1:T(8,128)} async-done(((f32[128,352]{0,1:T(8,128)}), f32[128,88]{0,1:T(8,128)}) %reduce-scatter.29.cloned.1.call-update) | async-done | bytes 45072
  285.1 25.6 %reduce-scatter.31.cloned.1.call-done = f32[128,88]{0,1:T(8,128)} async-done(((f32[128,352]{0,1:T(8,128)}), f32[128,88]{0,1:T(8,128)}) %reduce-scatter.31.cloned.1.call-update) | async-done | bytes 45072
  310.7 0.9 multiply_convert_fusion.1
  311.6 0.1 broadcast_in_dim.16
  311.7 29.0 %all_to_all.33 = bf16[32,128,88]{1,2,0:T(8,128)(2,1)S(1)} all-to-all(bf16[32,128,88]{1,2,0:T(8,128)(2,1)S(1)} %broadcast_in_dim.16), channel_id=1, replica_groups=mesh['ra_0'=8,'ra_1'=4,'cb'=4,'dp'=2] {'ra_0','ra_1'}, dimensions={0} | all-to-all | bytes 1441792 | tf_op jit(solution)/shard_map/all_to_all | solution.py:12
  340.7 0.4 fusion
  341.1 0.7 broadcast_in_dim.17
  341.9 4.3 %all-to-all-start.5 = ((f32[4,128,128]{2,1,0:T(8,128)}), f32[4,128,128]{2,1,0:T(8,128)S(1)}, u32[]{:S(2)}, u32[]{:S(2)}) async-start(f32[4,128,128]{2,1,0:T(8,128)} %broadcast_in_dim.17), calls=%async_computation.9 | async-start | bytes 524288 | tf_op jit(solution)/shard_map/all_to_all | solution.py:12
  346.2 6.7 %all-to-all-done.5 = f32[4,128,128]{2,1,0:T(8,128)S(1)} async-done(((f32[4,128,128]{2,1,0:T(8,128)}), f32[4,128,128]{2,1,0:T(8,128)S(1)}, u32[]{:S(2)}, u32[]{:S(2)}) %all-to-all-start.5) | async-done | bytes 262176 | tf_op jit(solution)/shard_map/all_to_all | solution.py:12
  352.9 0.7 multiply_add_fusion
  (35 shorter events, 0.2 us)
Async XLA Ops:
  6.5 46.5 %reduce-scatter.17.cloned.1.call-start = ((), (), s32[]{:S(2)}) async-start(), calls=%async_computation.14 | async-start | bytes 1622016 | tf_op jit(solution)/shard_map/reduce_scatter | solution.py:23
  6.5 3.1 copy-start.1
  9.6 0.8 copy-start
  9.6 0.8 copy-start.6
  9.6 84.7 %reduce-scatter.19.cloned.1.call-start = ((), (), s32[]{:S(2)}) async-start(), calls=%async_computation.15 | async-start | bytes 1622016 | tf_op jit(solution)/shard_map/reduce_scatter | solution.py:23
  11.9 160.5 %copy-start.2 = (f32[2816,128]{1,0:T(8,128)S(1)}, f32[2816,128]{1,0:T(8,128)}, u32[]{:S(2)}) copy-start(f32[2816,128]{1,0:T(8,128)} %param.21) | copy-start | bytes 4325380
  11.9 105.1 %reduce-scatter.25.cloned.1.call-start = ((), (), s32[]{:S(2)}) async-start(), calls=%async_computation.18 | async-start | bytes 225280
  53.0 89.4 %reduce-scatter.27.cloned.1.call-start = ((), (), s32[]{:S(2)}) async-start(), calls=%async_computation.19 | async-start | bytes 225280
  95.1 16.0 %all-to-all-start = ((f32[32,1,128]{2,1,0:T(1,128)}), f32[32,1,128]{2,1,0:T(1,128)S(1)}, u32[]{:S(2)}, u32[]{:S(2)}) async-start(f32[32,1,128]{2,1,0:T(1,128)} %broadcast_in_dim.12), calls=%async_computation.1 | async-start | bytes 32768 | tf_op jit(solution)/shard_map/all_to_all | solution.py:12
  172.4 5.4 %copy-start.8 = (f32[128]{0:T(128)S(1)}, f32[128]{0:T(128)}, u32[]{:S(2)}) copy-start(f32[128]{0:T(128)} %param.22) | copy-start | bytes 1540
  172.4 12.1 %copy-start.3 = (f32[128,2816]{1,0:T(8,128)S(1)}, f32[128,2816]{1,0:T(8,128)}, u32[]{:S(2)}) copy-start(f32[128,2816]{1,0:T(8,128)} %param.24) | copy-start | bytes 4325380
  172.4 12.1 %copy-start.7 = (f32[128]{0:T(128)S(1)}, f32[128]{0:T(128)}, u32[]{:S(2)}) copy-start(f32[128]{0:T(128)} %param.23) | copy-start | bytes 1540
  173.6 10.9 %all-to-all-start.2 = ((f32[4,128,128]{2,1,0:T(8,128)}), f32[4,128,128]{2,1,0:T(8,128)S(1)}, u32[]{:S(2)}, u32[]{:S(2)}) async-start(f32[4,128,128]{2,1,0:T(8,128)} %broadcast_in_dim.14), calls=%async_computation.4 | async-start | bytes 524288 | tf_op jit(solution)/shard_map/all_to_all | solution.py:12
  177.8 43.4 %reduce-scatter.21.cloned.1.call-start = ((), (), s32[]{:S(2)}) async-start(), calls=%async_computation.16 | async-start | bytes 1622016 | tf_op jit(solution)/shard_map/reduce_scatter | solution.py:23
  186.1 1.4 copy-start.4
  186.1 76.4 %reduce-scatter.23.cloned.1.call-start = ((), (), s32[]{:S(2)}) async-start(), calls=%async_computation.17 | async-start | bytes 1622016 | tf_op jit(solution)/shard_map/reduce_scatter | solution.py:23
  189.0 151.7 %copy-start.5 = (f32[2816,128]{1,0:T(8,128)S(1)}, f32[2816,128]{1,0:T(8,128)}, u32[]{:S(2)}) copy-start(f32[2816,128]{1,0:T(8,128)} %param.28) | copy-start | bytes 4325380
  189.0 96.1 %reduce-scatter.29.cloned.1.call-start = ((), (), s32[]{:S(2)}) async-start(), calls=%async_computation.20 | async-start | bytes 225280
  221.3 89.4 %reduce-scatter.31.cloned.1.call-start = ((), (), s32[]{:S(2)}) async-start(), calls=%async_computation.21 | async-start | bytes 225280
  263.3 16.0 %all-to-all-start.3 = ((f32[32,1,128]{2,1,0:T(1,128)}), f32[32,1,128]{2,1,0:T(1,128)S(1)}, u32[]{:S(2)}, u32[]{:S(2)}) async-start(f32[32,1,128]{2,1,0:T(1,128)} %broadcast_in_dim.15), calls=%async_computation.6 | async-start | bytes 32768 | tf_op jit(solution)/shard_map/all_to_all | solution.py:12
  340.7 5.4 %copy-start.9 = (f32[128]{0:T(128)S(1)}, f32[128]{0:T(128)}, u32[]{:S(2)}) copy-start(f32[128]{0:T(128)} %param.29) | copy-start | bytes 1540
  341.9 11.0 %all-to-all-start.5 = ((f32[4,128,128]{2,1,0:T(8,128)}), f32[4,128,128]{2,1,0:T(8,128)S(1)}, u32[]{:S(2)}, u32[]{:S(2)}) async-start(f32[4,128,128]{2,1,0:T(8,128)} %broadcast_in_dim.17), calls=%async_computation.9 | async-start | bytes 524288 | tf_op jit(solution)/shard_map/all_to_all | solution.py:12
Sparse Core Ops, SparseCore 0:
  9.9 43.0 reduce-scatter.16
  55.5 38.7 reduce-scatter.18
  96.9 20.0 reduce-scatter.24
  119.3 22.9 reduce-scatter.26
  186.2 34.9 reduce-scatter.20
  223.7 38.7 reduce-scatter.22
  265.0 20.0 reduce-scatter.28
  287.6 23.0 reduce-scatter.30
where the time goes:
time: 361 us; the launch traced here: 360 us
  waiting for transfers between devices  246 us (68%)
  blocking collectives  58.1 us (16%)
  starting transfers between devices  23.8 us (7%)
  between operations  13.6 us (4%)
  matrix products  8.47 us (2%)
  local copies, waits for them, and re-layouts  7.95 us (2%)
    reduce_scatter x4, waiting for transfers between devices, sum_by_axis(): shard = lax.psum_scatter(shard, axis, scatter_dimension=dim, tiled=True)  156 us
    unnamed x12, waiting for transfers between devices  62.7 us
    all_to_all x2, blocking collectives, sent_to_all(): lax.all_to_all(jnp.broadcast_to(shard[None], (size, *shard.shape)), axis,...  58.1 us
    all_to_all x4, waiting for transfers between devices, sent_to_all(): lax.all_to_all(jnp.broadcast_to(shard[None], (size, *shard.shape)), axis,...  27.2 us
    all_to_all x4, starting transfers between devices, sent_to_all(): lax.all_to_all(jnp.broadcast_to(shard[None], (size, *shard.shape)), axis,...  23.6 us
  transfers between devices with their start and end apart: 12, of which 12 were waited for; matrix products, arithmetic and copies ran while one was open for 2% of the time, Pallas kernels for 0%

commit v1 on v0

v1 whole, which is shorter than its diff:
```python
import jax
import jax.numpy as jnp
from jax import lax
from jax.sharding import Mesh
from jax.sharding import PartitionSpec as P

BF = jnp.bfloat16
F32 = jnp.float32
XY = ("x", "y")


def swap(v, axis, size):
    return lax.all_to_all(v, axis, 0, 0, tiled=True)


def to_all(v, axis):
    n = lax.axis_size(axis)
    return lax.all_to_all(jnp.broadcast_to(v[None], (n, *v.shape)), axis, 0, 0, tiled=True)


def other_core(v):
    return lax.ppermute(v, "c", [(0, 1), (1, 0)])


def half_of(v, c, dim):
    first = lax.index_in_dim(v, 0, dim, keepdims=False)
    second = lax.index_in_dim(v, 1, dim, keepdims=False)
    return jnp.where(c == 0, first, second)


def pack_up(gate, up, gain, c):
    nx = lax.axis_size("x")
    rows, cols = gate.shape
    parts = []
    for w in (gate, up):
        scaled = (w * gain[:, None]).astype(BF)
        parts.append(half_of(scaled.reshape(rows, nx, 2, cols // nx // 2), c, 2))
    packed = jnp.concatenate(parts, axis=2)
    return packed.transpose(1, 0, 2)


def pack_down(down, c):
    nx = lax.axis_size("x")
    rows, cols = down.shape
    return half_of(down.astype(BF).reshape(nx, 2, rows // nx // 2, cols), c, 1)


def reshard(packed):
    own = lax.all_to_all(packed, "x", 0, 0, tiled=True)
    return own, other_core(own)


def scales_of(scale, x, c):
    size = scale.shape[0] // lax.axis_size("x") // 2
    base = x * 2 * size
    return (
        lax.dynamic_slice_in_dim(scale, base + c * size, size, 0),
        lax.dynamic_slice_in_dim(scale, base + (1 - c) * size, size, 0),
    )


def hidden_part(stream, ups, gate_scale, up_scale, x, c, width):
    nz = lax.axis_size("z")
    tokens = stream.shape[1]
    rows = tokens // nz
    flat = stream.transpose(1, 0, 2).reshape(tokens, -1)
    squares = jnp.sum(flat * flat, axis=1, keepdims=True)
    high = squares.astype(BF)
    low = (squares - high.astype(F32)).astype(BF)
    lanes = jnp.concatenate([jnp.broadcast_to(high, (tokens, 64)), jnp.broadcast_to(low, (tokens, 64))], axis=1)
    flat_bf = flat.astype(BF)
    sums = [
        jnp.dot(flat_bf, w.reshape(-1, w.shape[-1]), preferred_element_type=F32).astype(BF)
        for w in ups
    ]
    payload = jnp.concatenate([*sums, lanes], axis=1)
    got = lax.all_to_all(payload.reshape(nz, rows, -1), "z", 0, 0, tiled=True)
    total = jnp.sum(got.astype(F32), axis=0)
    half = sums[0].shape[1] // 2
    mean = jnp.sum(total[:, 4 * half :], axis=1, keepdims=True) / 64.0 / width
    inverse = lax.rsqrt(mean + 1e-06)
    gate_scales = scales_of(gate_scale, x, c)
    up_scales = scales_of(up_scale, x, c)
    hidden = []
    for k in range(2):
        gate = total[:, 2 * k * half : (2 * k + 1) * half] * inverse * gate_scales[k]
        up = total[:, (2 * k + 1) * half : (2 * k + 2) * half] * inverse * up_scales[k]
        hidden.append((jax.nn.silu(gate) * up).astype(BF))
    hidden = jnp.concatenate(hidden, axis=1)
    return to_all(hidden, "z").reshape(tokens, -1)


def down_part(hidden, downs):
    half = hidden.shape[1] // 2
    own = jnp.einsum("tf,xfd->xtd", hidden[:, :half], downs[0], preferred_element_type=F32)
    other = jnp.einsum("tf,xfd->xtd", hidden[:, half:], downs[1], preferred_element_type=F32)
    return (own + other).astype(BF)


def local(
    tokens,
    first_gain,
    first_gate,
    first_gate_scale,
    first_up,
    first_up_scale,
    first_down,
    first_down_scale,
    second_gain,
    second_gate,
    second_gate_scale,
    second_up,
    second_up_scale,
    second_down,
    second_down_scale,
):
    x = lax.axis_index("x")
    y = lax.axis_index("y")
    c = lax.axis_index("c")
    nx, ny, nz = lax.axis_size("x"), lax.axis_size("y"), lax.axis_size("z")
    n_tok, n_col = tokens.shape
    width = n_col * nx * nz
    rows = n_tok // ny

    first_ups = reshard(pack_up(first_gate, first_up, first_gain, c))
    stream = to_all(tokens, "x").astype(F32)
    first_downs = reshard(pack_down(first_down, c))
    second_ups = reshard(pack_up(second_gate, second_up, second_gain, c))
    second_downs = reshard(pack_down(second_down, c))

    hidden = hidden_part(stream, first_ups, first_gate_scale, first_up_scale, x, c, width)
    part = down_part(hidden, first_downs)
    got = lax.all_to_all(part.reshape(nx * ny, rows, n_col), XY, 0, 0, tiled=True)
    branch = jnp.sum(got.astype(F32), axis=0) * first_down_scale
    mine = lax.dynamic_slice_in_dim(tokens, y * rows, rows, 0).astype(F32)
    mine = 0.5 * mine + 0.5 * branch
    stream = to_all(mine, XY).reshape(nx, n_tok, n_col)

    hidden = hidden_part(stream, second_ups, second_gate_scale, second_up_scale, x, c, width)
    part = down_part(hidden, second_downs)
    spread = jnp.broadcast_to(part[:, None], (nx, ny, n_tok, n_col)).reshape(nx * ny, n_tok, n_col)
    got = lax.all_to_all(spread, XY, 0, 0, tiled=True)
    branch = jnp.sum(got.astype(F32), axis=0) * second_down_scale
    mine = lax.dynamic_index_in_dim(stream, x, 0, keepdims=False)
    return 0.5 * mine + 0.5 * branch


def solution(mesh):
    torus = Mesh(
        mesh.devices.reshape(8, 4, mesh.shape["cb"], mesh.shape["dp"]), ("z", "x", "y", "c")
    )
    ra = ("z", "x")
    wide, tall = P(ra, "y"), P("y", ra)
    half = (P(ra), wide, P("y"), wide, P("y"), tall, P(ra))
    in_specs = (P("c", ra), *half, *half)
    return jax.shard_map(
        local, mesh=torus, in_specs=in_specs, out_specs=P("c", ra), check_vma=False
    )
```

time: 361 us -> 177 us (0.49)
  waiting for transfers between devices: 246 us -> 75.8 us
  blocking collectives: 58.1 us -> 23.4 us
  starting transfers between devices: 23.8 us -> 51 us
  between operations: 13.6 us -> 0.41 us
  local copies, waits for them, and re-layouts: 7.95 us -> 12.7 us
  other arithmetic: 2.76 us -> 7.06 us
  matrix products: 8.47 us -> 4.2 us
    reduce_scatter x4 -> x0, waiting for transfers between devices: 156 us -> none  [sum_by_axis(): shard = lax.psum_scatter(shard, axis, scatter_dimension=dim, tiled=True)]
    unnamed x12 -> x0, waiting for transfers between devices: 62.7 us -> none
    all_to_all x4 -> x10, waiting for transfers between devices: 27.2 us -> 75.8 us  [the longest x3 25.6 us: to_all(): lax.all_to_all(jnp.broadcast_to(v[None], (n, *v.shape)), axis, 0, 0, tile...]
    all_to_all x2, blocking collectives: 58.1 us -> 23.4 us  [the longest x1 14.8 us: reshard(): own = lax.all_to_all(packed, 'x', 0, 0, tiled=True)]
    all_to_all x4 -> x10, starting transfers between devices: 23.6 us -> 50.8 us  [the longest x3 15.7 us: reshard(): own = lax.all_to_all(packed, 'x', 0, 0, tiled=True)]
    dot_general x6 -> x8, matrix products: 8.47 us -> 4.2 us  [the longest x2 1.5 us: down_part(): jnp.einsum('tf,xfd->xtd', hidden[:, :half], downs[0], preferred_element_t...]
    unnamed x20, local copies, waits for them, and re-layouts: 1.99 us -> 5.84 us
  transfers between devices with their start and end apart: 12 -> 14, of which waited for: 12 -> 10; matrix products, arithmetic and copies ran while one was open for 2% -> 7% of each run, Pallas kernels for 0% -> 0%
where the time goes in v1:
time: 177 us; the launch traced here: 174 us
  waiting for transfers between devices  75.8 us (43%)
  starting transfers between devices  51 us (29%)
  blocking collectives  23.4 us (13%)
  local copies, waits for them, and re-layouts  12.7 us (7%)
  other arithmetic  7.06 us (4%)
  matrix products  4.2 us (2%)
    all_to_all x3, waiting for transfers between devices, to_all(): lax.all_to_all(jnp.broadcast_to(v[None], (n, *v.shape)), axis, 0, 0, tile...  25.6 us
    all_to_all x3, waiting for transfers between devices, reshard(): own = lax.all_to_all(packed, 'x', 0, 0, tiled=True)  18.5 us
    all_to_all x2, waiting for transfers between devices, hidden_part(): got = lax.all_to_all(payload.reshape(nz, rows, -1), 'z', 0, 0, tiled=True)  18.3 us
    all_to_all x3, starting transfers between devices, reshard(): own = lax.all_to_all(packed, 'x', 0, 0, tiled=True)  15.7 us
    all_to_all x1, blocking collectives, reshard(): own = lax.all_to_all(packed, 'x', 0, 0, tiled=True)  14.8 us
    all_to_all x2, starting transfers between devices, hidden_part(): got = lax.all_to_all(payload.reshape(nz, rows, -1), 'z', 0, 0, tiled=True)  12 us
    all_to_all x3, starting transfers between devices, to_all(): lax.all_to_all(jnp.broadcast_to(v[None], (n, *v.shape)), axis, 0, 0, tile...  11.7 us
    all_to_all x1, blocking collectives, to_all(): lax.all_to_all(jnp.broadcast_to(v[None], (n, *v.shape)), axis, 0, 0, tile...  8.6 us
  transfers between devices with their start and end apart: 14, of which 10 were waited for; matrix products, arithmetic and copies ran while one was open for 7% of the time, Pallas kernels for 0%

profile of v1, /device:TPU:2, one launch (start us, length us, event | category | flops | bytes accessed | tf_op | source)
XLA Modules:
  0.0 174.5 jit_solution(7005852109997353373)
XLA Ops:
  0.0 1.8 %copy.42 = f32[128,2816]{0,1:T(8,128)S(1)} copy(f32[128,2816]{1,0:T(8,128)} %param.17) | data formatting | bytes 2883584 | tf_op args[2]
  1.8 1.8 %copy.45 = f32[128,2816]{0,1:T(8,128)S(1)} copy(f32[128,2816]{1,0:T(8,128)} %param.19) | data formatting | bytes 2883584 | tf_op args[4]
  3.6 0.2 multiply_convert_fusion.3
  4.0 14.8 %all_to_all.60 = bf16[4,128,704]{1,2,0:T(8,128)(2,1)S(1)} all-to-all(bf16[4,128,704]{1,2,0:T(8,128)(2,1)S(1)} %maximum_bitcast_fusion), channel_id=1, replica_groups=mesh['z'=8,'x'=4,'y'=4,'c'=2] {'x'}, dimensions={0} | all-to-all | bytes 1441792 | tf_op jit(solution)/shard_map/all_to_all | solution.py:49
  18.8 8.6 %all_to_all.61 = bf16[4,128,128]{2,1,0:T(8,128)(2,1)S(1)} all-to-all(bf16[4,128,128]{2,1,0:T(8,128)(2,1)S(1)} %broadcast_in_dim.18), channel_id=1, replica_groups=mesh['z'=8,'x'=4,'y'=4,'c'=2] {'x'}, dimensions={0} | all-to-all | bytes 262144 | tf_op jit(solution)/shard_map/all_to_all | solution.py:18
  27.5 0.4 fusion.7
  27.9 0.3 fusion.6
  28.3 0.9 copy.48
  29.3 8.6 %all-to-all-start.3 = ((bf16[8,16,1536]{2,1,0:T(8,128)(2,1)}), bf16[8,16,1536]{2,1,0:T(8,128)(2,1)S(1)}, u32[]{:S(2)}, u32[]{:S(2)}) async-start(bf16[8,16,1536]{2,1,0:T(8,128)(2,1)} %bitcast.12), calls=%async_computation.3 | async-start | bytes 786432 | tf_op jit(solution)/shard_map/all_to_all | solution.py:77
  37.9 1.0 convert_element_type.147
  38.8 0.4 copy.53
  39.3 1.8 %copy.56 = f32[128,2816]{0,1:T(8,128)S(1)} copy(f32[128,2816]{1,0:T(8,128)} %param.26) | data formatting | bytes 2883584 | tf_op args[11]
  41.1 0.9 fusion.48
  41.9 1.9 %fusion.16 = bf16[4,352,128]{2,1,0:T(8,128)(2,1)} fusion(bf16[4,2,352,128]{3,2,1,0:T(8,128)(2,1)} %bitcast.165, pred[]{:T(512)S(6)} %eq.2), kind=kLoop, calls=%fused_computation.40 | loop fusion | flops 180224 | bytes 1081345 | tf_op jit(solution)/shard_map/jit(_where)/select_n | solution.py:28
  43.8 8.2 %all-to-all-done.3 = bf16[8,16,1536]{2,1,0:T(8,128)(2,1)S(1)} async-done(((bf16[8,16,1536]{2,1,0:T(8,128)(2,1)}), bf16[8,16,1536]{2,1,0:T(8,128)(2,1)S(1)}, u32[]{:S(2)}, u32[]{:S(2)}) %all-to-all-start.3) | async-done | bytes 393248 | tf_op jit(solution)/shard_map/all_to_all | solution.py:77
  52.1 5.5 %all-to-all-start = ((bf16[4,352,128]{2,1,0:T(8,128)(2,1)}), bf16[4,352,128]{2,1,0:T(8,128)(2,1)}, u32[]{:S(2)}, u32[]{:S(2)}) async-start(bf16[4,352,128]{2,1,0:T(8,128)(2,1)} %fusion.16), calls=%async_computation | async-start | bytes 720896 | tf_op jit(solution)/shard_map/all_to_all | solution.py:49
  58.0 5.5 %all-to-all-done = bf16[4,352,128]{2,1,0:T(8,128)(2,1)} async-done(((bf16[4,352,128]{2,1,0:T(8,128)(2,1)}), bf16[4,352,128]{2,1,0:T(8,128)(2,1)}, u32[]{:S(2)}, u32[]{:S(2)}) %all-to-all-start) | async-done | bytes 360480 | tf_op jit(solution)/shard_map/all_to_all | solution.py:49
  63.4 0.7 broadcast_in_dim.21
  64.1 3.4 %all-to-all-start.4 = ((bf16[8,16,704]{2,1,0:T(8,128)(2,1)}), bf16[8,16,704]{2,1,0:T(8,128)(2,1)S(1)}, u32[]{:S(2)}, u32[]{:S(2)}) async-start(bf16[8,16,704]{2,1,0:T(8,128)(2,1)} %broadcast_in_dim.21), calls=%async_computation.4 | async-start | bytes 393216 | tf_op jit(solution)/shard_map/all_to_all | solution.py:18
  68.0 9.3 %all-to-all-done.4 = bf16[8,16,704]{2,1,0:T(8,128)(2,1)S(1)} async-done(((bf16[8,16,704]{2,1,0:T(8,128)(2,1)}), bf16[8,16,704]{2,1,0:T(8,128)(2,1)S(1)}, u32[]{:S(2)}, u32[]{:S(2)}) %all-to-all-start.4) | async-done | bytes 180256 | tf_op jit(solution)/shard_map/all_to_all | solution.py:18
  77.2 1.2 fusion.26
  78.4 0.9 fusion.5
  79.4 6.5 %all-to-all-start.5 = ((bf16[16,32,128]{2,1,0:T(8,128)(2,1)}), bf16[16,32,128]{2,1,0:T(8,128)(2,1)S(1)}, u32[]{:S(2)}, u32[]{:S(2)}) async-start(bf16[16,32,128]{2,1,0:T(8,128)(2,1)} %bitcast.17), calls=%async_computation.5 | async-start | bytes 262144 | tf_op jit(solution)/shard_map/all_to_all | solution.py:133
  85.9 0.9 maximum_bitcast_fusion.1
  86.9 5.4 %all-to-all-done.5 = bf16[16,32,128]{2,1,0:T(8,128)(2,1)S(1)} async-done(((bf16[16,32,128]{2,1,0:T(8,128)(2,1)}), bf16[16,32,128]{2,1,0:T(8,128)(2,1)S(1)}, u32[]{:S(2)}, u32[]{:S(2)}) %all-to-all-start.5) | async-done | bytes 131104 | tf_op jit(solution)/shard_map/all_to_all | solution.py:133
  92.3 5.0 %all-to-all-start.8 = ((bf16[4,128,704]{1,2,0:T(8,128)(2,1)}), bf16[4,128,704]{1,2,0:T(8,128)(2,1)S(1)}, u32[]{:S(2)}, u32[]{:S(2)}) async-start(bf16[4,128,704]{1,2,0:T(8,128)(2,1)} %maximum_bitcast_fusion.1), calls=%async_computation.8 | async-start | bytes 1441792 | tf_op jit(solution)/shard_map/all_to_all | solution.py:49
  97.4 7.6 %all-to-all-done.8 = bf16[4,128,704]{1,2,0:T(8,128)(2,1)S(1)} async-done(((bf16[4,128,704]{1,2,0:T(8,128)(2,1)}), bf16[4,128,704]{1,2,0:T(8,128)(2,1)S(1)}, u32[]{:S(2)}, u32[]{:S(2)}) %all-to-all-start.8) | async-done | bytes 720928 | tf_op jit(solution)/shard_map/all_to_all | solution.py:49
  105.0 0.7 broadcast_in_dim.22
  105.7 4.9 %all-to-all-start.6 = ((f32[16,32,128]{2,1,0:T(8,128)}), f32[16,32,128]{2,1,0:T(8,128)S(1)}, u32[]{:S(2)}, u32[]{:S(2)}) async-start(f32[16,32,128]{2,1,0:T(8,128)} %broadcast_in_dim.22), calls=%async_computation.6 | async-start | bytes 524288 | tf_op jit(solution)/shard_map/all_to_all | solution.py:18
  110.6 6.8 %all-to-all-done.6 = f32[16,32,128]{2,1,0:T(8,128)S(1)} async-done(((f32[16,32,128]{2,1,0:T(8,128)}), f32[16,32,128]{2,1,0:T(8,128)S(1)}, u32[]{:S(2)}, u32[]{:S(2)}) %all-to-all-start.6) | async-done | bytes 262176 | tf_op jit(solution)/shard_map/all_to_all | solution.py:18
  117.5 0.3 fusion.2
  117.9 0.3 fusion.3
  118.3 0.9 copy.59
  119.2 3.5 %all-to-all-start.9 = ((bf16[8,16,1536]{2,1,0:T(8,128)(2,1)}), bf16[8,16,1536]{2,1,0:T(8,128)(2,1)S(1)}, u32[]{:S(2)}, u32[]{:S(2)}) async-start(bf16[8,16,1536]{2,1,0:T(8,128)(2,1)} %bitcast.30), calls=%async_computation.9 | async-start | bytes 786432 | tf_op jit(solution)/shard_map/all_to_all | solution.py:77
  122.8 0.9 fusion.46
  123.7 0.8 fusion.14
  124.4 10.1 %all-to-all-done.9 = bf16[8,16,1536]{2,1,0:T(8,128)(2,1)S(1)} async-done(((bf16[8,16,1536]{2,1,0:T(8,128)(2,1)}), bf16[8,16,1536]{2,1,0:T(8,128)(2,1)S(1)}, u32[]{:S(2)}, u32[]{:S(2)}) %all-to-all-start.9) | async-done | bytes 393248 | tf_op jit(solution)/shard_map/all_to_all | solution.py:77
  134.5 5.2 %all-to-all-start.7 = ((bf16[4,352,128]{2,1,0:T(8,128)(2,1)}), bf16[4,352,128]{2,1,0:T(8,128)(2,1)S(1)}, u32[]{:S(2)}, u32[]{:S(2)}) async-start(bf16[4,352,128]{2,1,0:T(8,128)(2,1)} %fusion.14), calls=%async_computation.7 | async-start | bytes 720896 | tf_op jit(solution)/shard_map/all_to_all | solution.py:49
  140.1 5.4 %all-to-all-done.7 = bf16[4,352,128]{2,1,0:T(8,128)(2,1)S(1)} async-done(((bf16[4,352,128]{2,1,0:T(8,128)(2,1)}), bf16[4,352,128]{2,1,0:T(8,128)(2,1)S(1)}, u32[]{:S(2)}, u32[]{:S(2)}) %all-to-all-start.7) | async-done | bytes 360480 | tf_op jit(solution)/shard_map/all_to_all | solution.py:49
  145.4 0.7 broadcast_in_dim.25
  146.2 3.4 %all-to-all-start.10 = ((bf16[8,16,704]{2,1,0:T(8,128)(2,1)}), bf16[8,16,704]{2,1,0:T(8,128)(2,1)S(1)}, u32[]{:S(2)}, u32[]{:S(2)}) async-start(bf16[8,16,704]{2,1,0:T(8,128)(2,1)} %broadcast_in_dim.25), calls=%async_computation.10 | async-start | bytes 393216 | tf_op jit(solution)/shard_map/all_to_all | solution.py:18
  149.6 9.6 %all-to-all-done.10 = bf16[8,16,704]{2,1,0:T(8,128)(2,1)S(1)} async-done(((bf16[8,16,704]{2,1,0:T(8,128)(2,1)}), bf16[8,16,704]{2,1,0:T(8,128)(2,1)S(1)}, u32[]{:S(2)}, u32[]{:S(2)}) %all-to-all-start.10) | async-done | bytes 180256 | tf_op jit(solution)/shard_map/all_to_all | solution.py:18
  159.2 0.3 fusion.25
  159.5 0.4 fusion.8
  160.1 0.9 broadcast_in_dim.26
  161.0 4.9 %all-to-all-start.11 = ((bf16[16,128,128]{2,1,0:T(8,128)(2,1)}), bf16[16,128,128]{2,1,0:T(8,128)(2,1)S(1)}, u32[]{:S(2)}, u32[]{:S(2)}) async-start(bf16[16,128,128]{2,1,0:T(8,128)(2,1)} %bitcast.35), calls=%async_computation.11 | async-start | bytes 1048576 | tf_op jit(solution)/shard_map/all_to_all | solution.py:142
  165.9 7.9 %all-to-all-done.11 = bf16[16,128,128]{2,1,0:T(8,128)(2,1)S(1)} async-done(((bf16[16,128,128]{2,1,0:T(8,128)(2,1)}), bf16[16,128,128]{2,1,0:T(8,128)(2,1)S(1)}, u32[]{:S(2)}, u32[]{:S(2)}) %all-to-all-start.11) | async-done | bytes 524320 | tf_op jit(solution)/shard_map/all_to_all | solution.py:142
  173.8 0.6 fusion.27
  (54 shorter events, 2.0 us)
Async XLA Ops:
  1.8 1.8 %copy-start.4 = (f32[128]{0:T(128)S(1)}, f32[128]{0:T(128)}, u32[]{:S(2)}) copy-start(f32[128]{0:T(128)} %param.16) | copy-start | bytes 1540
  3.9 14.8 %copy-start.3 = (bf16[128,128]{1,0:T(8,128)(2,1)S(1)}, bf16[128,128]{1,0:T(8,128)(2,1)}, u32[]{:S(2)}) copy-start(bf16[128,128]{1,0:T(8,128)(2,1)} %param.15) | copy-start | bytes 98308
  18.8 9.1 %collective-permute-start = (bf16[4,128,704]{1,2,0:T(8,128)(2,1)S(1)}, bf16[4,128,704]{1,2,0:T(8,128)(2,1)S(1)}, u32[]{:S(2)}, u32[]{:S(2)}) collective-permute-start(bf16[4,128,704]{1,2,0:T(8,128)(2,1)S(1)} %all_to_all.60), channel_id=1, source_target_pairs={{0,1},{1,0},{2,3},{3,2},{4,5},{5,4},{6,7},{7,6},{8,9},{9,8},{10,11... | collective-permute-start | bytes 2162696 | tf_op jit(solution)/shard_map/ppermute | solution.py:22
  28.2 9.6 %copy-start = (f32[2816,128]{1,0:T(8,128)S(1)}, f32[2816,128]{1,0:T(8,128)}, u32[]{:S(2)}) copy-start(f32[2816,128]{1,0:T(8,128)} %param.21) | copy-start | bytes 4325380
  29.2 9.6 %copy-start.1 = (f32[128,2816]{1,0:T(8,128)S(1)}, f32[128,2816]{1,0:T(8,128)}, u32[]{:S(2)}) copy-start(f32[128,2816]{1,0:T(8,128)} %param.24) | copy-start | bytes 4325380
  29.3 22.8 %all-to-all-start.3 = ((bf16[8,16,1536]{2,1,0:T(8,128)(2,1)}), bf16[8,16,1536]{2,1,0:T(8,128)(2,1)S(1)}, u32[]{:S(2)}, u32[]{:S(2)}) async-start(bf16[8,16,1536]{2,1,0:T(8,128)(2,1)} %bitcast.12), calls=%async_computation.3 | async-start | bytes 786432 | tf_op jit(solution)/shard_map/all_to_all | solution.py:77
  41.9 25.6 %copy-start.5 = (f32[128]{0:T(128)S(1)}, f32[128]{0:T(128)}, u32[]{:S(2)}) copy-start(f32[128]{0:T(128)} %param.23) | copy-start | bytes 1540
  52.1 11.4 %all-to-all-start = ((bf16[4,352,128]{2,1,0:T(8,128)(2,1)}), bf16[4,352,128]{2,1,0:T(8,128)(2,1)}, u32[]{:S(2)}, u32[]{:S(2)}) async-start(bf16[4,352,128]{2,1,0:T(8,128)(2,1)} %fusion.16), calls=%async_computation | async-start | bytes 720896 | tf_op jit(solution)/shard_map/all_to_all | solution.py:49
  64.1 13.1 %all-to-all-start.4 = ((bf16[8,16,704]{2,1,0:T(8,128)(2,1)}), bf16[8,16,704]{2,1,0:T(8,128)(2,1)S(1)}, u32[]{:S(2)}, u32[]{:S(2)}) async-start(bf16[8,16,704]{2,1,0:T(8,128)(2,1)} %broadcast_in_dim.21), calls=%async_computation.4 | async-start | bytes 393216 | tf_op jit(solution)/shard_map/all_to_all | solution.py:18
  67.8 10.7 %collective-permute-start.1 = (bf16[4,352,128]{2,1,0:T(8,128)(2,1)}, bf16[4,352,128]{2,1,0:T(8,128)(2,1)S(1)}, u32[]{:S(2)}, u32[]{:S(2)}) collective-permute-start(bf16[4,352,128]{2,1,0:T(8,128)(2,1)} %all-to-all-done), channel_id=1, source_target_pairs={{0,1},{1,0},{2,3},{3,2},{4,5},{5,4},{6,7},{7,6},{8,9},{9,8},{10,11... | collective-permute-start | bytes 1081352 | tf_op jit(solution)/shard_map/ppermute | solution.py:22
  79.4 12.9 %all-to-all-start.5 = ((bf16[16,32,128]{2,1,0:T(8,128)(2,1)}), bf16[16,32,128]{2,1,0:T(8,128)(2,1)S(1)}, u32[]{:S(2)}, u32[]{:S(2)}) async-start(bf16[16,32,128]{2,1,0:T(8,128)(2,1)} %bitcast.17), calls=%async_computation.5 | async-start | bytes 262144 | tf_op jit(solution)/shard_map/all_to_all | solution.py:133
  85.9 11.4 %copy-start.6 = (f32[128]{0:T(128)S(1)}, f32[128]{0:T(128)}, u32[]{:S(2)}) copy-start(f32[128]{0:T(128)} %param.22) | copy-start | bytes 1540
  92.3 12.7 %all-to-all-start.8 = ((bf16[4,128,704]{1,2,0:T(8,128)(2,1)}), bf16[4,128,704]{1,2,0:T(8,128)(2,1)S(1)}, u32[]{:S(2)}, u32[]{:S(2)}) async-start(bf16[4,128,704]{1,2,0:T(8,128)(2,1)} %maximum_bitcast_fusion.1), calls=%async_computation.8 | async-start | bytes 1441792 | tf_op jit(solution)/shard_map/all_to_all | solution.py:49
  105.7 11.7 %all-to-all-start.6 = ((f32[16,32,128]{2,1,0:T(8,128)}), f32[16,32,128]{2,1,0:T(8,128)S(1)}, u32[]{:S(2)}, u32[]{:S(2)}) async-start(f32[16,32,128]{2,1,0:T(8,128)} %broadcast_in_dim.22), calls=%async_computation.6 | async-start | bytes 524288 | tf_op jit(solution)/shard_map/all_to_all | solution.py:18
  110.6 7.3 %collective-permute-start.2 = (bf16[4,128,704]{1,2,0:T(8,128)(2,1)S(1)}, bf16[4,128,704]{1,2,0:T(8,128)(2,1)S(1)}, u32[]{:S(2)}, u32[]{:S(2)}) collective-permute-start(bf16[4,128,704]{1,2,0:T(8,128)(2,1)S(1)} %all-to-all-done.8), channel_id=1, source_target_pairs={{0,1},{1,0},{2,3},{3,2},{4,5},{5,4},{6,7},{7,6},{8,9},{9,8},{10,11... | collective-permute-start | bytes 2162696 | tf_op jit(solution)/shard_map/ppermute | solution.py:22
  118.2 4.5 %copy-start.2 = (f32[2816,128]{1,0:T(8,128)S(1)}, f32[2816,128]{1,0:T(8,128)}, u32[]{:S(2)}) copy-start(f32[2816,128]{1,0:T(8,128)} %param.28) | copy-start | bytes 4325380
  119.2 15.3 %all-to-all-start.9 = ((bf16[8,16,1536]{2,1,0:T(8,128)(2,1)}), bf16[8,16,1536]{2,1,0:T(8,128)(2,1)S(1)}, u32[]{:S(2)}, u32[]{:S(2)}) async-start(bf16[8,16,1536]{2,1,0:T(8,128)(2,1)} %bitcast.30), calls=%async_computation.9 | async-start | bytes 786432 | tf_op jit(solution)/shard_map/all_to_all | solution.py:77
  134.5 10.9 %all-to-all-start.7 = ((bf16[4,352,128]{2,1,0:T(8,128)(2,1)}), bf16[4,352,128]{2,1,0:T(8,128)(2,1)S(1)}, u32[]{:S(2)}, u32[]{:S(2)}) async-start(bf16[4,352,128]{2,1,0:T(8,128)(2,1)} %fusion.14), calls=%async_computation.7 | async-start | bytes 720896 | tf_op jit(solution)/shard_map/all_to_all | solution.py:49
  146.2 13.1 %all-to-all-start.10 = ((bf16[8,16,704]{2,1,0:T(8,128)(2,1)}), bf16[8,16,704]{2,1,0:T(8,128)(2,1)S(1)}, u32[]{:S(2)}, u32[]{:S(2)}) async-start(bf16[8,16,704]{2,1,0:T(8,128)(2,1)} %broadcast_in_dim.25), calls=%async_computation.10 | async-start | bytes 393216 | tf_op jit(solution)/shard_map/all_to_all | solution.py:18
  149.5 10.0 %collective-permute-start.3 = (bf16[4,352,128]{2,1,0:T(8,128)(2,1)S(1)}, bf16[4,352,128]{2,1,0:T(8,128)(2,1)S(1)}, u32[]{:S(2)}, u32[]{:S(2)}) collective-permute-start(bf16[4,352,128]{2,1,0:T(8,128)(2,1)S(1)} %all-to-all-done.7), channel_id=1, source_target_pairs={{0,1},{1,0},{2,3},{3,2},{4,5},{5,4},{6,7},{7,6},{8,9},{9,8},{10,11... | collective-permute-start | bytes 1081352 | tf_op jit(solution)/shard_map/ppermute | solution.py:22
  159.9 13.9 %copy-start.7 = (f32[128]{0:T(128)S(1)}, f32[128]{0:T(128)}, u32[]{:S(2)}) copy-start(f32[128]{0:T(128)} %param.29) | copy-start | bytes 1540
  161.0 12.8 %all-to-all-start.11 = ((bf16[16,128,128]{2,1,0:T(8,128)(2,1)}), bf16[16,128,128]{2,1,0:T(8,128)(2,1)S(1)}, u32[]{:S(2)}, u32[]{:S(2)}) async-start(bf16[16,128,128]{2,1,0:T(8,128)(2,1)} %bitcast.35), calls=%async_computation.11 | async-start | bytes 1048576 | tf_op jit(solution)/shard_map/all_to_all | solution.py:142

commit v2 on v0

v2 whole, which is shorter than its diff:
```python
import jax
import jax.numpy as jnp
from jax import lax
from jax.experimental import pallas as pl
from jax.experimental.pallas import tpu as pltpu
from jax.sharding import Mesh
from jax.sharding import PartitionSpec as P

BF = jnp.bfloat16
F32 = jnp.float32
XY = ("x", "y")
NX, NY, NZ = 4, 4, 8
N = 128
HALF = 352
PAD = 384
WIDE = 2 * PAD
CHUNK = 2 * HALF
WIDTH = 4096

SMEM = pl.BlockSpec(memory_space=pltpu.SMEM)
VMEM = pl.BlockSpec(memory_space=pltpu.VMEM)


def shape(*dims, dtype=BF):
    return jax.ShapeDtypeStruct(dims, dtype)


def call(body, outs, n_in, scratch=(), name=None):
    many = isinstance(outs, (list, tuple))
    return pl.pallas_call(
        body,
        out_shape=outs,
        in_specs=[SMEM] + [VMEM] * n_in,
        out_specs=[VMEM] * len(outs) if many else VMEM,
        scratch_shapes=list(scratch),
        name=name,
    )


def high_low(v):
    high = v.astype(BF).astype(F32)
    return high, (v - high).astype(BF).astype(F32)


def padded_chunk(ref, i):
    part = ref[:, i * HALF : (i + 1) * HALF]
    return jnp.concatenate([part, jnp.zeros((N, PAD - HALF), F32)], axis=1)


def with_columns(tile, first, second):
    lane = lax.broadcasted_iota(jnp.int32, tile.shape, 1)
    at = HALF - (PAD - N)
    return jnp.where(lane == at, first, jnp.where(lane == at + 1, second, tile))


def pack_first_body(at, gate, up, tokens, gain, p0, p1, p2, p3, other, chunks):
    x, c = at[0], at[2]
    for i in range(2 * NX):
        chunks[i, :, :PAD] = padded_chunk(gate, i).astype(BF)
        chunks[i, :, PAD:] = padded_chunk(up, i).astype(BF)
    stream = tokens[...].astype(F32)
    scaled = (stream * gain[...]).astype(BF)
    high, low = high_low(jnp.sum(stream * stream, axis=1, keepdims=True))
    for k, out in enumerate((p0, p1, p2, p3)):
        index = 2 * lax.rem(x + k, NX) + c
        out[:, :WIDE] = chunks[index]
        out[:, WIDE:] = scaled
        tile = chunks[index, :, PAD - N : PAD].astype(F32)
        out[:, PAD - N : PAD] = with_columns(tile, high, low).astype(BF)
    other[...] = chunks[2 * x + 1 - c]


def pack_second_body(at, gate, up, p0, p1, p2, p3, chunks):
    x = at[0]
    for i in range(2 * NX):
        chunks[i, :, :PAD] = padded_chunk(gate, i).astype(BF)
        chunks[i, :, PAD:] = padded_chunk(up, i).astype(BF)
    for k, out in enumerate((p0, p1, p2, p3)):
        index = 2 * lax.rem(x + k, NX)
        out[:, :WIDE] = chunks[index]
        out[:, WIDE:] = chunks[index + 1]


def pack_down_body(at, down, gain, p0, p1, p2, p3):
    x = at[0]
    value = gain[...]
    high = value.astype(BF).astype(F32)
    rest = value - high
    middle = rest.astype(BF).astype(F32)
    low = rest - middle
    row = lax.broadcasted_iota(jnp.int32, (PAD - HALF, N), 0)
    tail = jnp.where(row == 0, high, jnp.where(row == 1, middle, jnp.where(row == 2, low, 0.0)))
    tail = tail.astype(BF)
    for k, out in enumerate((p0, p1, p2, p3)):
        base = lax.rem(x + k, NX) * CHUNK
        for h in range(2):
            start = pl.multiple_of(base + h * HALF, 32)
            out[h * PAD : h * PAD + HALF, :] = down[pl.ds(start, HALF), :].astype(BF)
            out[h * PAD + HALF : (h + 1) * PAD, :] = tail


def store_payload(out, slot, sums, high, low):
    tile = with_columns(sums[:, PAD - N : PAD], high, low)
    sums = jnp.concatenate([sums[:, : PAD - N], tile, sums[:, PAD:]], axis=1)
    out[:, slot] = sums.astype(BF).reshape(NZ, N // NZ, WIDE)


def dot(a, b):
    return jnp.dot(a, b, preferred_element_type=F32)


def enter_first_body(at, r0, r1, r2, r3, q0, s1, s2, s3, out):
    c = at[2]
    mine = (r0, r1, r2, r3)
    theirs = (q0, s1, s2, s3)
    scaled = jnp.concatenate([r[:, WIDE:] for r in mine], axis=1)
    squares = jnp.zeros((N, N), F32)
    for r in mine:
        squares = squares + r[:, PAD - N : PAD].astype(F32)
    lane = lax.broadcasted_iota(jnp.int32, (N, N), 1)
    at_lane = HALF - (PAD - N)
    keep = (lane == at_lane) | (lane == at_lane + 1)
    squares = jnp.sum(jnp.where(keep, squares, 0.0), axis=1, keepdims=True)
    high, low = high_low(squares)
    for slot, group in ((c, mine), (1 - c, theirs)):
        weights = jnp.concatenate([r[:, :WIDE] for r in group], axis=0)
        store_payload(out, slot, dot(scaled, weights), high, low)


def enter_second_body(at, stream, d0, d1, d2, d3, w0, w1, w2, w3, out):
    x = at[0]
    scaled = []
    squares = jnp.zeros((N, 1), F32)
    for k, d in enumerate((d0, d1, d2, d3)):
        index = lax.rem(x + NX - k, NX)
        s = stream[pl.ds(index * NY, NY)].reshape(N, N)
        squares = squares + jnp.sum(s * s, axis=1, keepdims=True)
        tail = d[HALF:PAD, :].astype(F32)
        gain = tail[0:1] + tail[1:2] + tail[2:3]
        scaled.append((s * gain).astype(BF))
    scaled = jnp.concatenate(scaled, axis=1)
    high, low = high_low(squares)
    for slot in range(2):
        cols = slice(slot * WIDE, (slot + 1) * WIDE)
        weights = jnp.concatenate([w[:, cols] for w in (w0, w1, w2, w3)], axis=0)
        store_payload(out, slot, dot(scaled, weights), high, low)


def hidden_body(at, got, scales, out):
    rows = N // NZ
    tile = jnp.zeros((rows, N), F32)
    for z in range(NZ):
        tile = tile + got[z, 0, :, PAD - N : PAD].astype(F32)
    lane = lax.broadcasted_iota(jnp.int32, (rows, N), 1)
    at_lane = HALF - (PAD - N)
    keep = (lane == at_lane) | (lane == at_lane + 1)
    total = jnp.sum(jnp.where(keep, tile, 0.0), axis=1, keepdims=True)
    inverse = lax.rsqrt(total / WIDTH + 1e-06)
    for h in range(2):
        sums = got[0, h].astype(F32)
        for z in range(1, NZ):
            sums = sums + got[z, h].astype(F32)
        scaled = sums * inverse * scales[h : h + 1, :]
        gate = scaled[:, :PAD]
        hidden = gate / (1.0 + jnp.exp(-gate)) * scaled[:, PAD:]
        hidden = hidden.astype(BF)
        for z in range(NZ):
            out[z, h] = hidden


def down_sums(hidden, pieces):
    wide = jnp.concatenate([hidden[:, h].reshape(N, PAD) for h in range(2)], axis=1)
    return [dot(wide, d[...]).astype(BF) for d in pieces]


def leave_first_body(at, hidden, d0, d1, d2, d3, out):
    x = at[0]
    for k, part in enumerate(down_sums(hidden, (d0, d1, d2, d3))):
        index = lax.rem(x + NX - k, NX)
        out[pl.ds(index * NY, NY)] = part.reshape(NY, N // NY, N)


def leave_second_body(at, hidden, d0, d1, d2, d3, out):
    x = at[0]
    for k, part in enumerate(down_sums(hidden, (d0, d1, d2, d3))):
        index = lax.rem(x + NX - k, NX)
        for y in range(NY):
            out[index * NY + y] = part


def stream_body(at, got, tokens, scale, out):
    y = at[1]
    rows = N // NY
    branch = jnp.sum(got[...].astype(F32), axis=0) * scale[...]
    old = tokens[pl.ds(pl.multiple_of(y * rows, rows), rows), :].astype(F32)
    new = 0.5 * old + 0.5 * branch
    out[...] = jnp.broadcast_to(new[None], out.shape)


def final_body(at, got, stream, scale, out):
    x = at[0]
    branch = jnp.sum(got[...].astype(F32), axis=0) * scale[...]
    old = stream[pl.ds(x * NY, NY)].reshape(N, N)
    out[...] = 0.5 * old + 0.5 * branch


def shift(v, k):
    return lax.ppermute(v, "x", [(i, (i + k) % NX) for i in range(NX)])


def other_core(v):
    return lax.ppermute(v, "c", [(0, 1), (1, 0)])


def around(pieces):
    return [pieces[0]] + [shift(pieces[k], k) for k in range(1, NX)]


def swap(v, axis):
    return lax.all_to_all(v, axis, 0, 0, tiled=True)


def scale_rows(gate_scale, up_scale, x):
    rows = []
    for scale in (gate_scale, up_scale):
        own = lax.dynamic_slice_in_dim(scale, x * CHUNK, CHUNK, 0).reshape(2, HALF)
        rows.append(jnp.pad(own, ((0, 0), (0, PAD - HALF))))
    return jnp.concatenate(rows, axis=1)


def local(
    tokens,
    first_gain,
    first_gate,
    first_gate_scale,
    first_up,
    first_up_scale,
    first_down,
    first_down_scale,
    second_gain,
    second_gate,
    second_gate_scale,
    second_up,
    second_up_scale,
    second_down,
    second_down_scale,
):
    x = lax.axis_index("x")
    at = jnp.stack([x, lax.axis_index("y"), lax.axis_index("c")]).astype(jnp.int32)
    chunks = pltpu.VMEM((2 * NX, N, WIDE), BF)
    payload = shape(NZ, 2, N // NZ, WIDE)
    spread = shape(NZ, 2, N // NZ, PAD)

    *packed, other = call(
        pack_first_body, [shape(N, WIDE + N)] * NX + [shape(N, WIDE)], 4, [chunks], "pack_first"
    )(at, first_gate, first_up, tokens, first_gain[None])
    mine = around(packed)
    theirs = [other] + [other_core(v) for v in mine[1:]]
    sums = call(enter_first_body, payload, 8, name="enter_first")(at, *mine, *theirs)
    sums, first_down, second_gate, second_up, second_down = lax.optimization_barrier(
        (sums, first_down, second_gate, second_up, second_down)
    )
    got = swap(sums, "z")
    downs = around(
        call(pack_down_body, [shape(2 * PAD, N)] * NX, 2, name="pack_down")(
            at, first_down, second_gain[None]
        )
    )
    ups = around(
        call(pack_second_body, [shape(N, 2 * WIDE)] * NX, 2, [chunks], "pack_second")(
            at, second_gate, second_up
        )
    )
    last_downs = around(
        call(pack_down_body, [shape(2 * PAD, N)] * NX, 2, name="pack_last")(
            at, second_down, second_gain[None]
        )
    )
    hidden = call(hidden_body, spread, 2, name="hidden_first")(
        at, got, scale_rows(first_gate_scale, first_up_scale, x)
    )
    hidden = swap(hidden, "z")
    part = call(leave_first_body, shape(NX * NY, N // NY, N), 5, name="leave_first")(
        at, hidden, *downs
    )
    got = swap(part, XY)
    stream = call(stream_body, shape(NX * NY, N // NY, N, dtype=F32), 3, name="stream")(
        at, got, tokens, first_down_scale[None]
    )
    stream = swap(stream, XY)

    sums = call(enter_second_body, payload, 9, name="enter_second")(at, stream, *downs, *ups)
    got = swap(sums, "z")
    hidden = call(hidden_body, spread, 2, name="hidden_second")(
        at, got, scale_rows(second_gate_scale, second_up_scale, x)
    )
    hidden = swap(hidden, "z")
    part = call(leave_second_body, shape(NX * NY, N, N), 5, name="leave_second")(
        at, hidden, *last_downs
    )
    got = swap(part, XY)
    return call(final_body, shape(N, N, dtype=F32), 3, name="final")(
        at, got, stream, second_down_scale[None]
    )


def solution(mesh):
    torus = Mesh(
        mesh.devices.reshape(NZ, NX, mesh.shape["cb"], mesh.shape["dp"]), ("z", "x", "y", "c")
    )
    ra = ("z", "x")
    wide, tall = P(ra, "y"), P("y", ra)
    half = (P(ra), wide, P("y"), wide, P("y"), tall, P(ra))
    in_specs = (P("c", ra), *half, *half)
    return jax.shard_map(
        local, mesh=torus, in_specs=in_specs, out_specs=P("c", ra), check_vma=False
    )
```

time: 361 us -> 169 us (0.47)
  waiting for transfers between devices: 246 us -> 51 us
  Pallas kernels: 0 us -> 29.2 us
  blocking collectives: 58.1 us -> 30.7 us
  starting transfers between devices: 23.8 us -> 45.2 us
  between operations: 13.6 us -> 0.19 us
  matrix products: 8.47 us -> 0 us
    reduce_scatter x4 -> x0, waiting for transfers between devices: 156 us -> none  [sum_by_axis(): shard = lax.psum_scatter(shard, axis, scatter_dimension=dim, tiled=True)]
    unnamed x12 -> x0, waiting for transfers between devices: 62.7 us -> none
    pallas_call x0 -> x12, Pallas kernels: none -> 29.2 us  [the longest x1 3.61 us: local(): call(pack_second_body, [shape(N, 2 * WIDE)] * NX, 2, [chunks], 'pack_seco...]
    all_to_all x2, blocking collectives: 58.1 us -> 30.7 us  [swap(): return lax.all_to_all(v, axis, 0, 0, tiled=True)]
    ppermute x0 -> x15, waiting for transfers between devices: none -> 20.5 us  [the longest x12 19 us: shift(): return lax.ppermute(v, 'x', [(i, (i + k) % NX) for i in range(NX)])]
    ppermute x0 -> x15, starting transfers between devices: none -> 17.4 us  [the longest x12 17.4 us: shift(): return lax.ppermute(v, 'x', [(i, (i + k) % NX) for i in range(NX)])]
    dot_general x6 -> x0, matrix products: 8.47 us -> none  [the longest x2 4.59 us: half_step(): jnp.dot(scaled, gate_w.astype(jnp.bfloat16), preferred_element_type=jnp.f...]
    all_to_all x4 -> x5, starting transfers between devices: 23.6 us -> 27.7 us  [swap(): return lax.all_to_all(v, axis, 0, 0, tiled=True)]
  transfers between devices with their start and end apart: 12 -> 20, of which waited for: 12 -> 11; matrix products, arithmetic and copies ran while one was open for 2% -> 3% of each run, Pallas kernels for 0% -> 7%
where the time goes in v2:
time: 169 us; the launch traced here: 166 us
  waiting for transfers between devices  51 us (30%)
  starting transfers between devices  45.2 us (27%)
  blocking collectives  30.7 us (18%)
  Pallas kernels  29.2 us (17%)
  local copies, waits for them, and re-layouts  7.77 us (5%)
  other arithmetic  1.8 us (1%)
    all_to_all x2, blocking collectives, swap(): return lax.all_to_all(v, axis, 0, 0, tiled=True)  30.7 us
    all_to_all x5, waiting for transfers between devices, swap(): return lax.all_to_all(v, axis, 0, 0, tiled=True)  30.5 us
    all_to_all x5, starting transfers between devices, swap(): return lax.all_to_all(v, axis, 0, 0, tiled=True)  27.7 us
    ppermute x12, waiting for transfers between devices, shift(): return lax.ppermute(v, 'x', [(i, (i + k) % NX) for i in range(NX)])  19 us
    ppermute x12, starting transfers between devices, shift(): return lax.ppermute(v, 'x', [(i, (i + k) % NX) for i in range(NX)])  17.4 us
    unnamed x40, local copies, waits for them, and re-layouts  4.37 us
    pallas_call x1, Pallas kernels, local(): call(pack_second_body, [shape(N, 2 * WIDE)] * NX, 2, [chunks], 'pack_seco...  3.61 us
    pallas_call x1, Pallas kernels, local(): call(pack_first_body, [shape(N, WIDE + N)] * NX + [shape(N, WIDE)], 4, [c...  3.39 us
  transfers between devices with their start and end apart: 20, of which 11 were waited for; matrix products, arithmetic and copies ran while one was open for 3% of the time, Pallas kernels for 7%

profile of v2, /device:TPU:2, one launch (start us, length us, event | category | flops | bytes accessed | tf_op | source)
XLA Modules:
  0.0 165.8 jit_solution(6003213402452005424)
XLA Ops:
  0.6 3.4 %pack_first.1 = (bf16[128,896]{1,0:T(8,128)(2,1)}, bf16[128,896]{1,0:T(8,128)(2,1)}, bf16[128,896]{1,0:T(8,128)(2,1)}, bf16[128,896]{1,0:T(8,128)(2,1)}, bf16[128,768]{1,0:T(8,128)(2,1)}) custom-call(s32[3]{0:T(128)} %pad_add_fusion.at, f32[128,2816]{1,0:T(8,128)} %gate.1, f32[128,2816]{1,0:T(8,128)} %up.1, bf16[128,128]{1,0:T(8,128)(2,1)} %tokens.3, ...), custom_call_target="tpu_custom_call" | custom-call | tf_op jit(solution)/shard_map/pack_first/pallas_call | solution.py:254
  4.0 1.5 collective-permute-start
  5.5 2.8 %collective-permute-start.1 = (bf16[128,896]{1,0:T(8,128)(2,1)}, bf16[128,896]{1,0:T(8,128)(2,1)S(1)}, u32[]{:S(2)}, u32[]{:S(2)}) collective-permute-start(bf16[128,896]{1,0:T(8,128)(2,1)} %get-tuple-element.29), channel_id=1, source_target_pairs={{0,16},{8,24},{16,0},{24,8},{1,17},{9,25},{17,1},{25,9},{2,18},{10... | collective-permute-start | bytes 688136 | tf_op jit(solution)/shard_map/ppermute | solution.py:208
  8.7 4.1 %collective-permute-done.r1 = bf16[128,896]{1,0:T(8,128)(2,1)S(1)} collective-permute-done((bf16[128,896]{1,0:T(8,128)(2,1)}, bf16[128,896]{1,0:T(8,128)(2,1)S(1)}, u32[]{:S(2)}, u32[]{:S(2)}) %collective-permute-start) | collective-permute-done | bytes 229408 | tf_op jit(solution)/shard_map/ppermute | solution.py:208
  12.9 2.8 %collective-permute-done.1.r2 = bf16[128,896]{1,0:T(8,128)(2,1)S(1)} collective-permute-done((bf16[128,896]{1,0:T(8,128)(2,1)}, bf16[128,896]{1,0:T(8,128)(2,1)S(1)}, u32[]{:S(2)}, u32[]{:S(2)}) %collective-permute-start.1) | collective-permute-done | bytes 229408 | tf_op jit(solution)/shard_map/ppermute | solution.py:208
  15.7 2.6 %collective-permute-done.2.r3 = bf16[128,896]{1,0:T(8,128)(2,1)S(1)} collective-permute-done((bf16[128,896]{1,0:T(8,128)(2,1)}, bf16[128,896]{1,0:T(8,128)(2,1)S(1)}, u32[]{:S(2)}, u32[]{:S(2)}) %collective-permute-start.2) | collective-permute-done | bytes 229408 | tf_op jit(solution)/shard_map/ppermute | solution.py:208
  18.3 1.4 collective-permute-done.5.s3
  20.5 2.7 %enter_first.1 = bf16[8,2,16,768]{3,2,1,0:T(8,128)(2,1)} custom-call(s32[3]{0:T(128)} %pad_add_fusion.at, bf16[128,896]{1,0:T(8,128)(2,1)} %get-tuple-element.27.r0, bf16[128,896]{1,0:T(8,128)(2,1)} %copy-done.11, bf16[128,896]{1,0:T(8,128)(2,1)} %copy-done.12, bf16[128,896]{1,0:T(8,128)(2,1)} %copy-done.13, bf16[128,768]{1,0:T(8,128)(2,1)} %get-tuple-element.31.q0, ...), custom_call_target="tpu_custom_call" | custom-call | tf_op jit(solution)/shard_map/enter_first/pallas_call | solution.py:259
  23.2 8.7 %all-to-all-start = ((bf16[8,2,16,768]{3,2,1,0:T(8,128)(2,1)}), bf16[8,2,16,768]{3,2,1,0:T(8,128)(2,1)S(1)}, u32[]{:S(2)}, u32[]{:S(2)}) async-start(bf16[8,2,16,768]{3,2,1,0:T(8,128)(2,1)} %enter_first.1), calls=%async_computation | async-start | bytes 786432 | tf_op jit(solution)/shard_map/all_to_all | solution.py:220
  31.8 0.8 dynamic_slice.13
  32.7 0.8 dynamic_slice.12
  34.1 12.7 %all-to-all-done.got = bf16[8,2,16,768]{3,2,1,0:T(8,128)(2,1)S(1)} async-done(((bf16[8,2,16,768]{3,2,1,0:T(8,128)(2,1)}), bf16[8,2,16,768]{3,2,1,0:T(8,128)(2,1)S(1)}, u32[]{:S(2)}, u32[]{:S(2)}) %all-to-all-start) | async-done | bytes 393248 | tf_op jit(solution)/shard_map/all_to_all | solution.py:220
  46.8 0.7 copy-done.1
  47.5 1.8 %hidden_first.1 = bf16[8,2,16,384]{3,2,1,0:T(8,128)(2,1)} custom-call(s32[3]{0:T(128)} %pad_add_fusion.at, bf16[8,2,16,768]{3,2,1,0:T(8,128)(2,1)} %copy-done.1, f32[2,768]{1,0:T(2,128)} %select_maximum_fusion.1.scales), custom_call_target="tpu_custom_call" | custom-call | tf_op jit(solution)/shard_map/hidden_first/pallas_call | solution.py:279
  49.4 3.4 %all-to-all-start.1 = ((bf16[8,2,16,384]{3,2,1,0:T(8,128)(2,1)}), bf16[8,2,16,384]{3,2,1,0:T(8,128)(2,1)S(1)}, u32[]{:S(2)}, u32[]{:S(2)}) async-start(bf16[8,2,16,384]{3,2,1,0:T(8,128)(2,1)} %hidden_first.1), calls=%async_computation.1 | async-start | bytes 393216 | tf_op jit(solution)/shard_map/all_to_all | solution.py:220
  52.7 2.3 %pack_down.1 = (bf16[768,128]{1,0:T(8,128)(2,1)}, bf16[768,128]{1,0:T(8,128)(2,1)}, bf16[768,128]{1,0:T(8,128)(2,1)}, bf16[768,128]{1,0:T(8,128)(2,1)}) custom-call(s32[3]{0:T(128)} %pad_add_fusion.at, f32[2816,128]{1,0:T(8,128)} %down, f32[1,128]{1,0:T(1,128)} %bitcast.7), custom_call_target="tpu_custom_call" | custom-call | tf_op jit(solution)/shard_map/pack_down/pallas_call | solution.py:265
  55.1 1.3 collective-permute-start.6
  56.4 1.9 %collective-permute-start.7 = (bf16[768,128]{1,0:T(8,128)(2,1)}, bf16[768,128]{1,0:T(8,128)(2,1)S(1)}, u32[]{:S(2)}, u32[]{:S(2)}) collective-permute-start(bf16[768,128]{1,0:T(8,128)(2,1)} %get-tuple-element.36), channel_id=1, source_target_pairs={{0,16},{8,24},{16,0},{24,8},{1,17},{9,25},{17,1},{25,9},{2,18},{10... | collective-permute-start | bytes 589832 | tf_op jit(solution)/shard_map/ppermute | solution.py:208
  58.2 1.3 collective-permute-start.8
  59.5 3.6 %pack_second.1 = (bf16[128,1536]{1,0:T(8,128)(2,1)}, bf16[128,1536]{1,0:T(8,128)(2,1)}, bf16[128,1536]{1,0:T(8,128)(2,1)}, bf16[128,1536]{1,0:T(8,128)(2,1)}) custom-call(s32[3]{0:T(128)} %pad_add_fusion.at, f32[128,2816]{1,0:T(8,128)} %gate.2, f32[128,2816]{1,0:T(8,128)} %up.2), custom_call_target="tpu_custom_call" | custom-call | tf_op jit(solution)/shard_map/pack_second/pallas_call | solution.py:270
  63.1 0.7 collective-permute-start.9
  63.9 2.9 %collective-permute-start.10 = (bf16[128,1536]{1,0:T(8,128)(2,1)}, bf16[128,1536]{1,0:T(8,128)(2,1)S(1)}, u32[]{:S(2)}, u32[]{:S(2)}) collective-permute-start(bf16[128,1536]{1,0:T(8,128)(2,1)} %get-tuple-element.42), channel_id=1, source_target_pairs={{0,16},{8,24},{16,0},{24,8},{1,17},{9,25},{17,1},{25,9},{2,18},{10... | collective-permute-start | bytes 1179656 | tf_op jit(solution)/shard_map/ppermute | solution.py:208
  66.8 3.4 %collective-permute-done.8.d3 = bf16[768,128]{1,0:T(8,128)(2,1)S(1)} collective-permute-done((bf16[768,128]{1,0:T(8,128)(2,1)}, bf16[768,128]{1,0:T(8,128)(2,1)S(1)}, u32[]{:S(2)}, u32[]{:S(2)}) %collective-permute-start.8) | collective-permute-done | bytes 196640 | tf_op jit(solution)/shard_map/ppermute | solution.py:208
  70.9 2.3 %leave_first.1 = bf16[16,32,128]{2,1,0:T(8,128)(2,1)} custom-call(s32[3]{0:T(128)} %pad_add_fusion.at, bf16[8,2,16,384]{3,2,1,0:T(8,128)(2,1)} %copy-done.6, bf16[768,128]{1,0:T(8,128)(2,1)} %get-tuple-element.34.d0, bf16[768,128]{1,0:T(8,128)(2,1)} %copy-done.3, bf16[768,128]{1,0:T(8,128)(2,1)} %copy-done.4, bf16[768,128]{1,0:T(8,128)(2,1)} %copy-done.5), custom_call_target="tpu_custom_call" | custom-call | tf_op jit(solution)/shard_map/leave_first/pallas_call | solution.py:283
  73.2 16.3 %all_to_all.35.got = bf16[16,32,128]{2,1,0:T(8,128)(2,1)} all-to-all(bf16[16,32,128]{2,1,0:T(8,128)(2,1)} %leave_first.1), channel_id=1, replica_groups=mesh['z'=8,'x'=4,'y'=4,'c'=2] {'x','y'}, dimensions={0} | all-to-all | bytes 262144 | tf_op jit(solution)/shard_map/all_to_all | solution.py:220
  89.5 1.7 %stream.1 = f32[16,32,128]{2,1,0:T(8,128)} custom-call(s32[3]{0:T(128)} %pad_add_fusion.at, bf16[16,32,128]{2,1,0:T(8,128)(2,1)} %all_to_all.35.got, bf16[128,128]{1,0:T(8,128)(2,1)} %tokens.3, f32[1,128]{1,0:T(1,128)} %bitcast.9), custom_call_target="tpu_custom_call" | custom-call | tf_op jit(solution)/shard_map/stream/pallas_call | solution.py:287
  91.2 5.3 %all-to-all-start.3 = ((f32[16,32,128]{2,1,0:T(8,128)}), f32[16,32,128]{2,1,0:T(8,128)S(1)}, u32[]{:S(2)}, u32[]{:S(2)}) async-start(f32[16,32,128]{2,1,0:T(8,128)} %stream.1), calls=%async_computation.3 | async-start | bytes 524288 | tf_op jit(solution)/shard_map/all_to_all | solution.py:220
  96.6 6.7 %all-to-all-done.3.stream = f32[16,32,128]{2,1,0:T(8,128)S(1)} async-done(((f32[16,32,128]{2,1,0:T(8,128)}), f32[16,32,128]{2,1,0:T(8,128)S(1)}, u32[]{:S(2)}, u32[]{:S(2)}) %all-to-all-start.3) | async-done | bytes 262176 | tf_op jit(solution)/shard_map/all_to_all | solution.py:220
  103.4 0.7 copy-done
  104.1 2.9 %enter_second.1 = bf16[8,2,16,768]{3,2,1,0:T(8,128)(2,1)} custom-call(s32[3]{0:T(128)} %pad_add_fusion.at, f32[16,32,128]{2,1,0:T(8,128)} %copy-done, bf16[768,128]{1,0:T(8,128)(2,1)} %get-tuple-element.34.d0, bf16[768,128]{1,0:T(8,128)(2,1)} %copy-done.3, bf16[768,128]{1,0:T(8,128)(2,1)} %copy-done.4, bf16[768,128]{1,0:T(8,128)(2,1)} %copy-done.5, ...), custom_call_target="tpu_custom_call" | custom-call | tf_op jit(solution)/shard_map/enter_second/pallas_call | solution.py:292
  106.9 7.0 %all-to-all-start.4 = ((bf16[8,2,16,768]{3,2,1,0:T(8,128)(2,1)}), bf16[8,2,16,768]{3,2,1,0:T(8,128)(2,1)S(1)}, u32[]{:S(2)}, u32[]{:S(2)}) async-start(bf16[8,2,16,768]{3,2,1,0:T(8,128)(2,1)} %enter_second.1), calls=%async_computation.4 | async-start | bytes 786432 | tf_op jit(solution)/shard_map/all_to_all | solution.py:220
  113.9 0.8 dynamic_slice.15
  114.8 0.8 dynamic_slice.14
  116.2 11.1 %all-to-all-done.4.got = bf16[8,2,16,768]{3,2,1,0:T(8,128)(2,1)S(1)} async-done(((bf16[8,2,16,768]{3,2,1,0:T(8,128)(2,1)}), bf16[8,2,16,768]{3,2,1,0:T(8,128)(2,1)S(1)}, u32[]{:S(2)}, u32[]{:S(2)}) %all-to-all-start.4) | async-done | bytes 393248 | tf_op jit(solution)/shard_map/all_to_all | solution.py:220
  127.3 0.7 copy-done.2
  128.1 1.8 %hidden_second.1 = bf16[8,2,16,384]{3,2,1,0:T(8,128)(2,1)} custom-call(s32[3]{0:T(128)} %pad_add_fusion.at, bf16[8,2,16,768]{3,2,1,0:T(8,128)(2,1)} %copy-done.2, f32[2,768]{1,0:T(2,128)} %select_maximum_fusion.scales), custom_call_target="tpu_custom_call" | custom-call | tf_op jit(solution)/shard_map/hidden_second/pallas_call | solution.py:294
  129.9 3.4 %all-to-all-start.5 = ((bf16[8,2,16,384]{3,2,1,0:T(8,128)(2,1)}), bf16[8,2,16,384]{3,2,1,0:T(8,128)(2,1)S(1)}, u32[]{:S(2)}, u32[]{:S(2)}) async-start(bf16[8,2,16,384]{3,2,1,0:T(8,128)(2,1)} %hidden_second.1), calls=%async_computation.5 | async-start | bytes 393216 | tf_op jit(solution)/shard_map/all_to_all | solution.py:220
  133.3 2.4 %pack_last.1 = (bf16[768,128]{1,0:T(8,128)(2,1)}, bf16[768,128]{1,0:T(8,128)(2,1)}, bf16[768,128]{1,0:T(8,128)(2,1)}, bf16[768,128]{1,0:T(8,128)(2,1)}) custom-call(s32[3]{0:T(128)} %pad_add_fusion.at, f32[2816,128]{1,0:T(8,128)} %down.1, f32[1,128]{1,0:T(1,128)} %bitcast.8), custom_call_target="tpu_custom_call" | custom-call | tf_op jit(solution)/shard_map/pack_last/pallas_call | solution.py:275
  135.7 1.1 collective-permute-start.12
  136.7 2.8 %collective-permute-start.13 = (bf16[768,128]{1,0:T(8,128)(2,1)}, bf16[768,128]{1,0:T(8,128)(2,1)S(1)}, u32[]{:S(2)}, u32[]{:S(2)}) collective-permute-start(bf16[768,128]{1,0:T(8,128)(2,1)} %get-tuple-element.47), channel_id=1, source_target_pairs={{0,16},{8,24},{16,0},{24,8},{1,17},{9,25},{17,1},{25,9},{2,18},{10... | collective-permute-start | bytes 589832 | tf_op jit(solution)/shard_map/ppermute | solution.py:208
  139.5 0.8 collective-permute-start.14
  140.3 2.0 %collective-permute-done.12.d1 = bf16[768,128]{1,0:T(8,128)(2,1)S(1)} collective-permute-done((bf16[768,128]{1,0:T(8,128)(2,1)}, bf16[768,128]{1,0:T(8,128)(2,1)S(1)}, u32[]{:S(2)}, u32[]{:S(2)}) %collective-permute-start.12) | collective-permute-done | bytes 196640 | tf_op jit(solution)/shard_map/ppermute | solution.py:208
  142.2 2.1 %collective-permute-done.13.d2 = bf16[768,128]{1,0:T(8,128)(2,1)S(1)} collective-permute-done((bf16[768,128]{1,0:T(8,128)(2,1)}, bf16[768,128]{1,0:T(8,128)(2,1)S(1)}, u32[]{:S(2)}, u32[]{:S(2)}) %collective-permute-start.13) | collective-permute-done | bytes 196640 | tf_op jit(solution)/shard_map/ppermute | solution.py:208
  144.3 2.0 %collective-permute-done.14.d3 = bf16[768,128]{1,0:T(8,128)(2,1)S(1)} collective-permute-done((bf16[768,128]{1,0:T(8,128)(2,1)}, bf16[768,128]{1,0:T(8,128)(2,1)S(1)}, u32[]{:S(2)}, u32[]{:S(2)}) %collective-permute-start.14) | collective-permute-done | bytes 196640 | tf_op jit(solution)/shard_map/ppermute | solution.py:208
  146.4 0.7 copy-done.19
  147.1 2.4 %leave_second.1 = bf16[16,128,128]{2,1,0:T(8,128)(2,1)} custom-call(s32[3]{0:T(128)} %pad_add_fusion.at, bf16[8,2,16,384]{3,2,1,0:T(8,128)(2,1)} %copy-done.7, bf16[768,128]{1,0:T(8,128)(2,1)} %get-tuple-element.45.d0, bf16[768,128]{1,0:T(8,128)(2,1)} %copy-done.17, bf16[768,128]{1,0:T(8,128)(2,1)} %copy-done.18, bf16[768,128]{1,0:T(8,128)(2,1)} %copy-done.19), custom_call_target="tpu_custom_call" | custom-call | tf_op jit(solution)/shard_map/leave_second/pallas_call | solution.py:298
  149.6 14.4 %all_to_all.36.got = bf16[16,128,128]{2,1,0:T(8,128)(2,1)} all-to-all(bf16[16,128,128]{2,1,0:T(8,128)(2,1)} %leave_second.1), channel_id=1, replica_groups=mesh['z'=8,'x'=4,'y'=4,'c'=2] {'x','y'}, dimensions={0} | all-to-all | bytes 1048576 | tf_op jit(solution)/shard_map/all_to_all | solution.py:220
  163.9 1.8 %final.1 = f32[128,128]{1,0:T(8,128)} custom-call(s32[3]{0:T(128)} %pad_add_fusion.at, bf16[16,128,128]{2,1,0:T(8,128)(2,1)} %all_to_all.36.got, f32[16,32,128]{2,1,0:T(8,128)} %copy-done, f32[1,128]{1,0:T(1,128)} %bitcast.10), custom_call_target="tpu_custom_call" | custom-call | tf_op jit(solution)/shard_map/final/pallas_call | solution.py:302
  (57 shorter events, 4.1 us)
Async XLA Ops:
  4.0 8.9 %collective-permute-start = (bf16[128,896]{1,0:T(8,128)(2,1)}, bf16[128,896]{1,0:T(8,128)(2,1)S(1)}, u32[]{:S(2)}, u32[]{:S(2)}) collective-permute-start(bf16[128,896]{1,0:T(8,128)(2,1)} %get-tuple-element.28), channel_id=1, source_target_pairs={{0,8},{8,16},{16,24},{24,0},{1,9},{9,17},{17,25},{25,1},{2,10},{10... | collective-permute-start | bytes 688136 | tf_op jit(solution)/shard_map/ppermute | solution.py:208
  5.5 10.2 %collective-permute-start.1 = (bf16[128,896]{1,0:T(8,128)(2,1)}, bf16[128,896]{1,0:T(8,128)(2,1)S(1)}, u32[]{:S(2)}, u32[]{:S(2)}) collective-permute-start(bf16[128,896]{1,0:T(8,128)(2,1)} %get-tuple-element.29), channel_id=1, source_target_pairs={{0,16},{8,24},{16,0},{24,8},{1,17},{9,25},{17,1},{25,9},{2,18},{10... | collective-permute-start | bytes 688136 | tf_op jit(solution)/shard_map/ppermute | solution.py:208
  8.3 10.0 %collective-permute-start.2 = (bf16[128,896]{1,0:T(8,128)(2,1)}, bf16[128,896]{1,0:T(8,128)(2,1)S(1)}, u32[]{:S(2)}, u32[]{:S(2)}) collective-permute-start(bf16[128,896]{1,0:T(8,128)(2,1)} %get-tuple-element.30), channel_id=1, source_target_pairs={{0,24},{8,0},{16,8},{24,16},{1,25},{9,1},{17,9},{25,17},{2,26},{10... | collective-permute-start | bytes 688136 | tf_op jit(solution)/shard_map/ppermute | solution.py:208
  12.9 6.9 %copy-start.11 = (bf16[128,896]{1,0:T(8,128)(2,1)}, bf16[128,896]{1,0:T(8,128)(2,1)S(1)}, u32[]{:S(2)}) copy-start(bf16[128,896]{1,0:T(8,128)(2,1)S(1)} %collective-permute-done.r1) | copy-start | bytes 688132
  12.9 5.4 %collective-permute-start.3 = (bf16[128,896]{1,0:T(8,128)(2,1)S(1)}, bf16[128,896]{1,0:T(8,128)(2,1)S(1)}, u32[]{:S(2)}, u32[]{:S(2)}) collective-permute-start(bf16[128,896]{1,0:T(8,128)(2,1)S(1)} %collective-permute-done.r1), channel_id=1, source_target_pairs={{0,1},{1,0},{2,3},{3,2},{4,5},{5,4},{6,7},{7,6},{8,9},{9,8},{10,11... | collective-permute-start | bytes 688136 | tf_op jit(solution)/shard_map/ppermute | solution.py:212
  15.7 4.1 %copy-start.12 = (bf16[128,896]{1,0:T(8,128)(2,1)}, bf16[128,896]{1,0:T(8,128)(2,1)S(1)}, u32[]{:S(2)}) copy-start(bf16[128,896]{1,0:T(8,128)(2,1)S(1)} %collective-permute-done.1.r2) | copy-start | bytes 688132
  15.7 2.7 %collective-permute-start.4 = (bf16[128,896]{1,0:T(8,128)(2,1)S(1)}, bf16[128,896]{1,0:T(8,128)(2,1)S(1)}, u32[]{:S(2)}, u32[]{:S(2)}) collective-permute-start(bf16[128,896]{1,0:T(8,128)(2,1)S(1)} %collective-permute-done.1.r2), channel_id=1, source_target_pairs={{0,1},{1,0},{2,3},{3,2},{4,5},{5,4},{6,7},{7,6},{8,9},{9,8},{10,11... | collective-permute-start | bytes 688136 | tf_op jit(solution)/shard_map/ppermute | solution.py:212
  18.3 1.5 copy-start.13
  18.3 1.5 collective-permute-start.5
  18.3 1.5 copy-start.14
  18.3 1.5 copy-start.15
  19.8 0.7 copy-start.16
  23.2 23.6 %all-to-all-start = ((bf16[8,2,16,768]{3,2,1,0:T(8,128)(2,1)}), bf16[8,2,16,768]{3,2,1,0:T(8,128)(2,1)S(1)}, u32[]{:S(2)}, u32[]{:S(2)}) async-start(bf16[8,2,16,768]{3,2,1,0:T(8,128)(2,1)} %enter_first.1), calls=%async_computation | async-start | bytes 786432 | tf_op jit(solution)/shard_map/all_to_all | solution.py:220
  46.8 0.7 copy-start.1
  49.4 20.8 %all-to-all-start.1 = ((bf16[8,2,16,384]{3,2,1,0:T(8,128)(2,1)}), bf16[8,2,16,384]{3,2,1,0:T(8,128)(2,1)S(1)}, u32[]{:S(2)}, u32[]{:S(2)}) async-start(bf16[8,2,16,384]{3,2,1,0:T(8,128)(2,1)} %hidden_first.1), calls=%async_computation.1 | async-start | bytes 393216 | tf_op jit(solution)/shard_map/all_to_all | solution.py:220
  55.1 11.7 %collective-permute-start.6 = (bf16[768,128]{1,0:T(8,128)(2,1)}, bf16[768,128]{1,0:T(8,128)(2,1)S(1)}, u32[]{:S(2)}, u32[]{:S(2)}) collective-permute-start(bf16[768,128]{1,0:T(8,128)(2,1)} %get-tuple-element.35), channel_id=1, source_target_pairs={{0,8},{8,16},{16,24},{24,0},{1,9},{9,17},{17,25},{25,1},{2,10},{10... | collective-permute-start | bytes 589832 | tf_op jit(solution)/shard_map/ppermute | solution.py:208
  56.4 10.4 %collective-permute-start.7 = (bf16[768,128]{1,0:T(8,128)(2,1)}, bf16[768,128]{1,0:T(8,128)(2,1)S(1)}, u32[]{:S(2)}, u32[]{:S(2)}) collective-permute-start(bf16[768,128]{1,0:T(8,128)(2,1)} %get-tuple-element.36), channel_id=1, source_target_pairs={{0,16},{8,24},{16,0},{24,8},{1,17},{9,25},{17,1},{25,9},{2,18},{10... | collective-permute-start | bytes 589832 | tf_op jit(solution)/shard_map/ppermute | solution.py:208
  58.2 12.0 %collective-permute-start.8 = (bf16[768,128]{1,0:T(8,128)(2,1)}, bf16[768,128]{1,0:T(8,128)(2,1)S(1)}, u32[]{:S(2)}, u32[]{:S(2)}) collective-permute-start(bf16[768,128]{1,0:T(8,128)(2,1)} %get-tuple-element.37), channel_id=1, source_target_pairs={{0,24},{8,0},{16,8},{24,16},{1,25},{9,1},{17,9},{25,17},{2,26},{10... | collective-permute-start | bytes 589832 | tf_op jit(solution)/shard_map/ppermute | solution.py:208
  63.1 33.4 %collective-permute-start.9 = (bf16[128,1536]{1,0:T(8,128)(2,1)}, bf16[128,1536]{1,0:T(8,128)(2,1)S(1)}, u32[]{:S(2)}, u32[]{:S(2)}) collective-permute-start(bf16[128,1536]{1,0:T(8,128)(2,1)} %get-tuple-element.41), channel_id=1, source_target_pairs={{0,8},{8,16},{16,24},{24,0},{1,9},{9,17},{17,25},{25,1},{2,10},{10... | collective-permute-start | bytes 1179656 | tf_op jit(solution)/shard_map/ppermute | solution.py:208
  63.9 32.7 %collective-permute-start.10 = (bf16[128,1536]{1,0:T(8,128)(2,1)}, bf16[128,1536]{1,0:T(8,128)(2,1)S(1)}, u32[]{:S(2)}, u32[]{:S(2)}) collective-permute-start(bf16[128,1536]{1,0:T(8,128)(2,1)} %get-tuple-element.42), channel_id=1, source_target_pairs={{0,16},{8,24},{16,0},{24,8},{1,17},{9,25},{17,1},{25,9},{2,18},{10... | collective-permute-start | bytes 1179656 | tf_op jit(solution)/shard_map/ppermute | solution.py:208
  66.7 3.4 %copy-start.3 = (bf16[768,128]{1,0:T(8,128)(2,1)}, bf16[768,128]{1,0:T(8,128)(2,1)S(1)}, u32[]{:S(2)}) copy-start(bf16[768,128]{1,0:T(8,128)(2,1)S(1)} %collective-permute-done.6.d1) | copy-start | bytes 589828
  66.7 29.8 %collective-permute-start.11 = (bf16[128,1536]{1,0:T(8,128)(2,1)}, bf16[128,1536]{1,0:T(8,128)(2,1)S(1)}, u32[]{:S(2)}, u32[]{:S(2)}) collective-permute-start(bf16[128,1536]{1,0:T(8,128)(2,1)} %get-tuple-element.43), channel_id=1, source_target_pairs={{0,24},{8,0},{16,8},{24,16},{1,25},{9,1},{17,9},{25,17},{2,26},{10... | collective-permute-start | bytes 1179656 | tf_op jit(solution)/shard_map/ppermute | solution.py:208
  66.8 3.4 %copy-start.4 = (bf16[768,128]{1,0:T(8,128)(2,1)}, bf16[768,128]{1,0:T(8,128)(2,1)S(1)}, u32[]{:S(2)}) copy-start(bf16[768,128]{1,0:T(8,128)(2,1)S(1)} %collective-permute-done.7.d2) | copy-start | bytes 589828
  70.2 0.7 copy-start.5
  70.2 0.8 copy-start.6
  91.2 12.1 %all-to-all-start.3 = ((f32[16,32,128]{2,1,0:T(8,128)}), f32[16,32,128]{2,1,0:T(8,128)S(1)}, u32[]{:S(2)}, u32[]{:S(2)}) async-start(f32[16,32,128]{2,1,0:T(8,128)} %stream.1), calls=%async_computation.3 | async-start | bytes 524288 | tf_op jit(solution)/shard_map/all_to_all | solution.py:220
  96.6 6.8 %copy-start.8 = (bf16[128,1536]{1,0:T(8,128)(2,1)}, bf16[128,1536]{1,0:T(8,128)(2,1)S(1)}, u32[]{:S(2)}) copy-start(bf16[128,1536]{1,0:T(8,128)(2,1)S(1)} %collective-permute-done.9.w1) | copy-start | bytes 1179652
  96.6 6.8 %copy-start.9 = (bf16[128,1536]{1,0:T(8,128)(2,1)}, bf16[128,1536]{1,0:T(8,128)(2,1)S(1)}, u32[]{:S(2)}) copy-start(bf16[128,1536]{1,0:T(8,128)(2,1)S(1)} %collective-permute-done.10.w2) | copy-start | bytes 1179652
  96.6 6.8 %copy-start.10 = (bf16[128,1536]{1,0:T(8,128)(2,1)}, bf16[128,1536]{1,0:T(8,128)(2,1)S(1)}, u32[]{:S(2)}) copy-start(bf16[128,1536]{1,0:T(8,128)(2,1)S(1)} %collective-permute-done.11.w3) | copy-start | bytes 1179652
  103.4 0.7 copy-start
  106.9 20.4 %all-to-all-start.4 = ((bf16[8,2,16,768]{3,2,1,0:T(8,128)(2,1)}), bf16[8,2,16,768]{3,2,1,0:T(8,128)(2,1)S(1)}, u32[]{:S(2)}, u32[]{:S(2)}) async-start(bf16[8,2,16,768]{3,2,1,0:T(8,128)(2,1)} %enter_second.1), calls=%async_computation.4 | async-start | bytes 786432 | tf_op jit(solution)/shard_map/all_to_all | solution.py:220
  127.3 0.7 copy-start.2
  129.9 16.4 %all-to-all-start.5 = ((bf16[8,2,16,384]{3,2,1,0:T(8,128)(2,1)}), bf16[8,2,16,384]{3,2,1,0:T(8,128)(2,1)S(1)}, u32[]{:S(2)}, u32[]{:S(2)}) async-start(bf16[8,2,16,384]{3,2,1,0:T(8,128)(2,1)} %hidden_second.1), calls=%async_computation.5 | async-start | bytes 393216 | tf_op jit(solution)/shard_map/all_to_all | solution.py:220
  135.7 6.6 %collective-permute-start.12 = (bf16[768,128]{1,0:T(8,128)(2,1)}, bf16[768,128]{1,0:T(8,128)(2,1)S(1)}, u32[]{:S(2)}, u32[]{:S(2)}) collective-permute-start(bf16[768,128]{1,0:T(8,128)(2,1)} %get-tuple-element.46), channel_id=1, source_target_pairs={{0,8},{8,16},{16,24},{24,0},{1,9},{9,17},{17,25},{25,1},{2,10},{10... | collective-permute-start | bytes 589832 | tf_op jit(solution)/shard_map/ppermute | solution.py:208
  136.7 7.6 %collective-permute-start.13 = (bf16[768,128]{1,0:T(8,128)(2,1)}, bf16[768,128]{1,0:T(8,128)(2,1)S(1)}, u32[]{:S(2)}, u32[]{:S(2)}) collective-permute-start(bf16[768,128]{1,0:T(8,128)(2,1)} %get-tuple-element.47), channel_id=1, source_target_pairs={{0,16},{8,24},{16,0},{24,8},{1,17},{9,25},{17,1},{25,9},{2,18},{10... | collective-permute-start | bytes 589832 | tf_op jit(solution)/shard_map/ppermute | solution.py:208
  139.5 6.8 %collective-permute-start.14 = (bf16[768,128]{1,0:T(8,128)(2,1)}, bf16[768,128]{1,0:T(8,128)(2,1)S(1)}, u32[]{:S(2)}, u32[]{:S(2)}) collective-permute-start(bf16[768,128]{1,0:T(8,128)(2,1)} %get-tuple-element.48), channel_id=1, source_target_pairs={{0,24},{8,0},{16,8},{24,16},{1,25},{9,1},{17,9},{25,17},{2,26},{10... | collective-permute-start | bytes 589832 | tf_op jit(solution)/shard_map/ppermute | solution.py:208
  142.2 4.1 %copy-start.17 = (bf16[768,128]{1,0:T(8,128)(2,1)}, bf16[768,128]{1,0:T(8,128)(2,1)S(1)}, u32[]{:S(2)}) copy-start(bf16[768,128]{1,0:T(8,128)(2,1)S(1)} %collective-permute-done.12.d1) | copy-start | bytes 589828
  144.3 2.0 %copy-start.18 = (bf16[768,128]{1,0:T(8,128)(2,1)}, bf16[768,128]{1,0:T(8,128)(2,1)S(1)}, u32[]{:S(2)}) copy-start(bf16[768,128]{1,0:T(8,128)(2,1)S(1)} %collective-permute-done.13.d2) | copy-start | bytes 589828
  146.3 0.7 copy-start.19
  146.3 0.8 copy-start.7

commit v3 on v2

--- a/solution.py
+++ b/solution.py
@@ -5,6 +5,7 @@
 from jax.experimental.pallas import tpu as pltpu
 from jax.sharding import Mesh
 from jax.sharding import PartitionSpec as P
+
 
 BF = jnp.bfloat16
 F32 = jnp.float32
@@ -16,6 +17,7 @@
 WIDE = 2 * PAD
 CHUNK = 2 * HALF
 WIDTH = 4096
+LIMIT = 16 * 2**20
 
 SMEM = pl.BlockSpec(memory_space=pltpu.SMEM)
 VMEM = pl.BlockSpec(memory_space=pltpu.VMEM)
@@ -25,7 +27,7 @@
     return jax.ShapeDtypeStruct(dims, dtype)
 
 
-def call(body, outs, n_in, scratch=(), name=None):
+def call(body, outs, n_in, scratch=()):
     many = isinstance(outs, (list, tuple))
     return pl.pallas_call(
         body,
@@ -33,7 +35,7 @@
         in_specs=[SMEM] + [VMEM] * n_in,
         out_specs=[VMEM] * len(outs) if many else VMEM,
         scratch_shapes=list(scratch),
-        name=name,
+        compiler_params=pltpu.CompilerParams(vmem_limit_bytes=LIMIT),
     )
 
 
@@ -252,54 +254,50 @@
     spread = shape(NZ, 2, N // NZ, PAD)
 
     *packed, other = call(
-        pack_first_body, [shape(N, WIDE + N)] * NX + [shape(N, WIDE)], 4, [chunks], "pack_first"
+        pack_first_body, [shape(N, WIDE + N)] * NX + [shape(N, WIDE)], 4, [chunks]
     )(at, first_gate, first_up, tokens, first_gain[None])
     mine = around(packed)
     theirs = [other] + [other_core(v) for v in mine[1:]]
-    sums = call(enter_first_body, payload, 8, name="enter_first")(at, *mine, *theirs)
+    sums = call(enter_first_body, payload, 8)(at, *mine, *theirs)
     sums, first_down, second_gate, second_up, second_down = lax.optimization_barrier(
         (sums, first_down, second_gate, second_up, second_down)
     )
     got = swap(sums, "z")
     downs = around(
-        call(pack_down_body, [shape(2 * PAD, N)] * NX, 2, name="pack_down")(
+        call(pack_down_body, [shape(2 * PAD, N)] * NX, 2)(
             at, first_down, second_gain[None]
-        )
+        ),
     )
     ups = around(
-        call(pack_second_body, [shape(N, 2 * WIDE)] * NX, 2, [chunks], "pack_second")(
+        call(pack_second_body, [shape(N, 2 * WIDE)] * NX, 2, [chunks])(
             at, second_gate, second_up
-        )
+        ),
     )
     last_downs = around(
-        call(pack_down_body, [shape(2 * PAD, N)] * NX, 2, name="pack_last")(
+        call(pack_down_body, [shape(2 * PAD, N)] * NX, 2)(
             at, second_down, second_gain[None]
-        )
-    )
-    hidden = call(hidden_body, spread, 2, name="hidden_first")(
+        ),
+    )
+    hidden = call(hidden_body, spread, 2)(
         at, got, scale_rows(first_gate_scale, first_up_scale, x)
     )
     hidden = swap(hidden, "z")
-    part = call(leave_first_body, shape(NX * NY, N // NY, N), 5, name="leave_first")(
-        at, hidden, *downs
-    )
+    part = call(leave_first_body, shape(NX * NY, N // NY, N), 5)(at, hidden, *downs)
     got = swap(part, XY)
-    stream = call(stream_body, shape(NX * NY, N // NY, N, dtype=F32), 3, name="stream")(
+    stream = call(stream_body, shape(NX * NY, N // NY, N, dtype=F32), 3)(
         at, got, tokens, first_down_scale[None]
     )
     stream = swap(stream, XY)
 
-    sums = call(enter_second_body, payload, 9, name="enter_second")(at, stream, *downs, *ups)
+    sums = call(enter_second_body, payload, 9)(at, stream, *downs, *ups)
     got = swap(sums, "z")
-    hidden = call(hidden_body, spread, 2, name="hidden_second")(
+    hidden = call(hidden_body, spread, 2)(
         at, got, scale_rows(second_gate_scale, second_up_scale, x)
     )
     hidden = swap(hidden, "z")
-    part = call(leave_second_body, shape(NX * NY, N, N), 5, name="leave_second")(
-        at, hidden, *last_downs
-    )
+    part = call(leave_second_body, shape(NX * NY, N, N), 5)(at, hidden, *last_downs)
     got = swap(part, XY)
-    return call(final_body, shape(N, N, dtype=F32), 3, name="final")(
+    return call(final_body, shape(N, N, dtype=F32), 3)(
         at, got, stream, second_down_scale[None]
     )
 

time: 169 us -> 156 us (0.923)
  Pallas kernels: 29.2 us -> 15 us
  blocking collectives: 30.7 us -> 32.5 us
  other arithmetic: 1.8 us -> 0.09 us
    pallas_call x11, Pallas kernels: 25.8 us -> 13.9 us  [the longest x2 2.7 us: local(): call(hidden_body, spread, 2)]
    pallas_call x1, Pallas kernels: 3.39 us -> 1.08 us  [local(): call(pack_first_body, [shape(N, WIDE + N)] * NX + [shape(N, WIDE)], 4, [c...]
    all_to_all x2, blocking collectives: 30.7 us -> 32.5 us  [swap(): return lax.all_to_all(v, axis, 0, 0, tiled=True)]
    unnamed x40 -> x24, local copies, waits for them, and re-layouts: 4.37 us -> 5.53 us
  transfers between devices with their start and end apart: 20 -> 20, of which waited for: 11 -> 11; matrix products, arithmetic and copies ran while one was open for 3% -> 2% of each run, Pallas kernels for 7% -> 4%
where the time goes in v3:
time: 156 us; the launch traced here: 154 us
  waiting for transfers between devices  51.6 us (33%)
  starting transfers between devices  45.5 us (29%)
  blocking collectives  32.5 us (21%)
  Pallas kernels  15 us (10%)
  local copies, waits for them, and re-layouts  9.04 us (6%)
    all_to_all x2, blocking collectives, swap(): return lax.all_to_all(v, axis, 0, 0, tiled=True)  32.5 us
    all_to_all x5, waiting for transfers between devices, swap(): return lax.all_to_all(v, axis, 0, 0, tiled=True)  31.6 us
    all_to_all x5, starting transfers between devices, swap(): return lax.all_to_all(v, axis, 0, 0, tiled=True)  27.9 us
    ppermute x12, waiting for transfers between devices, shift(): return lax.ppermute(v, 'x', [(i, (i + k) % NX) for i in range(NX)])  18.5 us
    ppermute x12, starting transfers between devices, shift(): return lax.ppermute(v, 'x', [(i, (i + k) % NX) for i in range(NX)])  17.6 us
    unnamed x24, local copies, waits for them, and re-layouts  5.53 us
    dynamic_slice x4, local copies, waits for them, and re-layouts, scale_rows(): own = lax.dynamic_slice_in_dim(scale, x * CHUNK, CHUNK, 0).reshape(2, HALF)  3.2 us
  transfers between devices with their start and end apart: 20, of which 11 were waited for; matrix products, arithmetic and copies ran while one was open for 2% of the time, Pallas kernels for 4%

profile of v3, /device:TPU:2, one launch (start us, length us, event | category | flops | bytes accessed | tf_op | source)
XLA Modules:
  0.0 153.9 jit_solution(12516396817352714786)
XLA Ops:
  0.1 1.4 copy-done.4
  1.4 1.4 copy-done.5
  2.8 0.8 copy-done.6
  3.6 0.7 copy-done.11
  4.2 1.1 shard_map.145
  5.3 1.6 %collective-permute-start = (bf16[128,896]{1,0:T(8,128)(2,1)S(1)}, bf16[128,896]{1,0:T(8,128)(2,1)S(1)}, u32[]{:S(2)}, u32[]{:S(2)}) collective-permute-start(bf16[128,896]{1,0:T(8,128)(2,1)S(1)} %get-tuple-element.28), channel_id=1, source_target_pairs={{0,8},{8,16},{16,24},{24,0},{1,9},{9,17},{17,25},{25,1},{2,10},{10... | collective-permute-start | bytes 688136 | tf_op jit(solution)/shard_map/ppermute | solution.py:210
  6.9 2.8 %collective-permute-start.1 = (bf16[128,896]{1,0:T(8,128)(2,1)S(1)}, bf16[128,896]{1,0:T(8,128)(2,1)S(1)}, u32[]{:S(2)}, u32[]{:S(2)}) collective-permute-start(bf16[128,896]{1,0:T(8,128)(2,1)S(1)} %get-tuple-element.29), channel_id=1, source_target_pairs={{0,16},{8,24},{16,0},{24,8},{1,17},{9,25},{17,1},{25,9},{2,18},{10... | collective-permute-start | bytes 688136 | tf_op jit(solution)/shard_map/ppermute | solution.py:210
  10.1 3.9 %collective-permute-done.r1 = bf16[128,896]{1,0:T(8,128)(2,1)S(1)} collective-permute-done((bf16[128,896]{1,0:T(8,128)(2,1)S(1)}, bf16[128,896]{1,0:T(8,128)(2,1)S(1)}, u32[]{:S(2)}, u32[]{:S(2)}) %collective-permute-start) | collective-permute-done | bytes 229408 | tf_op jit(solution)/shard_map/ppermute | solution.py:210
  14.1 2.8 %collective-permute-done.1.r2 = bf16[128,896]{1,0:T(8,128)(2,1)S(1)} collective-permute-done((bf16[128,896]{1,0:T(8,128)(2,1)S(1)}, bf16[128,896]{1,0:T(8,128)(2,1)S(1)}, u32[]{:S(2)}, u32[]{:S(2)}) %collective-permute-start.1) | collective-permute-done | bytes 229408 | tf_op jit(solution)/shard_map/ppermute | solution.py:210
  16.9 2.7 %collective-permute-done.2.r3 = bf16[128,896]{1,0:T(8,128)(2,1)S(1)} collective-permute-done((bf16[128,896]{1,0:T(8,128)(2,1)S(1)}, bf16[128,896]{1,0:T(8,128)(2,1)S(1)}, u32[]{:S(2)}, u32[]{:S(2)}) %collective-permute-start.2) | collective-permute-done | bytes 229408 | tf_op jit(solution)/shard_map/ppermute | solution.py:210
  19.6 1.5 collective-permute-done.5.s3
  21.1 1.7 %shard_map.146 = bf16[8,2,16,768]{3,2,1,0:T(8,128)(2,1)} custom-call(s32[3]{0:T(128)S(1)} %pad_add_fusion.at, bf16[128,896]{1,0:T(8,128)(2,1)S(1)} %get-tuple-element.27.r0, bf16[128,896]{1,0:T(8,128)(2,1)S(1)} %collective-permute-done.r1, bf16[128,896]{1,0:T(8,128)(2,1)S(1)} %collective-permute-done.1.r2, bf16[128,896]{1,0:T(8,128)(2,1)S(1)} %collective-permute-done.2.r3, ...), custom_call_target="tpu_custom_call" | custom-call | tf_op jit(solution)/shard_map/pallas_call | solution.py:261
  22.8 8.7 %all-to-all-start = ((bf16[8,2,16,768]{3,2,1,0:T(8,128)(2,1)}), bf16[8,2,16,768]{3,2,1,0:T(8,128)(2,1)S(1)}, u32[]{:S(2)}, u32[]{:S(2)}) async-start(bf16[8,2,16,768]{3,2,1,0:T(8,128)(2,1)} %shard_map.146), calls=%async_computation | async-start | bytes 786432 | tf_op jit(solution)/shard_map/all_to_all | solution.py:222
  31.5 0.9 dynamic_slice.13
  32.4 0.8 dynamic_slice.12
  33.3 13.2 %all-to-all-done.got = bf16[8,2,16,768]{3,2,1,0:T(8,128)(2,1)S(1)} async-done(((bf16[8,2,16,768]{3,2,1,0:T(8,128)(2,1)}), bf16[8,2,16,768]{3,2,1,0:T(8,128)(2,1)S(1)}, u32[]{:S(2)}, u32[]{:S(2)}) %all-to-all-start) | async-done | bytes 393248 | tf_op jit(solution)/shard_map/all_to_all | solution.py:222
  46.4 1.4 shard_map.147
  47.8 3.4 %all-to-all-start.1 = ((bf16[8,2,16,384]{3,2,1,0:T(8,128)(2,1)}), bf16[8,2,16,384]{3,2,1,0:T(8,128)(2,1)S(1)}, u32[]{:S(2)}, u32[]{:S(2)}) async-start(bf16[8,2,16,384]{3,2,1,0:T(8,128)(2,1)} %shard_map.147), calls=%async_computation.1 | async-start | bytes 393216 | tf_op jit(solution)/shard_map/all_to_all | solution.py:222
  51.2 0.6 shard_map.148
  51.8 1.4 collective-permute-start.6
  53.2 1.9 %collective-permute-start.7 = (bf16[768,128]{1,0:T(8,128)(2,1)S(1)}, bf16[768,128]{1,0:T(8,128)(2,1)S(1)}, u32[]{:S(2)}, u32[]{:S(2)}) collective-permute-start(bf16[768,128]{1,0:T(8,128)(2,1)S(1)} %get-tuple-element.36), channel_id=1, source_target_pairs={{0,16},{8,24},{16,0},{24,8},{1,17},{9,25},{17,1},{25,9},{2,18},{10... | collective-permute-start | bytes 589832 | tf_op jit(solution)/shard_map/ppermute | solution.py:210
  55.1 1.3 collective-permute-start.8
  56.3 1.4 copy-done.2
  57.7 2.2 %shard_map.151 = (bf16[128,1536]{1,0:T(8,128)(2,1)S(1)}, bf16[128,1536]{1,0:T(8,128)(2,1)}, bf16[128,1536]{1,0:T(8,128)(2,1)}, bf16[128,1536]{1,0:T(8,128)(2,1)}) custom-call(s32[3]{0:T(128)S(1)} %pad_add_fusion.at, f32[128,2816]{1,0:T(8,128)S(1)} %copy-done.1, f32[128,2816]{1,0:T(8,128)S(1)} %copy-done.2), custom_call_target="tpu_custom_call" | custom-call | tf_op jit(solution)/shard_map/pallas_call | solution.py:272
  59.9 0.7 collective-permute-start.9
  60.7 2.9 %collective-permute-start.10 = (bf16[128,1536]{1,0:T(8,128)(2,1)}, bf16[128,1536]{1,0:T(8,128)(2,1)S(1)}, u32[]{:S(2)}, u32[]{:S(2)}) collective-permute-start(bf16[128,1536]{1,0:T(8,128)(2,1)} %get-tuple-element.42), channel_id=1, source_target_pairs={{0,16},{8,24},{16,0},{24,8},{1,17},{9,25},{17,1},{25,9},{2,18},{10... | collective-permute-start | bytes 1179656 | tf_op jit(solution)/shard_map/ppermute | solution.py:210
  63.6 3.2 %collective-permute-done.8.d3 = bf16[768,128]{1,0:T(8,128)(2,1)S(1)} collective-permute-done((bf16[768,128]{1,0:T(8,128)(2,1)S(1)}, bf16[768,128]{1,0:T(8,128)(2,1)S(1)}, u32[]{:S(2)}, u32[]{:S(2)}) %collective-permute-start.8) | collective-permute-done | bytes 196640 | tf_op jit(solution)/shard_map/ppermute | solution.py:210
  66.8 0.9 shard_map.149
  67.7 18.4 %all_to_all.35.got = bf16[16,32,128]{2,1,0:T(8,128)(2,1)S(1)} all-to-all(bf16[16,32,128]{2,1,0:T(8,128)(2,1)S(1)} %shard_map.149), channel_id=1, replica_groups=mesh['z'=8,'x'=4,'y'=4,'c'=2] {'x','y'}, dimensions={0} | all-to-all | bytes 262144 | tf_op jit(solution)/shard_map/all_to_all | solution.py:222
  86.1 1.3 shard_map.150
  87.4 5.3 %all-to-all-start.3 = ((f32[16,32,128]{2,1,0:T(8,128)}), f32[16,32,128]{2,1,0:T(8,128)S(1)}, u32[]{:S(2)}, u32[]{:S(2)}) async-start(f32[16,32,128]{2,1,0:T(8,128)} %shard_map.150), calls=%async_computation.3 | async-start | bytes 524288 | tf_op jit(solution)/shard_map/all_to_all | solution.py:222
  92.7 6.8 %all-to-all-done.3.stream = f32[16,32,128]{2,1,0:T(8,128)S(1)} async-done(((f32[16,32,128]{2,1,0:T(8,128)}), f32[16,32,128]{2,1,0:T(8,128)S(1)}, u32[]{:S(2)}, u32[]{:S(2)}) %all-to-all-start.3) | async-done | bytes 262176 | tf_op jit(solution)/shard_map/all_to_all | solution.py:222
  99.5 1.7 %shard_map.152 = bf16[8,2,16,768]{3,2,1,0:T(8,128)(2,1)} custom-call(s32[3]{0:T(128)S(1)} %pad_add_fusion.at, f32[16,32,128]{2,1,0:T(8,128)S(1)} %all-to-all-done.3.stream, bf16[768,128]{1,0:T(8,128)(2,1)S(1)} %get-tuple-element.34.d0, bf16[768,128]{1,0:T(8,128)(2,1)S(1)} %collective-permute-done.6.d1, bf16[768,128]{1,0:T(8,128)(2,1)S(1)} %collective-permute-done.7.d2, ...), custom_call_target="tpu_custom_call" | custom-call | tf_op jit(solution)/shard_map/pallas_call | solution.py:292
  101.2 7.1 %all-to-all-start.4 = ((bf16[8,2,16,768]{3,2,1,0:T(8,128)(2,1)}), bf16[8,2,16,768]{3,2,1,0:T(8,128)(2,1)S(1)}, u32[]{:S(2)}, u32[]{:S(2)}) async-start(bf16[8,2,16,768]{3,2,1,0:T(8,128)(2,1)} %shard_map.152), calls=%async_computation.4 | async-start | bytes 786432 | tf_op jit(solution)/shard_map/all_to_all | solution.py:222
  108.3 0.8 dynamic_slice.15
  109.1 0.8 dynamic_slice.14
  110.0 11.7 %all-to-all-done.4.got = bf16[8,2,16,768]{3,2,1,0:T(8,128)(2,1)S(1)} async-done(((bf16[8,2,16,768]{3,2,1,0:T(8,128)(2,1)}), bf16[8,2,16,768]{3,2,1,0:T(8,128)(2,1)S(1)}, u32[]{:S(2)}, u32[]{:S(2)}) %all-to-all-start.4) | async-done | bytes 393248 | tf_op jit(solution)/shard_map/all_to_all | solution.py:222
  121.7 1.3 shard_map.153
  123.0 3.4 %all-to-all-start.5 = ((bf16[8,2,16,384]{3,2,1,0:T(8,128)(2,1)}), bf16[8,2,16,384]{3,2,1,0:T(8,128)(2,1)S(1)}, u32[]{:S(2)}, u32[]{:S(2)}) async-start(bf16[8,2,16,384]{3,2,1,0:T(8,128)(2,1)} %shard_map.153), calls=%async_computation.5 | async-start | bytes 393216 | tf_op jit(solution)/shard_map/all_to_all | solution.py:222
  127.1 1.2 collective-permute-start.12
  128.2 2.8 %collective-permute-start.13 = (bf16[768,128]{1,0:T(8,128)(2,1)S(1)}, bf16[768,128]{1,0:T(8,128)(2,1)S(1)}, u32[]{:S(2)}, u32[]{:S(2)}) collective-permute-start(bf16[768,128]{1,0:T(8,128)(2,1)S(1)} %get-tuple-element.47), channel_id=1, source_target_pairs={{0,16},{8,24},{16,0},{24,8},{1,17},{9,25},{17,1},{25,9},{2,18},{10... | collective-permute-start | bytes 589832 | tf_op jit(solution)/shard_map/ppermute | solution.py:210
  131.0 0.8 collective-permute-start.14
  131.8 1.8 %collective-permute-done.12.d1 = bf16[768,128]{1,0:T(8,128)(2,1)S(1)} collective-permute-done((bf16[768,128]{1,0:T(8,128)(2,1)S(1)}, bf16[768,128]{1,0:T(8,128)(2,1)S(1)}, u32[]{:S(2)}, u32[]{:S(2)}) %collective-permute-start.12) | collective-permute-done | bytes 196640 | tf_op jit(solution)/shard_map/ppermute | solution.py:210
  133.5 2.1 %collective-permute-done.13.d2 = bf16[768,128]{1,0:T(8,128)(2,1)S(1)} collective-permute-done((bf16[768,128]{1,0:T(8,128)(2,1)S(1)}, bf16[768,128]{1,0:T(8,128)(2,1)S(1)}, u32[]{:S(2)}, u32[]{:S(2)}) %collective-permute-start.13) | collective-permute-done | bytes 196640 | tf_op jit(solution)/shard_map/ppermute | solution.py:210
  135.6 2.0 %collective-permute-done.14.d3 = bf16[768,128]{1,0:T(8,128)(2,1)S(1)} collective-permute-done((bf16[768,128]{1,0:T(8,128)(2,1)S(1)}, bf16[768,128]{1,0:T(8,128)(2,1)S(1)}, u32[]{:S(2)}, u32[]{:S(2)}) %collective-permute-start.14) | collective-permute-done | bytes 196640 | tf_op jit(solution)/shard_map/ppermute | solution.py:210
  137.6 0.9 shard_map.155
  138.5 14.1 %all_to_all.36.got = bf16[16,128,128]{2,1,0:T(8,128)(2,1)S(1)} all-to-all(bf16[16,128,128]{2,1,0:T(8,128)(2,1)S(1)} %shard_map.155), channel_id=1, replica_groups=mesh['z'=8,'x'=4,'y'=4,'c'=2] {'x','y'}, dimensions={0} | all-to-all | bytes 1048576 | tf_op jit(solution)/shard_map/all_to_all | solution.py:222
  152.6 1.3 shard_map.156
  (41 shorter events, 1.5 us)
Async XLA Ops:
  0.1 1.4 copy-start.4
  1.4 1.4 copy-start.5
  2.8 0.8 copy-start.6
  3.6 0.7 copy-start.11
  5.3 8.8 %collective-permute-start = (bf16[128,896]{1,0:T(8,128)(2,1)S(1)}, bf16[128,896]{1,0:T(8,128)(2,1)S(1)}, u32[]{:S(2)}, u32[]{:S(2)}) collective-permute-start(bf16[128,896]{1,0:T(8,128)(2,1)S(1)} %get-tuple-element.28), channel_id=1, source_target_pairs={{0,8},{8,16},{16,24},{24,0},{1,9},{9,17},{17,25},{25,1},{2,10},{10... | collective-permute-start | bytes 688136 | tf_op jit(solution)/shard_map/ppermute | solution.py:210
  6.9 10.0 %collective-permute-start.1 = (bf16[128,896]{1,0:T(8,128)(2,1)S(1)}, bf16[128,896]{1,0:T(8,128)(2,1)S(1)}, u32[]{:S(2)}, u32[]{:S(2)}) collective-permute-start(bf16[128,896]{1,0:T(8,128)(2,1)S(1)} %get-tuple-element.29), channel_id=1, source_target_pairs={{0,16},{8,24},{16,0},{24,8},{1,17},{9,25},{17,1},{25,9},{2,18},{10... | collective-permute-start | bytes 688136 | tf_op jit(solution)/shard_map/ppermute | solution.py:210
  9.7 9.9 %collective-permute-start.2 = (bf16[128,896]{1,0:T(8,128)(2,1)S(1)}, bf16[128,896]{1,0:T(8,128)(2,1)S(1)}, u32[]{:S(2)}, u32[]{:S(2)}) collective-permute-start(bf16[128,896]{1,0:T(8,128)(2,1)S(1)} %get-tuple-element.30), channel_id=1, source_target_pairs={{0,24},{8,0},{16,8},{24,16},{1,25},{9,1},{17,9},{25,17},{2,26},{10... | collective-permute-start | bytes 688136 | tf_op jit(solution)/shard_map/ppermute | solution.py:210
  14.1 5.5 %collective-permute-start.3 = (bf16[128,896]{1,0:T(8,128)(2,1)S(1)}, bf16[128,896]{1,0:T(8,128)(2,1)S(1)}, u32[]{:S(2)}, u32[]{:S(2)}) collective-permute-start(bf16[128,896]{1,0:T(8,128)(2,1)S(1)} %collective-permute-done.r1), channel_id=1, source_target_pairs={{0,1},{1,0},{2,3},{3,2},{4,5},{5,4},{6,7},{7,6},{8,9},{9,8},{10,11... | collective-permute-start | bytes 688136 | tf_op jit(solution)/shard_map/ppermute | solution.py:214
  16.9 2.7 %collective-permute-start.4 = (bf16[128,896]{1,0:T(8,128)(2,1)S(1)}, bf16[128,896]{1,0:T(8,128)(2,1)S(1)}, u32[]{:S(2)}, u32[]{:S(2)}) collective-permute-start(bf16[128,896]{1,0:T(8,128)(2,1)S(1)} %collective-permute-done.1.r2), channel_id=1, source_target_pairs={{0,1},{1,0},{2,3},{3,2},{4,5},{5,4},{6,7},{7,6},{8,9},{9,8},{10,11... | collective-permute-start | bytes 688136 | tf_op jit(solution)/shard_map/ppermute | solution.py:214
  19.6 1.5 collective-permute-start.5
  22.8 28.4 %copy-start = (f32[2816,128]{1,0:T(8,128)S(1)}, f32[2816,128]{1,0:T(8,128)}, u32[]{:S(2)}) copy-start(f32[2816,128]{1,0:T(8,128)} %down) | copy-start | bytes 4325380
  22.8 28.5 %copy-start.8 = (f32[128]{0:T(128)S(1)}, f32[128]{0:T(128)}, u32[]{:S(2)}) copy-start(f32[128]{0:T(128)} %param.23) | copy-start | bytes 1540
  22.8 23.7 %all-to-all-start = ((bf16[8,2,16,768]{3,2,1,0:T(8,128)(2,1)}), bf16[8,2,16,768]{3,2,1,0:T(8,128)(2,1)S(1)}, u32[]{:S(2)}, u32[]{:S(2)}) async-start(bf16[8,2,16,768]{3,2,1,0:T(8,128)(2,1)} %shard_map.146), calls=%async_computation | async-start | bytes 786432 | tf_op jit(solution)/shard_map/all_to_all | solution.py:222
  31.5 24.9 %copy-start.1 = (f32[128,2816]{1,0:T(8,128)S(1)}, f32[128,2816]{1,0:T(8,128)}, u32[]{:S(2)}) copy-start(f32[128,2816]{1,0:T(8,128)} %gate.2) | copy-start | bytes 4325380
  47.8 19.0 %all-to-all-start.1 = ((bf16[8,2,16,384]{3,2,1,0:T(8,128)(2,1)}), bf16[8,2,16,384]{3,2,1,0:T(8,128)(2,1)S(1)}, u32[]{:S(2)}, u32[]{:S(2)}) async-start(bf16[8,2,16,384]{3,2,1,0:T(8,128)(2,1)} %shard_map.147), calls=%async_computation.1 | async-start | bytes 393216 | tf_op jit(solution)/shard_map/all_to_all | solution.py:222
  51.8 11.7 %collective-permute-start.6 = (bf16[768,128]{1,0:T(8,128)(2,1)S(1)}, bf16[768,128]{1,0:T(8,128)(2,1)S(1)}, u32[]{:S(2)}, u32[]{:S(2)}) collective-permute-start(bf16[768,128]{1,0:T(8,128)(2,1)S(1)} %get-tuple-element.35), channel_id=1, source_target_pairs={{0,8},{8,16},{16,24},{24,0},{1,9},{9,17},{17,25},{25,1},{2,10},{10... | collective-permute-start | bytes 589832 | tf_op jit(solution)/shard_map/ppermute | solution.py:210
  53.2 10.4 %collective-permute-start.7 = (bf16[768,128]{1,0:T(8,128)(2,1)S(1)}, bf16[768,128]{1,0:T(8,128)(2,1)S(1)}, u32[]{:S(2)}, u32[]{:S(2)}) collective-permute-start(bf16[768,128]{1,0:T(8,128)(2,1)S(1)} %get-tuple-element.36), channel_id=1, source_target_pairs={{0,16},{8,24},{16,0},{24,8},{1,17},{9,25},{17,1},{25,9},{2,18},{10... | collective-permute-start | bytes 589832 | tf_op jit(solution)/shard_map/ppermute | solution.py:210
  55.1 11.7 %collective-permute-start.8 = (bf16[768,128]{1,0:T(8,128)(2,1)S(1)}, bf16[768,128]{1,0:T(8,128)(2,1)S(1)}, u32[]{:S(2)}, u32[]{:S(2)}) collective-permute-start(bf16[768,128]{1,0:T(8,128)(2,1)S(1)} %get-tuple-element.37), channel_id=1, source_target_pairs={{0,24},{8,0},{16,8},{24,16},{1,25},{9,1},{17,9},{25,17},{2,26},{10... | collective-permute-start | bytes 589832 | tf_op jit(solution)/shard_map/ppermute | solution.py:210
  56.3 1.4 copy-start.2
  57.7 28.4 %copy-start.7 = (bf16[128,128]{1,0:T(8,128)(2,1)S(1)}, bf16[128,128]{1,0:T(8,128)(2,1)}, u32[]{:S(2)}) copy-start(bf16[128,128]{1,0:T(8,128)(2,1)} %tokens.3) | copy-start | bytes 98308
  57.7 28.4 %copy-start.9 = (f32[128]{0:T(128)S(1)}, f32[128]{0:T(128)}, u32[]{:S(2)}) copy-start(f32[128]{0:T(128)} %param.22) | copy-start | bytes 1540
  59.9 32.7 %collective-permute-start.9 = (bf16[128,1536]{1,0:T(8,128)(2,1)}, bf16[128,1536]{1,0:T(8,128)(2,1)S(1)}, u32[]{:S(2)}, u32[]{:S(2)}) collective-permute-start(bf16[128,1536]{1,0:T(8,128)(2,1)} %get-tuple-element.41), channel_id=1, source_target_pairs={{0,8},{8,16},{16,24},{24,0},{1,9},{9,17},{17,25},{25,1},{2,10},{10... | collective-permute-start | bytes 1179656 | tf_op jit(solution)/shard_map/ppermute | solution.py:210
  60.7 32.0 %collective-permute-start.10 = (bf16[128,1536]{1,0:T(8,128)(2,1)}, bf16[128,1536]{1,0:T(8,128)(2,1)S(1)}, u32[]{:S(2)}, u32[]{:S(2)}) collective-permute-start(bf16[128,1536]{1,0:T(8,128)(2,1)} %get-tuple-element.42), channel_id=1, source_target_pairs={{0,16},{8,24},{16,0},{24,8},{1,17},{9,25},{17,1},{25,9},{2,18},{10... | collective-permute-start | bytes 1179656 | tf_op jit(solution)/shard_map/ppermute | solution.py:210
  63.6 29.1 %collective-permute-start.11 = (bf16[128,1536]{1,0:T(8,128)(2,1)}, bf16[128,1536]{1,0:T(8,128)(2,1)S(1)}, u32[]{:S(2)}, u32[]{:S(2)}) collective-permute-start(bf16[128,1536]{1,0:T(8,128)(2,1)} %get-tuple-element.43), channel_id=1, source_target_pairs={{0,24},{8,0},{16,8},{24,16},{1,25},{9,1},{17,9},{25,17},{2,26},{10... | collective-permute-start | bytes 1179656 | tf_op jit(solution)/shard_map/ppermute | solution.py:210
  87.4 12.1 %all-to-all-start.3 = ((f32[16,32,128]{2,1,0:T(8,128)}), f32[16,32,128]{2,1,0:T(8,128)S(1)}, u32[]{:S(2)}, u32[]{:S(2)}) async-start(f32[16,32,128]{2,1,0:T(8,128)} %shard_map.150), calls=%async_computation.3 | async-start | bytes 524288 | tf_op jit(solution)/shard_map/all_to_all | solution.py:222
  101.2 25.3 %copy-start.3 = (f32[2816,128]{1,0:T(8,128)S(1)}, f32[2816,128]{1,0:T(8,128)}, u32[]{:S(2)}) copy-start(f32[2816,128]{1,0:T(8,128)} %down.1) | copy-start | bytes 4325380
  101.2 20.5 %all-to-all-start.4 = ((bf16[8,2,16,768]{3,2,1,0:T(8,128)(2,1)}), bf16[8,2,16,768]{3,2,1,0:T(8,128)(2,1)S(1)}, u32[]{:S(2)}, u32[]{:S(2)}) async-start(bf16[8,2,16,768]{3,2,1,0:T(8,128)(2,1)} %shard_map.152), calls=%async_computation.4 | async-start | bytes 786432 | tf_op jit(solution)/shard_map/all_to_all | solution.py:222
  123.0 14.6 %all-to-all-start.5 = ((bf16[8,2,16,384]{3,2,1,0:T(8,128)(2,1)}), bf16[8,2,16,384]{3,2,1,0:T(8,128)(2,1)S(1)}, u32[]{:S(2)}, u32[]{:S(2)}) async-start(bf16[8,2,16,384]{3,2,1,0:T(8,128)(2,1)} %shard_map.153), calls=%async_computation.5 | async-start | bytes 393216 | tf_op jit(solution)/shard_map/all_to_all | solution.py:222
  127.1 25.5 %copy-start.10 = (f32[128]{0:T(128)S(1)}, f32[128]{0:T(128)}, u32[]{:S(2)}) copy-start(f32[128]{0:T(128)} %param.29) | copy-start | bytes 1540
  127.1 6.5 %collective-permute-start.12 = (bf16[768,128]{1,0:T(8,128)(2,1)S(1)}, bf16[768,128]{1,0:T(8,128)(2,1)S(1)}, u32[]{:S(2)}, u32[]{:S(2)}) collective-permute-start(bf16[768,128]{1,0:T(8,128)(2,1)S(1)} %get-tuple-element.46), channel_id=1, source_target_pairs={{0,8},{8,16},{16,24},{24,0},{1,9},{9,17},{17,25},{25,1},{2,10},{10... | collective-permute-start | bytes 589832 | tf_op jit(solution)/shard_map/ppermute | solution.py:210
  128.2 7.4 %collective-permute-start.13 = (bf16[768,128]{1,0:T(8,128)(2,1)S(1)}, bf16[768,128]{1,0:T(8,128)(2,1)S(1)}, u32[]{:S(2)}, u32[]{:S(2)}) collective-permute-start(bf16[768,128]{1,0:T(8,128)(2,1)S(1)} %get-tuple-element.47), channel_id=1, source_target_pairs={{0,16},{8,24},{16,0},{24,8},{1,17},{9,25},{17,1},{25,9},{2,18},{10... | collective-permute-start | bytes 589832 | tf_op jit(solution)/shard_map/ppermute | solution.py:210
  131.0 6.6 %collective-permute-start.14 = (bf16[768,128]{1,0:T(8,128)(2,1)S(1)}, bf16[768,128]{1,0:T(8,128)(2,1)S(1)}, u32[]{:S(2)}, u32[]{:S(2)}) collective-permute-start(bf16[768,128]{1,0:T(8,128)(2,1)S(1)} %get-tuple-element.48), channel_id=1, source_target_pairs={{0,24},{8,0},{16,8},{24,16},{1,25},{9,1},{17,9},{25,17},{2,26},{10... | collective-permute-start | bytes 589832 | tf_op jit(solution)/shard_map/ppermute | solution.py:210

commit v4 on v3

--- a/solution.py
+++ b/solution.py
@@ -17,36 +17,66 @@
 WIDE = 2 * PAD
 CHUNK = 2 * HALF
 WIDTH = 4096
-LIMIT = 16 * 2**20
+LIMIT = 8 * 2**20
 
 SMEM = pl.BlockSpec(memory_space=pltpu.SMEM)
 VMEM = pl.BlockSpec(memory_space=pltpu.VMEM)
+HBM = pl.BlockSpec(memory_space=pltpu.HBM)
+BLOCKS = 4
 
 
 def shape(*dims, dtype=BF):
     return jax.ShapeDtypeStruct(dims, dtype)
 
 
-def call(body, outs, n_in, scratch=()):
+def call(body, outs, n_in, scratch=(), far=0):
     many = isinstance(outs, (list, tuple))
-    return pl.pallas_call(
+    kernel = pl.pallas_call(
         body,
         out_shape=outs,
-        in_specs=[SMEM] + [VMEM] * n_in,
+        in_specs=[SMEM] + [HBM] * far + [VMEM] * (n_in - far),
         out_specs=[VMEM] * len(outs) if many else VMEM,
         scratch_shapes=list(scratch),
         compiler_params=pltpu.CompilerParams(vmem_limit_bytes=LIMIT),
     )
 
+    def run(*args):
+        there = [pltpu.with_memory_space_constraint(v, pltpu.HBM) for v in args[1 : 1 + far]]
+        return kernel(args[0], *there, *args[1 + far :])
+
+    return run
+
 
 def high_low(v):
     high = v.astype(BF).astype(F32)
     return high, (v - high).astype(BF).astype(F32)
 
 
-def padded_chunk(ref, i):
-    part = ref[:, i * HALF : (i + 1) * HALF]
-    return jnp.concatenate([part, jnp.zeros((N, PAD - HALF), F32)], axis=1)
+def loads(pairs, sems):
+    copies = []
+    for block in range(BLOCKS):
+        for j, (source, target) in enumerate(pairs):
+            rows = source.shape[0] // BLOCKS
+            part = pl.ds(block * rows, rows)
+            copies.append(
+                pltpu.make_async_copy(source.at[part], target.at[part], sems.at[block, j])
+            )
+    for copy in copies:
+        copy.start()
+    return [copies[i : i + len(pairs)] for i in range(0, len(copies), len(pairs))]
+
+
+def cut_chunks(gate, up, gate_here, up_here, sems, chunks):
+    rows = N // BLOCKS
+    for block, copies in enumerate(loads(((gate, gate_here), (up, up_here)), sems)):
+        for copy in copies:
+            copy.wait()
+        part = slice(block * rows, (block + 1) * rows)
+        for here, first in ((gate_here, 0), (up_here, PAD)):
+            for i in range(2 * NX):
+                cut = here[part, i * HALF : (i + 1) * HALF]
+                cut = jnp.concatenate([cut, jnp.zeros((rows, PAD - HALF), F32)], axis=1)
+                chunks[i, part, first : first + PAD] = cut.astype(BF)
 
 
 def with_columns(tile, first, second):
@@ -55,12 +85,15 @@
     return jnp.where(lane == at, first, jnp.where(lane == at + 1, second, tile))
 
 
-def pack_first_body(at, gate, up, tokens, gain, p0, p1, p2, p3, other, chunks):
+def pack_first_body(
+    at, gate, up, tokens, gain, p0, p1, p2, p3, other, chunks, gate_here, up_here, sems, here, sem
+):
     x, c = at[0], at[2]
-    for i in range(2 * NX):
-        chunks[i, :, :PAD] = padded_chunk(gate, i).astype(BF)
-        chunks[i, :, PAD:] = padded_chunk(up, i).astype(BF)
-    stream = tokens[...].astype(F32)
+    copy = pltpu.make_async_copy(tokens, here, sem)
+    copy.start()
+    cut_chunks(gate, up, gate_here, up_here, sems, chunks)
+    copy.wait()
+    stream = here[...].astype(F32)
     scaled = (stream * gain[...]).astype(BF)
     high, low = high_low(jnp.sum(stream * stream, axis=1, keepdims=True))
     for k, out in enumerate((p0, p1, p2, p3)):
@@ -72,19 +105,18 @@
     other[...] = chunks[2 * x + 1 - c]
 
 
-def pack_second_body(at, gate, up, p0, p1, p2, p3, chunks):
-    x = at[0]
-    for i in range(2 * NX):
-        chunks[i, :, :PAD] = padded_chunk(gate, i).astype(BF)
-        chunks[i, :, PAD:] = padded_chunk(up, i).astype(BF)
+def pack_second_body(at, gate, up, p0, p1, p2, p3, chunks, gate_here, up_here, sems):
+    x = at[0]
+    cut_chunks(gate, up, gate_here, up_here, sems, chunks)
     for k, out in enumerate((p0, p1, p2, p3)):
         index = 2 * lax.rem(x + k, NX)
         out[:, :WIDE] = chunks[index]
         out[:, WIDE:] = chunks[index + 1]
 
 
-def pack_down_body(at, down, gain, p0, p1, p2, p3):
-    x = at[0]
+def pack_down_body(at, far, gain, p0, p1, p2, p3, down, sems):
+    x = at[0]
+    waits = loads(((far, down),), sems)
     value = gain[...]
     high = value.astype(BF).astype(F32)
     rest = value - high
@@ -93,6 +125,8 @@
     row = lax.broadcasted_iota(jnp.int32, (PAD - HALF, N), 0)
     tail = jnp.where(row == 0, high, jnp.where(row == 1, middle, jnp.where(row == 2, low, 0.0)))
     tail = tail.astype(BF)
+    for copies in waits:
+        copies[0].wait()
     for k, out in enumerate((p0, p1, p2, p3)):
         base = lax.rem(x + k, NX) * CHUNK
         for h in range(2):
@@ -249,38 +283,38 @@
 ):
     x = lax.axis_index("x")
     at = jnp.stack([x, lax.axis_index("y"), lax.axis_index("c")]).astype(jnp.int32)
-    chunks = pltpu.VMEM((2 * NX, N, WIDE), BF)
+    columns = 2 * NX * HALF
+    wide_here = pltpu.VMEM((N, columns), F32)
+    sems = pltpu.SemaphoreType.DMA((BLOCKS, 2))
+    cutting = [pltpu.VMEM((2 * NX, N, WIDE), BF), wide_here, wide_here, sems]
+    entering = [*cutting, pltpu.VMEM((N, N), BF), pltpu.SemaphoreType.DMA(())]
+    lowering = [pltpu.VMEM((columns, N), F32), pltpu.SemaphoreType.DMA((BLOCKS, 1))]
     payload = shape(NZ, 2, N // NZ, WIDE)
     spread = shape(NZ, 2, N // NZ, PAD)
 
     *packed, other = call(
-        pack_first_body, [shape(N, WIDE + N)] * NX + [shape(N, WIDE)], 4, [chunks]
+        pack_first_body, [shape(N, WIDE + N)] * NX + [shape(N, WIDE)], 4, entering, 3
     )(at, first_gate, first_up, tokens, first_gain[None])
     mine = around(packed)
     theirs = [other] + [other_core(v) for v in mine[1:]]
     sums = call(enter_first_body, payload, 8)(at, *mine, *theirs)
-    sums, first_down, second_gate, second_up, second_down = lax.optimization_barrier(
-        (sums, first_down, second_gate, second_up, second_down)
-    )
     got = swap(sums, "z")
     downs = around(
-        call(pack_down_body, [shape(2 * PAD, N)] * NX, 2)(
+        call(pack_down_body, [shape(2 * PAD, N)] * NX, 2, lowering, 1)(
             at, first_down, second_gain[None]
         ),
     )
     ups = around(
-        call(pack_second_body, [shape(N, 2 * WIDE)] * NX, 2, [chunks])(
+        call(pack_second_body, [shape(N, 2 * WIDE)] * NX, 2, cutting, 2)(
             at, second_gate, second_up
         ),
     )
     last_downs = around(
-        call(pack_down_body, [shape(2 * PAD, N)] * NX, 2)(
+        call(pack_down_body, [shape(2 * PAD, N)] * NX, 2, lowering, 1)(
             at, second_down, second_gain[None]
         ),
     )
-    hidden = call(hidden_body, spread, 2)(
-        at, got, scale_rows(first_gate_scale, first_up_scale, x)
-    )
+    hidden = call(hidden_body, spread, 2)(at, got, scale_rows(first_gate_scale, first_up_scale, x))
     hidden = swap(hidden, "z")
     part = call(leave_first_body, shape(NX * NY, N // NY, N), 5)(at, hidden, *downs)
     got = swap(part, XY)
@@ -297,9 +331,7 @@
     hidden = swap(hidden, "z")
     part = call(leave_second_body, shape(NX * NY, N, N), 5)(at, hidden, *last_downs)
     got = swap(part, XY)
-    return call(final_body, shape(N, N, dtype=F32), 3)(
-        at, got, stream, second_down_scale[None]
-    )
+    return call(final_body, shape(N, N, dtype=F32), 3)(at, got, stream, second_down_scale[None])
 
 
 def solution(mesh):

time: 156 us -> 157 us (level)
  Pallas kernels: 15 us -> 20.3 us
  local copies, waits for them, and re-layouts: 9.04 us -> 4.07 us
    pallas_call x12, Pallas kernels: 15 us -> 20.3 us  [run(): return kernel(args[0], *there, *args[1 + far:])]
    unnamed x24 -> x10, local copies, waits for them, and re-layouts: 5.53 us -> 0.67 us
  transfers between devices with their start and end apart: 20 -> 20, of which waited for: 11 -> 11; matrix products, arithmetic and copies ran while one was open for 2% -> 2% of each run, Pallas kernels for 4% -> 6%
where the time goes in v4:
time: 157 us; the launch traced here: 155 us
  waiting for transfers between devices  52.6 us (34%)
  starting transfers between devices  45.1 us (29%)
  blocking collectives  32.4 us (21%)
  Pallas kernels  20.3 us (13%)
  local copies, waits for them, and re-layouts  4.07 us (3%)
    all_to_all x2, blocking collectives, swap(): return lax.all_to_all(v, axis, 0, 0, tiled=True)  32.4 us
    all_to_all x5, waiting for transfers between devices, swap(): return lax.all_to_all(v, axis, 0, 0, tiled=True)  31.7 us
    all_to_all x5, starting transfers between devices, swap(): return lax.all_to_all(v, axis, 0, 0, tiled=True)  28 us
    pallas_call x12, Pallas kernels, run(): return kernel(args[0], *there, *args[1 + far:])  20.3 us
    ppermute x12, waiting for transfers between devices, shift(): return lax.ppermute(v, 'x', [(i, (i + k) % NX) for i in range(NX)])  19.3 us
    ppermute x12, starting transfers between devices, shift(): return lax.ppermute(v, 'x', [(i, (i + k) % NX) for i in range(NX)])  17.1 us
  transfers between devices with their start and end apart: 20, of which 11 were waited for; matrix products, arithmetic and copies ran while one was open for 2% of the time, Pallas kernels for 6%

profile of v4, /device:TPU:2, one launch (start us, length us, event | category | flops | bytes accessed | tf_op | source)
XLA Modules:
  0.0 154.6 jit_solution(5721518230267974089)
XLA Ops:
  0.1 0.7 copy-done.4
  0.7 2.7 %shard_map.145 = (bf16[128,896]{1,0:T(8,128)(2,1)S(1)}, bf16[128,896]{1,0:T(8,128)(2,1)S(1)}, bf16[128,896]{1,0:T(8,128)(2,1)S(1)}, bf16[128,896]{1,0:T(8,128)(2,1)S(1)}, bf16[128,768]{1,0:T(8,128)(2,1)S(1)}) custom-call(s32[3]{0:T(128)S(1)} %pad_add_fusion.at, f32[128,2816]{1,0:T(8,128)} %gate.2, f32[128,2816]{1,0:T(8,128)} %up.2, bf16[128,128]{1,0:T(8,128)(2,1)} %tokens.3, ...), custom_call_target="tpu_custom_call" | custom-call | tf_op jit(solution)/shard_map/pallas_call | solution.py:45
  3.4 1.6 %collective-permute-start = (bf16[128,896]{1,0:T(8,128)(2,1)S(1)}, bf16[128,896]{1,0:T(8,128)(2,1)S(1)}, u32[]{:S(2)}, u32[]{:S(2)}) collective-permute-start(bf16[128,896]{1,0:T(8,128)(2,1)S(1)} %get-tuple-element.23), channel_id=1, source_target_pairs={{0,8},{8,16},{16,24},{24,0},{1,9},{9,17},{17,25},{25,1},{2,10},{10... | collective-permute-start | bytes 688136 | tf_op jit(solution)/shard_map/ppermute | solution.py:244
  5.0 2.8 %collective-permute-start.1 = (bf16[128,896]{1,0:T(8,128)(2,1)S(1)}, bf16[128,896]{1,0:T(8,128)(2,1)S(1)}, u32[]{:S(2)}, u32[]{:S(2)}) collective-permute-start(bf16[128,896]{1,0:T(8,128)(2,1)S(1)} %get-tuple-element.24), channel_id=1, source_target_pairs={{0,16},{8,24},{16,0},{24,8},{1,17},{9,25},{17,1},{25,9},{2,18},{10... | collective-permute-start | bytes 688136 | tf_op jit(solution)/shard_map/ppermute | solution.py:244
  7.8 0.4 collective-permute-start.2
  8.2 3.9 %collective-permute-done.r1 = bf16[128,896]{1,0:T(8,128)(2,1)S(1)} collective-permute-done((bf16[128,896]{1,0:T(8,128)(2,1)S(1)}, bf16[128,896]{1,0:T(8,128)(2,1)S(1)}, u32[]{:S(2)}, u32[]{:S(2)}) %collective-permute-start) | collective-permute-done | bytes 229408 | tf_op jit(solution)/shard_map/ppermute | solution.py:244
  12.2 2.8 %collective-permute-done.1.r2 = bf16[128,896]{1,0:T(8,128)(2,1)S(1)} collective-permute-done((bf16[128,896]{1,0:T(8,128)(2,1)S(1)}, bf16[128,896]{1,0:T(8,128)(2,1)S(1)}, u32[]{:S(2)}, u32[]{:S(2)}) %collective-permute-start.1) | collective-permute-done | bytes 229408 | tf_op jit(solution)/shard_map/ppermute | solution.py:244
  15.0 2.7 %collective-permute-done.2.r3 = bf16[128,896]{1,0:T(8,128)(2,1)S(1)} collective-permute-done((bf16[128,896]{1,0:T(8,128)(2,1)S(1)}, bf16[128,896]{1,0:T(8,128)(2,1)S(1)}, u32[]{:S(2)}, u32[]{:S(2)}) %collective-permute-start.2) | collective-permute-done | bytes 229408 | tf_op jit(solution)/shard_map/ppermute | solution.py:244
  17.7 1.5 collective-permute-done.5.s3
  19.2 1.7 %shard_map.146 = bf16[8,2,16,768]{3,2,1,0:T(8,128)(2,1)} custom-call(s32[3]{0:T(128)S(1)} %pad_add_fusion.at, bf16[128,896]{1,0:T(8,128)(2,1)S(1)} %get-tuple-element.22.r0, bf16[128,896]{1,0:T(8,128)(2,1)S(1)} %collective-permute-done.r1, bf16[128,896]{1,0:T(8,128)(2,1)S(1)} %collective-permute-done.1.r2, bf16[128,896]{1,0:T(8,128)(2,1)S(1)} %collective-permute-done.2.r3, ...), custom_call_target="tpu_custom_call" | custom-call | tf_op jit(solution)/shard_map/pallas_call | solution.py:45
  20.9 8.7 %all-to-all-start = ((bf16[8,2,16,768]{3,2,1,0:T(8,128)(2,1)}), bf16[8,2,16,768]{3,2,1,0:T(8,128)(2,1)S(1)}, u32[]{:S(2)}, u32[]{:S(2)}) async-start(bf16[8,2,16,768]{3,2,1,0:T(8,128)(2,1)} %shard_map.146), calls=%async_computation | async-start | bytes 786432 | tf_op jit(solution)/shard_map/all_to_all | solution.py:256
  29.6 0.8 dynamic_slice.12
  30.3 0.1 reshape.12
  30.4 0.8 dynamic_slice.13
  31.3 13.3 %all-to-all-done.got = bf16[8,2,16,768]{3,2,1,0:T(8,128)(2,1)S(1)} async-done(((bf16[8,2,16,768]{3,2,1,0:T(8,128)(2,1)}), bf16[8,2,16,768]{3,2,1,0:T(8,128)(2,1)S(1)}, u32[]{:S(2)}, u32[]{:S(2)}) %all-to-all-start) | async-done | bytes 393248 | tf_op jit(solution)/shard_map/all_to_all | solution.py:256
  44.5 1.4 shard_map.147
  45.9 3.4 %all-to-all-start.1 = ((bf16[8,2,16,384]{3,2,1,0:T(8,128)(2,1)}), bf16[8,2,16,384]{3,2,1,0:T(8,128)(2,1)S(1)}, u32[]{:S(2)}, u32[]{:S(2)}) async-start(bf16[8,2,16,384]{3,2,1,0:T(8,128)(2,1)} %shard_map.147), calls=%async_computation.1 | async-start | bytes 393216 | tf_op jit(solution)/shard_map/all_to_all | solution.py:256
  49.3 2.0 %shard_map.148 = (bf16[768,128]{1,0:T(8,128)(2,1)S(1)}, bf16[768,128]{1,0:T(8,128)(2,1)S(1)}, bf16[768,128]{1,0:T(8,128)(2,1)S(1)}, bf16[768,128]{1,0:T(8,128)(2,1)S(1)}) custom-call(s32[3]{0:T(128)S(1)} %pad_add_fusion.at, f32[2816,128]{1,0:T(8,128)} %far.2, f32[1,128]{1,0:T(1,128)S(1)} %bitcast.7), custom_call_target="tpu_custom_call" | custom-call | tf_op jit(solution)/shard_map/pallas_call | solution.py:45
  51.3 1.4 collective-permute-start.6
  52.6 1.9 %collective-permute-start.7 = (bf16[768,128]{1,0:T(8,128)(2,1)S(1)}, bf16[768,128]{1,0:T(8,128)(2,1)S(1)}, u32[]{:S(2)}, u32[]{:S(2)}) collective-permute-start(bf16[768,128]{1,0:T(8,128)(2,1)S(1)} %get-tuple-element.29), channel_id=1, source_target_pairs={{0,16},{8,24},{16,0},{24,8},{1,17},{9,25},{17,1},{25,9},{2,18},{10... | collective-permute-start | bytes 589832 | tf_op jit(solution)/shard_map/ppermute | solution.py:244
  54.5 1.3 collective-permute-start.8
  55.8 3.3 %shard_map.151 = (bf16[128,1536]{1,0:T(8,128)(2,1)S(1)}, bf16[128,1536]{1,0:T(8,128)(2,1)S(1)}, bf16[128,1536]{1,0:T(8,128)(2,1)}, bf16[128,1536]{1,0:T(8,128)(2,1)S(1)}) custom-call(s32[3]{0:T(128)S(1)} %pad_add_fusion.at, f32[128,2816]{1,0:T(8,128)} %gate.3, f32[128,2816]{1,0:T(8,128)} %up.3), custom_call_target="tpu_custom_call" | custom-call | tf_op jit(solution)/shard_map/pallas_call | solution.py:45
  59.1 0.6 collective-permute-start.10
  59.7 2.3 %collective-permute-start.11 = (bf16[128,1536]{1,0:T(8,128)(2,1)S(1)}, bf16[128,1536]{1,0:T(8,128)(2,1)S(1)}, u32[]{:S(2)}, u32[]{:S(2)}) collective-permute-start(bf16[128,1536]{1,0:T(8,128)(2,1)S(1)} %get-tuple-element.34), channel_id=1, source_target_pairs={{0,24},{8,0},{16,8},{24,16},{1,25},{9,1},{17,9},{25,17},{2,26},{10... | collective-permute-start | bytes 1179656 | tf_op jit(solution)/shard_map/ppermute | solution.py:244
  62.0 0.2 collective-permute-start.9
  62.2 4.0 %collective-permute-done.8.d3 = bf16[768,128]{1,0:T(8,128)(2,1)S(1)} collective-permute-done((bf16[768,128]{1,0:T(8,128)(2,1)S(1)}, bf16[768,128]{1,0:T(8,128)(2,1)S(1)}, u32[]{:S(2)}, u32[]{:S(2)}) %collective-permute-start.8) | collective-permute-done | bytes 196640 | tf_op jit(solution)/shard_map/ppermute | solution.py:244
  66.2 0.9 shard_map.149
  67.1 18.3 %all_to_all.35.got = bf16[16,32,128]{2,1,0:T(8,128)(2,1)S(1)} all-to-all(bf16[16,32,128]{2,1,0:T(8,128)(2,1)S(1)} %shard_map.149), channel_id=1, replica_groups=mesh['z'=8,'x'=4,'y'=4,'c'=2] {'x','y'}, dimensions={0} | all-to-all | bytes 262144 | tf_op jit(solution)/shard_map/all_to_all | solution.py:256
  85.5 1.3 shard_map.150
  86.8 5.3 %all-to-all-start.3 = ((f32[16,32,128]{2,1,0:T(8,128)}), f32[16,32,128]{2,1,0:T(8,128)S(1)}, u32[]{:S(2)}, u32[]{:S(2)}) async-start(f32[16,32,128]{2,1,0:T(8,128)} %shard_map.150), calls=%async_computation.3 | async-start | bytes 524288 | tf_op jit(solution)/shard_map/all_to_all | solution.py:256
  92.1 6.8 %all-to-all-done.3.stream = f32[16,32,128]{2,1,0:T(8,128)S(1)} async-done(((f32[16,32,128]{2,1,0:T(8,128)}), f32[16,32,128]{2,1,0:T(8,128)S(1)}, u32[]{:S(2)}, u32[]{:S(2)}) %all-to-all-start.3) | async-done | bytes 262176 | tf_op jit(solution)/shard_map/all_to_all | solution.py:256
  98.9 1.7 %shard_map.152 = bf16[8,2,16,768]{3,2,1,0:T(8,128)(2,1)} custom-call(s32[3]{0:T(128)S(1)} %pad_add_fusion.at, f32[16,32,128]{2,1,0:T(8,128)S(1)} %all-to-all-done.3.stream, bf16[768,128]{1,0:T(8,128)(2,1)S(1)} %get-tuple-element.27.d0, bf16[768,128]{1,0:T(8,128)(2,1)S(1)} %collective-permute-done.6.d1, bf16[768,128]{1,0:T(8,128)(2,1)S(1)} %collective-permute-done.7.d2, ...), custom_call_target="tpu_custom_call" | custom-call | tf_op jit(solution)/shard_map/pallas_call | solution.py:45
  100.6 7.0 %all-to-all-start.4 = ((bf16[8,2,16,768]{3,2,1,0:T(8,128)(2,1)}), bf16[8,2,16,768]{3,2,1,0:T(8,128)(2,1)S(1)}, u32[]{:S(2)}, u32[]{:S(2)}) async-start(bf16[8,2,16,768]{3,2,1,0:T(8,128)(2,1)} %shard_map.152), calls=%async_computation.4 | async-start | bytes 786432 | tf_op jit(solution)/shard_map/all_to_all | solution.py:256
  107.6 0.8 dynamic_slice.14
  108.4 0.8 dynamic_slice.15
  109.3 11.7 %all-to-all-done.4.got = bf16[8,2,16,768]{3,2,1,0:T(8,128)(2,1)S(1)} async-done(((bf16[8,2,16,768]{3,2,1,0:T(8,128)(2,1)}), bf16[8,2,16,768]{3,2,1,0:T(8,128)(2,1)S(1)}, u32[]{:S(2)}, u32[]{:S(2)}) %all-to-all-start.4) | async-done | bytes 393248 | tf_op jit(solution)/shard_map/all_to_all | solution.py:256
  121.0 1.3 shard_map.153
  122.3 3.6 %all-to-all-start.5 = ((bf16[8,2,16,384]{3,2,1,0:T(8,128)(2,1)}), bf16[8,2,16,384]{3,2,1,0:T(8,128)(2,1)S(1)}, u32[]{:S(2)}, u32[]{:S(2)}) async-start(bf16[8,2,16,384]{3,2,1,0:T(8,128)(2,1)} %shard_map.153), calls=%async_computation.5 | async-start | bytes 393216 | tf_op jit(solution)/shard_map/all_to_all | solution.py:256
  125.9 2.0 %shard_map.154 = (bf16[768,128]{1,0:T(8,128)(2,1)S(1)}, bf16[768,128]{1,0:T(8,128)(2,1)S(1)}, bf16[768,128]{1,0:T(8,128)(2,1)S(1)}, bf16[768,128]{1,0:T(8,128)(2,1)S(1)}) custom-call(s32[3]{0:T(128)S(1)} %pad_add_fusion.at, f32[2816,128]{1,0:T(8,128)} %far.3, f32[1,128]{1,0:T(1,128)S(1)} %bitcast.8), custom_call_target="tpu_custom_call" | custom-call | tf_op jit(solution)/shard_map/pallas_call | solution.py:45
  127.9 1.2 collective-permute-start.12
  129.0 2.8 %collective-permute-start.13 = (bf16[768,128]{1,0:T(8,128)(2,1)S(1)}, bf16[768,128]{1,0:T(8,128)(2,1)S(1)}, u32[]{:S(2)}, u32[]{:S(2)}) collective-permute-start(bf16[768,128]{1,0:T(8,128)(2,1)S(1)} %get-tuple-element.37), channel_id=1, source_target_pairs={{0,16},{8,24},{16,0},{24,8},{1,17},{9,25},{17,1},{25,9},{2,18},{10... | collective-permute-start | bytes 589832 | tf_op jit(solution)/shard_map/ppermute | solution.py:244
  131.8 0.8 collective-permute-start.14
  132.5 1.8 %collective-permute-done.12.d1 = bf16[768,128]{1,0:T(8,128)(2,1)S(1)} collective-permute-done((bf16[768,128]{1,0:T(8,128)(2,1)S(1)}, bf16[768,128]{1,0:T(8,128)(2,1)S(1)}, u32[]{:S(2)}, u32[]{:S(2)}) %collective-permute-start.12) | collective-permute-done | bytes 196640 | tf_op jit(solution)/shard_map/ppermute | solution.py:244
  134.3 2.1 %collective-permute-done.13.d2 = bf16[768,128]{1,0:T(8,128)(2,1)S(1)} collective-permute-done((bf16[768,128]{1,0:T(8,128)(2,1)S(1)}, bf16[768,128]{1,0:T(8,128)(2,1)S(1)}, u32[]{:S(2)}, u32[]{:S(2)}) %collective-permute-start.13) | collective-permute-done | bytes 196640 | tf_op jit(solution)/shard_map/ppermute | solution.py:244
  136.4 2.0 %collective-permute-done.14.d3 = bf16[768,128]{1,0:T(8,128)(2,1)S(1)} collective-permute-done((bf16[768,128]{1,0:T(8,128)(2,1)S(1)}, bf16[768,128]{1,0:T(8,128)(2,1)S(1)}, u32[]{:S(2)}, u32[]{:S(2)}) %collective-permute-start.14) | collective-permute-done | bytes 196640 | tf_op jit(solution)/shard_map/ppermute | solution.py:244
  138.4 0.9 shard_map.155
  139.3 14.1 %all_to_all.36.got = bf16[16,128,128]{2,1,0:T(8,128)(2,1)S(1)} all-to-all(bf16[16,128,128]{2,1,0:T(8,128)(2,1)S(1)} %shard_map.155), channel_id=1, replica_groups=mesh['z'=8,'x'=4,'y'=4,'c'=2] {'x','y'}, dimensions={0} | all-to-all | bytes 1048576 | tf_op jit(solution)/shard_map/all_to_all | solution.py:256
  153.4 1.3 shard_map.156
  (27 shorter events, 0.4 us)
Async XLA Ops:
  0.1 0.7 copy-start.4
  3.4 8.8 %collective-permute-start = (bf16[128,896]{1,0:T(8,128)(2,1)S(1)}, bf16[128,896]{1,0:T(8,128)(2,1)S(1)}, u32[]{:S(2)}, u32[]{:S(2)}) collective-permute-start(bf16[128,896]{1,0:T(8,128)(2,1)S(1)} %get-tuple-element.23), channel_id=1, source_target_pairs={{0,8},{8,16},{16,24},{24,0},{1,9},{9,17},{17,25},{25,1},{2,10},{10... | collective-permute-start | bytes 688136 | tf_op jit(solution)/shard_map/ppermute | solution.py:244
  5.0 10.0 %collective-permute-start.1 = (bf16[128,896]{1,0:T(8,128)(2,1)S(1)}, bf16[128,896]{1,0:T(8,128)(2,1)S(1)}, u32[]{:S(2)}, u32[]{:S(2)}) collective-permute-start(bf16[128,896]{1,0:T(8,128)(2,1)S(1)} %get-tuple-element.24), channel_id=1, source_target_pairs={{0,16},{8,24},{16,0},{24,8},{1,17},{9,25},{17,1},{25,9},{2,18},{10... | collective-permute-start | bytes 688136 | tf_op jit(solution)/shard_map/ppermute | solution.py:244
  7.8 9.9 %collective-permute-start.2 = (bf16[128,896]{1,0:T(8,128)(2,1)S(1)}, bf16[128,896]{1,0:T(8,128)(2,1)S(1)}, u32[]{:S(2)}, u32[]{:S(2)}) collective-permute-start(bf16[128,896]{1,0:T(8,128)(2,1)S(1)} %get-tuple-element.25), channel_id=1, source_target_pairs={{0,24},{8,0},{16,8},{24,16},{1,25},{9,1},{17,9},{25,17},{2,26},{10... | collective-permute-start | bytes 688136 | tf_op jit(solution)/shard_map/ppermute | solution.py:244
  12.2 5.5 %collective-permute-start.3 = (bf16[128,896]{1,0:T(8,128)(2,1)S(1)}, bf16[128,896]{1,0:T(8,128)(2,1)S(1)}, u32[]{:S(2)}, u32[]{:S(2)}) collective-permute-start(bf16[128,896]{1,0:T(8,128)(2,1)S(1)} %collective-permute-done.r1), channel_id=1, source_target_pairs={{0,1},{1,0},{2,3},{3,2},{4,5},{5,4},{6,7},{7,6},{8,9},{9,8},{10,11... | collective-permute-start | bytes 688136 | tf_op jit(solution)/shard_map/ppermute | solution.py:248
  15.0 2.7 %collective-permute-start.4 = (bf16[128,896]{1,0:T(8,128)(2,1)S(1)}, bf16[128,896]{1,0:T(8,128)(2,1)S(1)}, u32[]{:S(2)}, u32[]{:S(2)}) collective-permute-start(bf16[128,896]{1,0:T(8,128)(2,1)S(1)} %collective-permute-done.1.r2), channel_id=1, source_target_pairs={{0,1},{1,0},{2,3},{3,2},{4,5},{5,4},{6,7},{7,6},{8,9},{9,8},{10,11... | collective-permute-start | bytes 688136 | tf_op jit(solution)/shard_map/ppermute | solution.py:248
  17.7 1.5 collective-permute-start.5
  20.9 28.4 %copy-start.1 = (f32[128]{0:T(128)S(1)}, f32[128]{0:T(128)}, u32[]{:S(2)}) copy-start(f32[128]{0:T(128)} %param.23) | copy-start | bytes 1540
  20.9 23.7 %all-to-all-start = ((bf16[8,2,16,768]{3,2,1,0:T(8,128)(2,1)}), bf16[8,2,16,768]{3,2,1,0:T(8,128)(2,1)S(1)}, u32[]{:S(2)}, u32[]{:S(2)}) async-start(bf16[8,2,16,768]{3,2,1,0:T(8,128)(2,1)} %shard_map.146), calls=%async_computation | async-start | bytes 786432 | tf_op jit(solution)/shard_map/all_to_all | solution.py:256
  45.9 20.3 %all-to-all-start.1 = ((bf16[8,2,16,384]{3,2,1,0:T(8,128)(2,1)}), bf16[8,2,16,384]{3,2,1,0:T(8,128)(2,1)S(1)}, u32[]{:S(2)}, u32[]{:S(2)}) async-start(bf16[8,2,16,384]{3,2,1,0:T(8,128)(2,1)} %shard_map.147), calls=%async_computation.1 | async-start | bytes 393216 | tf_op jit(solution)/shard_map/all_to_all | solution.py:256
  51.3 10.7 %collective-permute-start.6 = (bf16[768,128]{1,0:T(8,128)(2,1)S(1)}, bf16[768,128]{1,0:T(8,128)(2,1)S(1)}, u32[]{:S(2)}, u32[]{:S(2)}) collective-permute-start(bf16[768,128]{1,0:T(8,128)(2,1)S(1)} %get-tuple-element.28), channel_id=1, source_target_pairs={{0,8},{8,16},{16,24},{24,0},{1,9},{9,17},{17,25},{25,1},{2,10},{10... | collective-permute-start | bytes 589832 | tf_op jit(solution)/shard_map/ppermute | solution.py:244
  52.6 9.6 %collective-permute-start.7 = (bf16[768,128]{1,0:T(8,128)(2,1)S(1)}, bf16[768,128]{1,0:T(8,128)(2,1)S(1)}, u32[]{:S(2)}, u32[]{:S(2)}) collective-permute-start(bf16[768,128]{1,0:T(8,128)(2,1)S(1)} %get-tuple-element.29), channel_id=1, source_target_pairs={{0,16},{8,24},{16,0},{24,8},{1,17},{9,25},{17,1},{25,9},{2,18},{10... | collective-permute-start | bytes 589832 | tf_op jit(solution)/shard_map/ppermute | solution.py:244
  54.5 31.0 %copy-start = (bf16[128,128]{1,0:T(8,128)(2,1)S(1)}, bf16[128,128]{1,0:T(8,128)(2,1)}, u32[]{:S(2)}) copy-start(bf16[128,128]{1,0:T(8,128)(2,1)} %tokens.3) | copy-start | bytes 98308
  54.5 31.0 %copy-start.2 = (f32[128]{0:T(128)S(1)}, f32[128]{0:T(128)}, u32[]{:S(2)}) copy-start(f32[128]{0:T(128)} %param.22) | copy-start | bytes 1540
  54.5 11.7 %collective-permute-start.8 = (bf16[768,128]{1,0:T(8,128)(2,1)S(1)}, bf16[768,128]{1,0:T(8,128)(2,1)S(1)}, u32[]{:S(2)}, u32[]{:S(2)}) collective-permute-start(bf16[768,128]{1,0:T(8,128)(2,1)S(1)} %get-tuple-element.30), channel_id=1, source_target_pairs={{0,24},{8,0},{16,8},{24,16},{1,25},{9,1},{17,9},{25,17},{2,26},{10... | collective-permute-start | bytes 589832 | tf_op jit(solution)/shard_map/ppermute | solution.py:244
  59.1 33.0 %collective-permute-start.10 = (bf16[128,1536]{1,0:T(8,128)(2,1)}, bf16[128,1536]{1,0:T(8,128)(2,1)S(1)}, u32[]{:S(2)}, u32[]{:S(2)}) collective-permute-start(bf16[128,1536]{1,0:T(8,128)(2,1)} %get-tuple-element.33), channel_id=1, source_target_pairs={{0,16},{8,24},{16,0},{24,8},{1,17},{9,25},{17,1},{25,9},{2,18},{10... | collective-permute-start | bytes 1179656 | tf_op jit(solution)/shard_map/ppermute | solution.py:244
  59.7 32.4 %collective-permute-start.11 = (bf16[128,1536]{1,0:T(8,128)(2,1)S(1)}, bf16[128,1536]{1,0:T(8,128)(2,1)S(1)}, u32[]{:S(2)}, u32[]{:S(2)}) collective-permute-start(bf16[128,1536]{1,0:T(8,128)(2,1)S(1)} %get-tuple-element.34), channel_id=1, source_target_pairs={{0,24},{8,0},{16,8},{24,16},{1,25},{9,1},{17,9},{25,17},{2,26},{10... | collective-permute-start | bytes 1179656 | tf_op jit(solution)/shard_map/ppermute | solution.py:244
  62.0 30.1 %collective-permute-start.9 = (bf16[128,1536]{1,0:T(8,128)(2,1)S(1)}, bf16[128,1536]{1,0:T(8,128)(2,1)S(1)}, u32[]{:S(2)}, u32[]{:S(2)}) collective-permute-start(bf16[128,1536]{1,0:T(8,128)(2,1)S(1)} %get-tuple-element.32), channel_id=1, source_target_pairs={{0,8},{8,16},{16,24},{24,0},{1,9},{9,17},{17,25},{25,1},{2,10},{10... | collective-permute-start | bytes 1179656 | tf_op jit(solution)/shard_map/ppermute | solution.py:244
  86.8 12.1 %all-to-all-start.3 = ((f32[16,32,128]{2,1,0:T(8,128)}), f32[16,32,128]{2,1,0:T(8,128)S(1)}, u32[]{:S(2)}, u32[]{:S(2)}) async-start(f32[16,32,128]{2,1,0:T(8,128)} %shard_map.150), calls=%async_computation.3 | async-start | bytes 524288 | tf_op jit(solution)/shard_map/all_to_all | solution.py:256
  100.6 20.4 %all-to-all-start.4 = ((bf16[8,2,16,768]{3,2,1,0:T(8,128)(2,1)}), bf16[8,2,16,768]{3,2,1,0:T(8,128)(2,1)S(1)}, u32[]{:S(2)}, u32[]{:S(2)}) async-start(bf16[8,2,16,768]{3,2,1,0:T(8,128)(2,1)} %shard_map.152), calls=%async_computation.4 | async-start | bytes 786432 | tf_op jit(solution)/shard_map/all_to_all | solution.py:256
  122.3 16.1 %all-to-all-start.5 = ((bf16[8,2,16,384]{3,2,1,0:T(8,128)(2,1)}), bf16[8,2,16,384]{3,2,1,0:T(8,128)(2,1)S(1)}, u32[]{:S(2)}, u32[]{:S(2)}) async-start(bf16[8,2,16,384]{3,2,1,0:T(8,128)(2,1)} %shard_map.153), calls=%async_computation.5 | async-start | bytes 393216 | tf_op jit(solution)/shard_map/all_to_all | solution.py:256
  127.8 25.5 %copy-start.3 = (f32[128]{0:T(128)S(1)}, f32[128]{0:T(128)}, u32[]{:S(2)}) copy-start(f32[128]{0:T(128)} %param.29) | copy-start | bytes 1540
  127.9 6.5 %collective-permute-start.12 = (bf16[768,128]{1,0:T(8,128)(2,1)S(1)}, bf16[768,128]{1,0:T(8,128)(2,1)S(1)}, u32[]{:S(2)}, u32[]{:S(2)}) collective-permute-start(bf16[768,128]{1,0:T(8,128)(2,1)S(1)} %get-tuple-element.36), channel_id=1, source_target_pairs={{0,8},{8,16},{16,24},{24,0},{1,9},{9,17},{17,25},{25,1},{2,10},{10... | collective-permute-start | bytes 589832 | tf_op jit(solution)/shard_map/ppermute | solution.py:244
  129.0 7.4 %collective-permute-start.13 = (bf16[768,128]{1,0:T(8,128)(2,1)S(1)}, bf16[768,128]{1,0:T(8,128)(2,1)S(1)}, u32[]{:S(2)}, u32[]{:S(2)}) collective-permute-start(bf16[768,128]{1,0:T(8,128)(2,1)S(1)} %get-tuple-element.37), channel_id=1, source_target_pairs={{0,16},{8,24},{16,0},{24,8},{1,17},{9,25},{17,1},{25,9},{2,18},{10... | collective-permute-start | bytes 589832 | tf_op jit(solution)/shard_map/ppermute | solution.py:244
  131.8 6.6 %collective-permute-start.14 = (bf16[768,128]{1,0:T(8,128)(2,1)S(1)}, bf16[768,128]{1,0:T(8,128)(2,1)S(1)}, u32[]{:S(2)}, u32[]{:S(2)}) collective-permute-start(bf16[768,128]{1,0:T(8,128)(2,1)S(1)} %get-tuple-element.38), channel_id=1, source_target_pairs={{0,24},{8,0},{16,8},{24,16},{1,25},{9,1},{17,9},{25,17},{2,26},{10... | collective-permute-start | bytes 589832 | tf_op jit(solution)/shard_map/ppermute | solution.py:244

commit v5 on v4

--- a/solution.py
+++ b/solution.py
@@ -19,7 +19,6 @@
 WIDTH = 4096
 LIMIT = 8 * 2**20
 
-SMEM = pl.BlockSpec(memory_space=pltpu.SMEM)
 VMEM = pl.BlockSpec(memory_space=pltpu.VMEM)
 HBM = pl.BlockSpec(memory_space=pltpu.HBM)
 BLOCKS = 4
@@ -34,15 +33,15 @@
     kernel = pl.pallas_call(
         body,
         out_shape=outs,
-        in_specs=[SMEM] + [HBM] * far + [VMEM] * (n_in - far),
+        in_specs=[HBM] * far + [VMEM] * (n_in - far),
         out_specs=[VMEM] * len(outs) if many else VMEM,
         scratch_shapes=list(scratch),
         compiler_params=pltpu.CompilerParams(vmem_limit_bytes=LIMIT),
     )
 
     def run(*args):
-        there = [pltpu.with_memory_space_constraint(v, pltpu.HBM) for v in args[1 : 1 + far]]
-        return kernel(args[0], *there, *args[1 + far :])
+        there = [pltpu.with_memory_space_constraint(v, pltpu.HBM) for v in args[:far]]
+        return kernel(*there, *args[far:])
 
     return run
 
@@ -86,15 +85,20 @@
 
 
 def pack_first_body(
-    at, gate, up, tokens, gain, p0, p1, p2, p3, other, chunks, gate_here, up_here, sems, here, sem
+    gate, up, tokens, gain, p0, p1, p2, p3, other, chunks, gate_here, up_here, sems, here, own, sem
 ):
-    x, c = at[0], at[2]
-    copy = pltpu.make_async_copy(tokens, here, sem)
-    copy.start()
+    x, c = lax.axis_index("x"), lax.axis_index("c")
+    copies = [
+        pltpu.make_async_copy(tokens, here, sem.at[0]),
+        pltpu.make_async_copy(gain, own, sem.at[1]),
+    ]
+    for copy in copies:
+        copy.start()
     cut_chunks(gate, up, gate_here, up_here, sems, chunks)
-    copy.wait()
+    for copy in copies:
+        copy.wait()
     stream = here[...].astype(F32)
-    scaled = (stream * gain[...]).astype(BF)
+    scaled = (stream * own[...]).astype(BF)
     high, low = high_low(jnp.sum(stream * stream, axis=1, keepdims=True))
     for k, out in enumerate((p0, p1, p2, p3)):
         index = 2 * lax.rem(x + k, NX) + c
@@ -105,8 +109,8 @@
     other[...] = chunks[2 * x + 1 - c]
 
 
-def pack_second_body(at, gate, up, p0, p1, p2, p3, chunks, gate_here, up_here, sems):
-    x = at[0]
+def pack_second_body(gate, up, p0, p1, p2, p3, chunks, gate_here, up_here, sems):
+    x = lax.axis_index("x")
     cut_chunks(gate, up, gate_here, up_here, sems, chunks)
     for k, out in enumerate((p0, p1, p2, p3)):
         index = 2 * lax.rem(x + k, NX)
@@ -114,8 +118,8 @@
         out[:, WIDE:] = chunks[index + 1]
 
 
-def pack_down_body(at, far, gain, p0, p1, p2, p3, down, sems):
-    x = at[0]
+def pack_down_body(far, gain, p0, p1, p2, p3, down, sems):
+    x = lax.axis_index("x")
     waits = loads(((far, down),), sems)
     value = gain[...]
     high = value.astype(BF).astype(F32)
@@ -145,8 +149,8 @@
     return jnp.dot(a, b, preferred_element_type=F32)
 
 
-def enter_first_body(at, r0, r1, r2, r3, q0, s1, s2, s3, out):
-    c = at[2]
+def enter_first_body(r0, r1, r2, r3, q0, s1, s2, s3, out):
+    c = lax.axis_index("c")
     mine = (r0, r1, r2, r3)
     theirs = (q0, s1, s2, s3)
     scaled = jnp.concatenate([r[:, WIDE:] for r in mine], axis=1)
@@ -163,8 +167,8 @@
         store_payload(out, slot, dot(scaled, weights), high, low)
 
 
-def enter_second_body(at, stream, d0, d1, d2, d3, w0, w1, w2, w3, out):
-    x = at[0]
+def enter_second_body(stream, d0, d1, d2, d3, w0, w1, w2, w3, out):
+    x = lax.axis_index("x")
     scaled = []
     squares = jnp.zeros((N, 1), F32)
     for k, d in enumerate((d0, d1, d2, d3)):
@@ -182,7 +186,9 @@
         store_payload(out, slot, dot(scaled, weights), high, low)
 
 
-def hidden_body(at, got, scales, out):
+def hidden_body(got, gate_scales, up_scales, out):
+    x = lax.axis_index("x")
+    blank = jnp.zeros((1, PAD - HALF), F32)
     rows = N // NZ
     tile = jnp.zeros((rows, N), F32)
     for z in range(NZ):
@@ -196,7 +202,10 @@
         sums = got[0, h].astype(F32)
         for z in range(1, NZ):
             sums = sums + got[z, h].astype(F32)
-        scaled = sums * inverse * scales[h : h + 1, :]
+        index = 2 * x + h
+        gate_row, up_row = gate_scales[pl.ds(index, 1), :], up_scales[pl.ds(index, 1), :]
+        row = jnp.concatenate([gate_row, blank, up_row, blank], axis=1)
+        scaled = sums * inverse * row
         gate = scaled[:, :PAD]
         hidden = gate / (1.0 + jnp.exp(-gate)) * scaled[:, PAD:]
         hidden = hidden.astype(BF)
@@ -209,23 +218,23 @@
     return [dot(wide, d[...]).astype(BF) for d in pieces]
 
 
-def leave_first_body(at, hidden, d0, d1, d2, d3, out):
-    x = at[0]
+def leave_first_body(hidden, d0, d1, d2, d3, out):
+    x = lax.axis_index("x")
     for k, part in enumerate(down_sums(hidden, (d0, d1, d2, d3))):
         index = lax.rem(x + NX - k, NX)
         out[pl.ds(index * NY, NY)] = part.reshape(NY, N // NY, N)
 
 
-def leave_second_body(at, hidden, d0, d1, d2, d3, out):
-    x = at[0]
+def leave_second_body(hidden, d0, d1, d2, d3, out):
+    x = lax.axis_index("x")
     for k, part in enumerate(down_sums(hidden, (d0, d1, d2, d3))):
         index = lax.rem(x + NX - k, NX)
         for y in range(NY):
             out[index * NY + y] = part
 
 
-def stream_body(at, got, tokens, scale, out):
-    y = at[1]
+def stream_body(got, tokens, scale, out):
+    y = lax.axis_index("y")
     rows = N // NY
     branch = jnp.sum(got[...].astype(F32), axis=0) * scale[...]
     old = tokens[pl.ds(pl.multiple_of(y * rows, rows), rows), :].astype(F32)
@@ -233,8 +242,8 @@
     out[...] = jnp.broadcast_to(new[None], out.shape)
 
 
-def final_body(at, got, stream, scale, out):
-    x = at[0]
+def final_body(got, stream, scale, out):
+    x = lax.axis_index("x")
     branch = jnp.sum(got[...].astype(F32), axis=0) * scale[...]
     old = stream[pl.ds(x * NY, NY)].reshape(N, N)
     out[...] = 0.5 * old + 0.5 * branch
@@ -256,12 +265,8 @@
     return lax.all_to_all(v, axis, 0, 0, tiled=True)
 
 
-def scale_rows(gate_scale, up_scale, x):
-    rows = []
-    for scale in (gate_scale, up_scale):
-        own = lax.dynamic_slice_in_dim(scale, x * CHUNK, CHUNK, 0).reshape(2, HALF)
-        rows.append(jnp.pad(own, ((0, 0), (0, PAD - HALF))))
-    return jnp.concatenate(rows, axis=1)
+def by_chunk(scale):
+    return scale.reshape(2 * NX, HALF)
 
 
 def local(
@@ -281,57 +286,60 @@
     second_down,
     second_down_scale,
 ):
-    x = lax.axis_index("x")
-    at = jnp.stack([x, lax.axis_index("y"), lax.axis_index("c")]).astype(jnp.int32)
     columns = 2 * NX * HALF
     wide_here = pltpu.VMEM((N, columns), F32)
     sems = pltpu.SemaphoreType.DMA((BLOCKS, 2))
     cutting = [pltpu.VMEM((2 * NX, N, WIDE), BF), wide_here, wide_here, sems]
-    entering = [*cutting, pltpu.VMEM((N, N), BF), pltpu.SemaphoreType.DMA(())]
+    entering = [
+        *cutting,
+        pltpu.VMEM((N, N), BF),
+        pltpu.VMEM((1, N), F32),
+        pltpu.SemaphoreType.DMA((2,)),
+    ]
     lowering = [pltpu.VMEM((columns, N), F32), pltpu.SemaphoreType.DMA((BLOCKS, 1))]
     payload = shape(NZ, 2, N // NZ, WIDE)
     spread = shape(NZ, 2, N // NZ, PAD)
 
     *packed, other = call(
-        pack_first_body, [shape(N, WIDE + N)] * NX + [shape(N, WIDE)], 4, entering, 3
-    )(at, first_gate, first_up, tokens, first_gain[None])
+        pack_first_body, [shape(N, WIDE + N)] * NX + [shape(N, WIDE)], 4, entering, 4
+    )(first_gate, first_up, tokens, first_gain[None])
     mine = around(packed)
     theirs = [other] + [other_core(v) for v in mine[1:]]
-    sums = call(enter_first_body, payload, 8)(at, *mine, *theirs)
+    sums = call(enter_first_body, payload, 8)(*mine, *theirs)
     got = swap(sums, "z")
     downs = around(
         call(pack_down_body, [shape(2 * PAD, N)] * NX, 2, lowering, 1)(
-            at, first_down, second_gain[None]
+            first_down, second_gain[None]
         ),
     )
     ups = around(
-        call(pack_second_body, [shape(N, 2 * WIDE)] * NX, 2, cutting, 2)(
-            at, second_gate, second_up
-        ),
+        call(pack_second_body, [shape(N, 2 * WIDE)] * NX, 2, cutting, 2)(second_gate, second_up),
     )
     last_downs = around(
         call(pack_down_body, [shape(2 * PAD, N)] * NX, 2, lowering, 1)(
-            at, second_down, second_gain[None]
+            second_down, second_gain[None]
         ),
     )
-    hidden = call(hidden_body, spread, 2)(at, got, scale_rows(first_gate_scale, first_up_scale, x))
+    hidden = call(hidden_body, spread, 3)(got, by_chunk(first_gate_scale), by_chunk(first_up_scale))
     hidden = swap(hidden, "z")
-    part = call(leave_first_body, shape(NX * NY, N // NY, N), 5)(at, hidden, *downs)
+    part = call(leave_first_body, shape(NX * NY, N // NY, N), 5)(
+        hidden, *downs
+    )
     got = swap(part, XY)
     stream = call(stream_body, shape(NX * NY, N // NY, N, dtype=F32), 3)(
-        at, got, tokens, first_down_scale[None]
+        got, tokens, first_down_scale[None]
     )
     stream = swap(stream, XY)
 
-    sums = call(enter_second_body, payload, 9)(at, stream, *downs, *ups)
+    sums = call(enter_second_body, payload, 9)(stream, *downs, *ups)
     got = swap(sums, "z")
-    hidden = call(hidden_body, spread, 2)(
-        at, got, scale_rows(second_gate_scale, second_up_scale, x)
+    hidden = call(hidden_body, spread, 3)(
+        got, by_chunk(second_gate_scale), by_chunk(second_up_scale)
     )
     hidden = swap(hidden, "z")
-    part = call(leave_second_body, shape(NX * NY, N, N), 5)(at, hidden, *last_downs)
+    part = call(leave_second_body, shape(NX * NY, N, N), 5)(hidden, *last_downs)
     got = swap(part, XY)
-    return call(final_body, shape(N, N, dtype=F32), 3)(at, got, stream, second_down_scale[None])
+    return call(final_body, shape(N, N, dtype=F32), 3)(got, stream, second_down_scale[None])
 
 
 def solution(mesh):

time: 157 us -> 151 us (0.962)
  Pallas kernels: 20.3 us -> 13.8 us
  local copies, waits for them, and re-layouts: 4.07 us -> 0.33 us
  waiting for transfers between devices: 52.6 us -> 56.2 us
    pallas_call x12, Pallas kernels: 20.3 us -> 13.8 us  [run(): return kernel(*there, *args[far:])]
    all_to_all x5, waiting for transfers between devices: 31.7 us -> 34.9 us  [swap(): return lax.all_to_all(v, axis, 0, 0, tiled=True)]
    dynamic_slice x4 -> x0, local copies, waits for them, and re-layouts: 3.08 us -> none  [scale_rows(): own = lax.dynamic_slice_in_dim(scale, x * CHUNK, CHUNK, 0).reshape(2, HALF)]
  transfers between devices with their start and end apart: 20 -> 20, of which waited for: 11 -> 12; matrix products, arithmetic and copies ran while one was open for 2% -> 0% of each run, Pallas kernels for 6% -> 5%
where the time goes in v5:
time: 151 us; the launch traced here: 148 us
  waiting for transfers between devices  56.2 us (37%)
  starting transfers between devices  44.9 us (30%)
  blocking collectives  33 us (22%)
  Pallas kernels  13.8 us (9%)
    all_to_all x5, waiting for transfers between devices, swap(): return lax.all_to_all(v, axis, 0, 0, tiled=True)  34.9 us
    all_to_all x2, blocking collectives, swap(): return lax.all_to_all(v, axis, 0, 0, tiled=True)  33 us
    all_to_all x5, starting transfers between devices, swap(): return lax.all_to_all(v, axis, 0, 0, tiled=True)  27.8 us
    ppermute x12, waiting for transfers between devices, shift(): return lax.ppermute(v, 'x', [(i, (i + k) % NX) for i in range(NX)])  19.8 us
    ppermute x12, starting transfers between devices, shift(): return lax.ppermute(v, 'x', [(i, (i + k) % NX) for i in range(NX)])  17.1 us
    pallas_call x12, Pallas kernels, run(): return kernel(*there, *args[far:])  13.8 us
  transfers between devices with their start and end apart: 20, of which 12 were waited for; matrix products, arithmetic and copies ran while one was open for 0% of the time, Pallas kernels for 5%

profile of v5, /device:TPU:2, one launch (start us, length us, event | category | flops | bytes accessed | tf_op | source)
XLA Modules:
  0.0 148.4 jit_solution(10815132335512721722)
XLA Ops:
  0.0 2.1 %shard_map.145 = (bf16[128,896]{1,0:T(8,128)(2,1)S(1)}, bf16[128,896]{1,0:T(8,128)(2,1)S(1)}, bf16[128,896]{1,0:T(8,128)(2,1)S(1)}, bf16[128,896]{1,0:T(8,128)(2,1)S(1)}, bf16[128,768]{1,0:T(8,128)(2,1)S(1)}) custom-call(f32[128,2816]{1,0:T(8,128)} %gate.2, f32[128,2816]{1,0:T(8,128)} %up.2, bf16[128,128]{1,0:T(8,128)(2,1)} %tokens.3, f32[1,128]{1,0:T(1,128)} %bitcast.8), custom_call_target="tpu_custom_call" | custom-call | tf_op jit(solution)/shard_map/pallas_call | solution.py:44
  2.2 1.6 %collective-permute-start = (bf16[128,896]{1,0:T(8,128)(2,1)S(1)}, bf16[128,896]{1,0:T(8,128)(2,1)S(1)}, u32[]{:S(2)}, u32[]{:S(2)}) collective-permute-start(bf16[128,896]{1,0:T(8,128)(2,1)S(1)} %get-tuple-element.23), channel_id=1, source_target_pairs={{0,8},{8,16},{16,24},{24,0},{1,9},{9,17},{17,25},{25,1},{2,10},{10... | collective-permute-start | bytes 688136 | tf_op jit(solution)/shard_map/ppermute | solution.py:253
  3.7 2.8 %collective-permute-start.1 = (bf16[128,896]{1,0:T(8,128)(2,1)S(1)}, bf16[128,896]{1,0:T(8,128)(2,1)S(1)}, u32[]{:S(2)}, u32[]{:S(2)}) collective-permute-start(bf16[128,896]{1,0:T(8,128)(2,1)S(1)} %get-tuple-element.24), channel_id=1, source_target_pairs={{0,16},{8,24},{16,0},{24,8},{1,17},{9,25},{17,1},{25,9},{2,18},{10... | collective-permute-start | bytes 688136 | tf_op jit(solution)/shard_map/ppermute | solution.py:253
  6.5 0.4 collective-permute-start.2
  7.0 3.9 %collective-permute-done.r1 = bf16[128,896]{1,0:T(8,128)(2,1)S(1)} collective-permute-done((bf16[128,896]{1,0:T(8,128)(2,1)S(1)}, bf16[128,896]{1,0:T(8,128)(2,1)S(1)}, u32[]{:S(2)}, u32[]{:S(2)}) %collective-permute-start) | collective-permute-done | bytes 229408 | tf_op jit(solution)/shard_map/ppermute | solution.py:253
  10.9 2.8 %collective-permute-done.1.r2 = bf16[128,896]{1,0:T(8,128)(2,1)S(1)} collective-permute-done((bf16[128,896]{1,0:T(8,128)(2,1)S(1)}, bf16[128,896]{1,0:T(8,128)(2,1)S(1)}, u32[]{:S(2)}, u32[]{:S(2)}) %collective-permute-start.1) | collective-permute-done | bytes 229408 | tf_op jit(solution)/shard_map/ppermute | solution.py:253
  13.7 2.7 %collective-permute-done.2.r3 = bf16[128,896]{1,0:T(8,128)(2,1)S(1)} collective-permute-done((bf16[128,896]{1,0:T(8,128)(2,1)S(1)}, bf16[128,896]{1,0:T(8,128)(2,1)S(1)}, u32[]{:S(2)}, u32[]{:S(2)}) %collective-permute-start.2) | collective-permute-done | bytes 229408 | tf_op jit(solution)/shard_map/ppermute | solution.py:253
  16.5 1.5 collective-permute-done.5.s3
  17.9 1.1 shard_map.146
  19.1 8.7 %all-to-all-start = ((bf16[8,2,16,768]{3,2,1,0:T(8,128)(2,1)}), bf16[8,2,16,768]{3,2,1,0:T(8,128)(2,1)S(1)}, u32[]{:S(2)}, u32[]{:S(2)}) async-start(bf16[8,2,16,768]{3,2,1,0:T(8,128)(2,1)} %shard_map.146), calls=%async_computation | async-start | bytes 786432 | tf_op jit(solution)/shard_map/all_to_all | solution.py:265
  27.8 0.1 reshape.12.gate_scales
  27.8 0.1 reshape.13.up_scales
  27.9 14.8 %all-to-all-done.got = bf16[8,2,16,768]{3,2,1,0:T(8,128)(2,1)S(1)} async-done(((bf16[8,2,16,768]{3,2,1,0:T(8,128)(2,1)}), bf16[8,2,16,768]{3,2,1,0:T(8,128)(2,1)S(1)}, u32[]{:S(2)}, u32[]{:S(2)}) %all-to-all-start) | async-done | bytes 393248 | tf_op jit(solution)/shard_map/all_to_all | solution.py:265
  42.7 0.8 shard_map.147
  43.6 3.4 %all-to-all-start.1 = ((bf16[8,2,16,384]{3,2,1,0:T(8,128)(2,1)}), bf16[8,2,16,384]{3,2,1,0:T(8,128)(2,1)S(1)}, u32[]{:S(2)}, u32[]{:S(2)}) async-start(bf16[8,2,16,384]{3,2,1,0:T(8,128)(2,1)} %shard_map.147), calls=%async_computation.1 | async-start | bytes 393216 | tf_op jit(solution)/shard_map/all_to_all | solution.py:265
  47.0 1.4 shard_map.148
  48.4 1.4 collective-permute-start.6
  49.8 1.9 %collective-permute-start.7 = (bf16[768,128]{1,0:T(8,128)(2,1)S(1)}, bf16[768,128]{1,0:T(8,128)(2,1)S(1)}, u32[]{:S(2)}, u32[]{:S(2)}) collective-permute-start(bf16[768,128]{1,0:T(8,128)(2,1)S(1)} %get-tuple-element.29), channel_id=1, source_target_pairs={{0,16},{8,24},{16,0},{24,8},{1,17},{9,25},{17,1},{25,9},{2,18},{10... | collective-permute-start | bytes 589832 | tf_op jit(solution)/shard_map/ppermute | solution.py:253
  51.6 1.3 collective-permute-start.8
  52.9 2.8 %shard_map.151 = (bf16[128,1536]{1,0:T(8,128)(2,1)S(1)}, bf16[128,1536]{1,0:T(8,128)(2,1)S(1)}, bf16[128,1536]{1,0:T(8,128)(2,1)}, bf16[128,1536]{1,0:T(8,128)(2,1)S(1)}) custom-call(f32[128,2816]{1,0:T(8,128)} %gate.3, f32[128,2816]{1,0:T(8,128)} %up.3), custom_call_target="tpu_custom_call" | custom-call | tf_op jit(solution)/shard_map/pallas_call | solution.py:44
  55.7 0.6 collective-permute-start.10
  56.3 2.3 %collective-permute-start.11 = (bf16[128,1536]{1,0:T(8,128)(2,1)S(1)}, bf16[128,1536]{1,0:T(8,128)(2,1)S(1)}, u32[]{:S(2)}, u32[]{:S(2)}) collective-permute-start(bf16[128,1536]{1,0:T(8,128)(2,1)S(1)} %get-tuple-element.34), channel_id=1, source_target_pairs={{0,24},{8,0},{16,8},{24,16},{1,25},{9,1},{17,9},{25,17},{2,26},{10... | collective-permute-start | bytes 1179656 | tf_op jit(solution)/shard_map/ppermute | solution.py:253
  58.6 0.2 collective-permute-start.9
  58.8 0.3 collective-permute-done.7.d2
  59.1 4.3 %collective-permute-done.8.d3 = bf16[768,128]{1,0:T(8,128)(2,1)S(1)} collective-permute-done((bf16[768,128]{1,0:T(8,128)(2,1)S(1)}, bf16[768,128]{1,0:T(8,128)(2,1)S(1)}, u32[]{:S(2)}, u32[]{:S(2)}) %collective-permute-start.8) | collective-permute-done | bytes 196640 | tf_op jit(solution)/shard_map/ppermute | solution.py:253
  63.4 0.4 shard_map.149
  63.7 18.9 %all_to_all.35.got = bf16[16,32,128]{2,1,0:T(8,128)(2,1)S(1)} all-to-all(bf16[16,32,128]{2,1,0:T(8,128)(2,1)S(1)} %shard_map.149), channel_id=1, replica_groups=mesh['z'=8,'x'=4,'y'=4,'c'=2] {'x','y'}, dimensions={0} | all-to-all | bytes 262144 | tf_op jit(solution)/shard_map/all_to_all | solution.py:265
  82.6 0.8 shard_map.150
  83.4 5.3 %all-to-all-start.3 = ((f32[16,32,128]{2,1,0:T(8,128)}), f32[16,32,128]{2,1,0:T(8,128)S(1)}, u32[]{:S(2)}, u32[]{:S(2)}) async-start(f32[16,32,128]{2,1,0:T(8,128)} %shard_map.150), calls=%async_computation.3 | async-start | bytes 524288 | tf_op jit(solution)/shard_map/all_to_all | solution.py:265
  88.7 6.8 %all-to-all-done.3.stream = f32[16,32,128]{2,1,0:T(8,128)S(1)} async-done(((f32[16,32,128]{2,1,0:T(8,128)}), f32[16,32,128]{2,1,0:T(8,128)S(1)}, u32[]{:S(2)}, u32[]{:S(2)}) %all-to-all-start.3) | async-done | bytes 262176 | tf_op jit(solution)/shard_map/all_to_all | solution.py:265
  95.5 1.1 shard_map.152
  96.6 7.0 %all-to-all-start.4 = ((bf16[8,2,16,768]{3,2,1,0:T(8,128)(2,1)}), bf16[8,2,16,768]{3,2,1,0:T(8,128)(2,1)S(1)}, u32[]{:S(2)}, u32[]{:S(2)}) async-start(bf16[8,2,16,768]{3,2,1,0:T(8,128)(2,1)} %shard_map.152), calls=%async_computation.4 | async-start | bytes 786432 | tf_op jit(solution)/shard_map/all_to_all | solution.py:265
  103.6 0.1 reshape.14.gate_scales
  103.7 0.1 reshape.15.up_scales
  103.8 13.2 %all-to-all-done.4.got = bf16[8,2,16,768]{3,2,1,0:T(8,128)(2,1)S(1)} async-done(((bf16[8,2,16,768]{3,2,1,0:T(8,128)(2,1)}), bf16[8,2,16,768]{3,2,1,0:T(8,128)(2,1)S(1)}, u32[]{:S(2)}, u32[]{:S(2)}) %all-to-all-start.4) | async-done | bytes 393248 | tf_op jit(solution)/shard_map/all_to_all | solution.py:265
  117.0 0.8 shard_map.153
  117.8 3.4 %all-to-all-start.5 = ((bf16[8,2,16,384]{3,2,1,0:T(8,128)(2,1)}), bf16[8,2,16,384]{3,2,1,0:T(8,128)(2,1)S(1)}, u32[]{:S(2)}, u32[]{:S(2)}) async-start(bf16[8,2,16,384]{3,2,1,0:T(8,128)(2,1)} %shard_map.153), calls=%async_computation.5 | async-start | bytes 393216 | tf_op jit(solution)/shard_map/all_to_all | solution.py:265
  121.2 1.4 shard_map.154
  122.7 0.0 copy-start.3
  122.7 1.2 collective-permute-start.12
  123.8 2.8 %collective-permute-start.13 = (bf16[768,128]{1,0:T(8,128)(2,1)S(1)}, bf16[768,128]{1,0:T(8,128)(2,1)S(1)}, u32[]{:S(2)}, u32[]{:S(2)}) collective-permute-start(bf16[768,128]{1,0:T(8,128)(2,1)S(1)} %get-tuple-element.37), channel_id=1, source_target_pairs={{0,16},{8,24},{16,0},{24,8},{1,17},{9,25},{17,1},{25,9},{2,18},{10... | collective-permute-start | bytes 589832 | tf_op jit(solution)/shard_map/ppermute | solution.py:253
  126.6 0.8 collective-permute-start.14
  127.3 1.8 %collective-permute-done.12.d1 = bf16[768,128]{1,0:T(8,128)(2,1)S(1)} collective-permute-done((bf16[768,128]{1,0:T(8,128)(2,1)S(1)}, bf16[768,128]{1,0:T(8,128)(2,1)S(1)}, u32[]{:S(2)}, u32[]{:S(2)}) %collective-permute-start.12) | collective-permute-done | bytes 196640 | tf_op jit(solution)/shard_map/ppermute | solution.py:253
  129.1 2.1 %collective-permute-done.13.d2 = bf16[768,128]{1,0:T(8,128)(2,1)S(1)} collective-permute-done((bf16[768,128]{1,0:T(8,128)(2,1)S(1)}, bf16[768,128]{1,0:T(8,128)(2,1)S(1)}, u32[]{:S(2)}, u32[]{:S(2)}) %collective-permute-start.13) | collective-permute-done | bytes 196640 | tf_op jit(solution)/shard_map/ppermute | solution.py:253
  131.2 2.0 %collective-permute-done.14.d3 = bf16[768,128]{1,0:T(8,128)(2,1)S(1)} collective-permute-done((bf16[768,128]{1,0:T(8,128)(2,1)S(1)}, bf16[768,128]{1,0:T(8,128)(2,1)S(1)}, u32[]{:S(2)}, u32[]{:S(2)}) %collective-permute-start.14) | collective-permute-done | bytes 196640 | tf_op jit(solution)/shard_map/ppermute | solution.py:253
  133.2 0.4 shard_map.155
  133.6 14.1 %all_to_all.36.got = bf16[16,128,128]{2,1,0:T(8,128)(2,1)S(1)} all-to-all(bf16[16,128,128]{2,1,0:T(8,128)(2,1)S(1)} %shard_map.155), channel_id=1, replica_groups=mesh['z'=8,'x'=4,'y'=4,'c'=2] {'x','y'}, dimensions={0} | all-to-all | bytes 1048576 | tf_op jit(solution)/shard_map/all_to_all | solution.py:265
  147.7 0.7 shard_map.156
  (26 shorter events, 0.1 us)
Async XLA Ops:
  2.2 8.8 %collective-permute-start = (bf16[128,896]{1,0:T(8,128)(2,1)S(1)}, bf16[128,896]{1,0:T(8,128)(2,1)S(1)}, u32[]{:S(2)}, u32[]{:S(2)}) collective-permute-start(bf16[128,896]{1,0:T(8,128)(2,1)S(1)} %get-tuple-element.23), channel_id=1, source_target_pairs={{0,8},{8,16},{16,24},{24,0},{1,9},{9,17},{17,25},{25,1},{2,10},{10... | collective-permute-start | bytes 688136 | tf_op jit(solution)/shard_map/ppermute | solution.py:253
  3.7 10.0 %collective-permute-start.1 = (bf16[128,896]{1,0:T(8,128)(2,1)S(1)}, bf16[128,896]{1,0:T(8,128)(2,1)S(1)}, u32[]{:S(2)}, u32[]{:S(2)}) collective-permute-start(bf16[128,896]{1,0:T(8,128)(2,1)S(1)} %get-tuple-element.24), channel_id=1, source_target_pairs={{0,16},{8,24},{16,0},{24,8},{1,17},{9,25},{17,1},{25,9},{2,18},{10... | collective-permute-start | bytes 688136 | tf_op jit(solution)/shard_map/ppermute | solution.py:253
  6.5 9.9 %collective-permute-start.2 = (bf16[128,896]{1,0:T(8,128)(2,1)S(1)}, bf16[128,896]{1,0:T(8,128)(2,1)S(1)}, u32[]{:S(2)}, u32[]{:S(2)}) collective-permute-start(bf16[128,896]{1,0:T(8,128)(2,1)S(1)} %get-tuple-element.25), channel_id=1, source_target_pairs={{0,24},{8,0},{16,8},{24,16},{1,25},{9,1},{17,9},{25,17},{2,26},{10... | collective-permute-start | bytes 688136 | tf_op jit(solution)/shard_map/ppermute | solution.py:253
  10.9 5.5 %collective-permute-start.3 = (bf16[128,896]{1,0:T(8,128)(2,1)S(1)}, bf16[128,896]{1,0:T(8,128)(2,1)S(1)}, u32[]{:S(2)}, u32[]{:S(2)}) collective-permute-start(bf16[128,896]{1,0:T(8,128)(2,1)S(1)} %collective-permute-done.r1), channel_id=1, source_target_pairs={{0,1},{1,0},{2,3},{3,2},{4,5},{5,4},{6,7},{7,6},{8,9},{9,8},{10,11... | collective-permute-start | bytes 688136 | tf_op jit(solution)/shard_map/ppermute | solution.py:257
  13.7 2.7 %collective-permute-start.4 = (bf16[128,896]{1,0:T(8,128)(2,1)S(1)}, bf16[128,896]{1,0:T(8,128)(2,1)S(1)}, u32[]{:S(2)}, u32[]{:S(2)}) collective-permute-start(bf16[128,896]{1,0:T(8,128)(2,1)S(1)} %collective-permute-done.1.r2), channel_id=1, source_target_pairs={{0,1},{1,0},{2,3},{3,2},{4,5},{5,4},{6,7},{7,6},{8,9},{9,8},{10,11... | collective-permute-start | bytes 688136 | tf_op jit(solution)/shard_map/ppermute | solution.py:257
  16.4 1.5 %collective-permute-start.5 = (bf16[128,896]{1,0:T(8,128)(2,1)S(1)}, bf16[128,896]{1,0:T(8,128)(2,1)S(1)}, u32[]{:S(2)}, u32[]{:S(2)}) collective-permute-start(bf16[128,896]{1,0:T(8,128)(2,1)S(1)} %collective-permute-done.2.r3), channel_id=1, source_target_pairs={{0,1},{1,0},{2,3},{3,2},{4,5},{5,4},{6,7},{7,6},{8,9},{9,8},{10,11... | collective-permute-start | bytes 688136 | tf_op jit(solution)/shard_map/ppermute | solution.py:257
  17.9 9.8 %copy-start.4 = (f32[2816]{0:T(1024)S(1)}, f32[2816]{0:T(1024)}, u32[]{:S(2)}) copy-start(f32[2816]{0:T(1024)} %param.18) | copy-start | bytes 33796
  17.9 9.9 %copy-start.5 = (f32[2816]{0:T(1024)S(1)}, f32[2816]{0:T(1024)}, u32[]{:S(2)}) copy-start(f32[2816]{0:T(1024)} %param.20) | copy-start | bytes 33796
  19.1 27.9 %copy-start.1 = (f32[128]{0:T(128)S(1)}, f32[128]{0:T(128)}, u32[]{:S(2)}) copy-start(f32[128]{0:T(128)} %param.23) | copy-start | bytes 1540
  19.1 23.7 %all-to-all-start = ((bf16[8,2,16,768]{3,2,1,0:T(8,128)(2,1)}), bf16[8,2,16,768]{3,2,1,0:T(8,128)(2,1)S(1)}, u32[]{:S(2)}, u32[]{:S(2)}) async-start(bf16[8,2,16,768]{3,2,1,0:T(8,128)(2,1)} %shard_map.146), calls=%async_computation | async-start | bytes 786432 | tf_op jit(solution)/shard_map/all_to_all | solution.py:265
  43.6 19.8 %all-to-all-start.1 = ((bf16[8,2,16,384]{3,2,1,0:T(8,128)(2,1)}), bf16[8,2,16,384]{3,2,1,0:T(8,128)(2,1)S(1)}, u32[]{:S(2)}, u32[]{:S(2)}) async-start(bf16[8,2,16,384]{3,2,1,0:T(8,128)(2,1)} %shard_map.147), calls=%async_computation.1 | async-start | bytes 393216 | tf_op jit(solution)/shard_map/all_to_all | solution.py:265
  48.4 10.2 %collective-permute-start.6 = (bf16[768,128]{1,0:T(8,128)(2,1)S(1)}, bf16[768,128]{1,0:T(8,128)(2,1)S(1)}, u32[]{:S(2)}, u32[]{:S(2)}) collective-permute-start(bf16[768,128]{1,0:T(8,128)(2,1)S(1)} %get-tuple-element.28), channel_id=1, source_target_pairs={{0,8},{8,16},{16,24},{24,0},{1,9},{9,17},{17,25},{25,1},{2,10},{10... | collective-permute-start | bytes 589832 | tf_op jit(solution)/shard_map/ppermute | solution.py:253
  49.8 9.3 %collective-permute-start.7 = (bf16[768,128]{1,0:T(8,128)(2,1)S(1)}, bf16[768,128]{1,0:T(8,128)(2,1)S(1)}, u32[]{:S(2)}, u32[]{:S(2)}) collective-permute-start(bf16[768,128]{1,0:T(8,128)(2,1)S(1)} %get-tuple-element.29), channel_id=1, source_target_pairs={{0,16},{8,24},{16,0},{24,8},{1,17},{9,25},{17,1},{25,9},{2,18},{10... | collective-permute-start | bytes 589832 | tf_op jit(solution)/shard_map/ppermute | solution.py:253
  51.6 31.0 %copy-start = (bf16[128,128]{1,0:T(8,128)(2,1)S(1)}, bf16[128,128]{1,0:T(8,128)(2,1)}, u32[]{:S(2)}) copy-start(bf16[128,128]{1,0:T(8,128)(2,1)} %tokens.3) | copy-start | bytes 98308
  51.6 31.0 %copy-start.2 = (f32[128]{0:T(128)S(1)}, f32[128]{0:T(128)}, u32[]{:S(2)}) copy-start(f32[128]{0:T(128)} %param.22) | copy-start | bytes 1540
  51.6 11.7 %collective-permute-start.8 = (bf16[768,128]{1,0:T(8,128)(2,1)S(1)}, bf16[768,128]{1,0:T(8,128)(2,1)S(1)}, u32[]{:S(2)}, u32[]{:S(2)}) collective-permute-start(bf16[768,128]{1,0:T(8,128)(2,1)S(1)} %get-tuple-element.30), channel_id=1, source_target_pairs={{0,24},{8,0},{16,8},{24,16},{1,25},{9,1},{17,9},{25,17},{2,26},{10... | collective-permute-start | bytes 589832 | tf_op jit(solution)/shard_map/ppermute | solution.py:253
  55.7 33.0 %collective-permute-start.10 = (bf16[128,1536]{1,0:T(8,128)(2,1)}, bf16[128,1536]{1,0:T(8,128)(2,1)S(1)}, u32[]{:S(2)}, u32[]{:S(2)}) collective-permute-start(bf16[128,1536]{1,0:T(8,128)(2,1)} %get-tuple-element.33), channel_id=1, source_target_pairs={{0,16},{8,24},{16,0},{24,8},{1,17},{9,25},{17,1},{25,9},{2,18},{10... | collective-permute-start | bytes 1179656 | tf_op jit(solution)/shard_map/ppermute | solution.py:253
  56.3 32.4 %collective-permute-start.11 = (bf16[128,1536]{1,0:T(8,128)(2,1)S(1)}, bf16[128,1536]{1,0:T(8,128)(2,1)S(1)}, u32[]{:S(2)}, u32[]{:S(2)}) collective-permute-start(bf16[128,1536]{1,0:T(8,128)(2,1)S(1)} %get-tuple-element.34), channel_id=1, source_target_pairs={{0,24},{8,0},{16,8},{24,16},{1,25},{9,1},{17,9},{25,17},{2,26},{10... | collective-permute-start | bytes 1179656 | tf_op jit(solution)/shard_map/ppermute | solution.py:253
  58.6 30.1 %collective-permute-start.9 = (bf16[128,1536]{1,0:T(8,128)(2,1)S(1)}, bf16[128,1536]{1,0:T(8,128)(2,1)S(1)}, u32[]{:S(2)}, u32[]{:S(2)}) collective-permute-start(bf16[128,1536]{1,0:T(8,128)(2,1)S(1)} %get-tuple-element.32), channel_id=1, source_target_pairs={{0,8},{8,16},{16,24},{24,0},{1,9},{9,17},{17,25},{25,1},{2,10},{10... | collective-permute-start | bytes 1179656 | tf_op jit(solution)/shard_map/ppermute | solution.py:253
  83.4 12.1 %all-to-all-start.3 = ((f32[16,32,128]{2,1,0:T(8,128)}), f32[16,32,128]{2,1,0:T(8,128)S(1)}, u32[]{:S(2)}, u32[]{:S(2)}) async-start(f32[16,32,128]{2,1,0:T(8,128)} %shard_map.150), calls=%async_computation.3 | async-start | bytes 524288 | tf_op jit(solution)/shard_map/all_to_all | solution.py:265
  95.5 8.1 %copy-start.6 = (f32[2816]{0:T(1024)S(1)}, f32[2816]{0:T(1024)}, u32[]{:S(2)}) copy-start(f32[2816]{0:T(1024)} %param.25) | copy-start | bytes 33796
  95.5 8.2 %copy-start.7 = (f32[2816]{0:T(1024)S(1)}, f32[2816]{0:T(1024)}, u32[]{:S(2)}) copy-start(f32[2816]{0:T(1024)} %param.27) | copy-start | bytes 33796
  96.6 20.4 %all-to-all-start.4 = ((bf16[8,2,16,768]{3,2,1,0:T(8,128)(2,1)}), bf16[8,2,16,768]{3,2,1,0:T(8,128)(2,1)S(1)}, u32[]{:S(2)}, u32[]{:S(2)}) async-start(bf16[8,2,16,768]{3,2,1,0:T(8,128)(2,1)} %shard_map.152), calls=%async_computation.4 | async-start | bytes 786432 | tf_op jit(solution)/shard_map/all_to_all | solution.py:265
  117.8 15.4 %all-to-all-start.5 = ((bf16[8,2,16,384]{3,2,1,0:T(8,128)(2,1)}), bf16[8,2,16,384]{3,2,1,0:T(8,128)(2,1)S(1)}, u32[]{:S(2)}, u32[]{:S(2)}) async-start(bf16[8,2,16,384]{3,2,1,0:T(8,128)(2,1)} %shard_map.153), calls=%async_computation.5 | async-start | bytes 393216 | tf_op jit(solution)/shard_map/all_to_all | solution.py:265
  122.7 25.0 %copy-start.3 = (f32[128]{0:T(128)S(1)}, f32[128]{0:T(128)}, u32[]{:S(2)}) copy-start(f32[128]{0:T(128)} %param.29) | copy-start | bytes 1540
  122.7 6.5 %collective-permute-start.12 = (bf16[768,128]{1,0:T(8,128)(2,1)S(1)}, bf16[768,128]{1,0:T(8,128)(2,1)S(1)}, u32[]{:S(2)}, u32[]{:S(2)}) collective-permute-start(bf16[768,128]{1,0:T(8,128)(2,1)S(1)} %get-tuple-element.36), channel_id=1, source_target_pairs={{0,8},{8,16},{16,24},{24,0},{1,9},{9,17},{17,25},{25,1},{2,10},{10... | collective-permute-start | bytes 589832 | tf_op jit(solution)/shard_map/ppermute | solution.py:253
  123.8 7.4 %collective-permute-start.13 = (bf16[768,128]{1,0:T(8,128)(2,1)S(1)}, bf16[768,128]{1,0:T(8,128)(2,1)S(1)}, u32[]{:S(2)}, u32[]{:S(2)}) collective-permute-start(bf16[768,128]{1,0:T(8,128)(2,1)S(1)} %get-tuple-element.37), channel_id=1, source_target_pairs={{0,16},{8,24},{16,0},{24,8},{1,17},{9,25},{17,1},{25,9},{2,18},{10... | collective-permute-start | bytes 589832 | tf_op jit(solution)/shard_map/ppermute | solution.py:253
  126.6 6.6 %collective-permute-start.14 = (bf16[768,128]{1,0:T(8,128)(2,1)S(1)}, bf16[768,128]{1,0:T(8,128)(2,1)S(1)}, u32[]{:S(2)}, u32[]{:S(2)}) collective-permute-start(bf16[768,128]{1,0:T(8,128)(2,1)S(1)} %get-tuple-element.38), channel_id=1, source_target_pairs={{0,24},{8,0},{16,8},{24,16},{1,25},{9,1},{17,9},{25,17},{2,26},{10... | collective-permute-start | bytes 589832 | tf_op jit(solution)/shard_map/ppermute | solution.py:253

commit v6 on v5

--- a/solution.py
+++ b/solution.py
@@ -167,17 +167,16 @@
         store_payload(out, slot, dot(scaled, weights), high, low)
 
 
-def enter_second_body(stream, d0, d1, d2, d3, w0, w1, w2, w3, out):
-    x = lax.axis_index("x")
+def enter_second_body(s0, s1, s2, s3, d0, d1, d2, d3, w0, w1, w2, w3, out):
     scaled = []
-    squares = jnp.zeros((N, 1), F32)
-    for k, d in enumerate((d0, d1, d2, d3)):
-        index = lax.rem(x + NX - k, NX)
-        s = stream[pl.ds(index * NY, NY)].reshape(N, N)
-        squares = squares + jnp.sum(s * s, axis=1, keepdims=True)
+    squares = jnp.zeros((N, N), F32)
+    for stream, d in ((s0, d0), (s1, d1), (s2, d2), (s3, d3)):
+        s = stream[...]
+        squares = squares + s * s
         tail = d[HALF:PAD, :].astype(F32)
         gain = tail[0:1] + tail[1:2] + tail[2:3]
         scaled.append((s * gain).astype(BF))
+    squares = jnp.sum(squares, axis=1, keepdims=True)
     scaled = jnp.concatenate(scaled, axis=1)
     high, low = high_low(squares)
     for slot in range(2):
@@ -218,14 +217,7 @@
     return [dot(wide, d[...]).astype(BF) for d in pieces]
 
 
-def leave_first_body(hidden, d0, d1, d2, d3, out):
-    x = lax.axis_index("x")
-    for k, part in enumerate(down_sums(hidden, (d0, d1, d2, d3))):
-        index = lax.rem(x + NX - k, NX)
-        out[pl.ds(index * NY, NY)] = part.reshape(NY, N // NY, N)
-
-
-def leave_second_body(hidden, d0, d1, d2, d3, out):
+def leave_body(hidden, d0, d1, d2, d3, out):
     x = lax.axis_index("x")
     for k, part in enumerate(down_sums(hidden, (d0, d1, d2, d3))):
         index = lax.rem(x + NX - k, NX)
@@ -233,20 +225,9 @@
             out[index * NY + y] = part
 
 
-def stream_body(got, tokens, scale, out):
-    y = lax.axis_index("y")
-    rows = N // NY
+def stream_body(got, old, scale, out):
     branch = jnp.sum(got[...].astype(F32), axis=0) * scale[...]
-    old = tokens[pl.ds(pl.multiple_of(y * rows, rows), rows), :].astype(F32)
-    new = 0.5 * old + 0.5 * branch
-    out[...] = jnp.broadcast_to(new[None], out.shape)
-
-
-def final_body(got, stream, scale, out):
-    x = lax.axis_index("x")
-    branch = jnp.sum(got[...].astype(F32), axis=0) * scale[...]
-    old = stream[pl.ds(x * NY, NY)].reshape(N, N)
-    out[...] = 0.5 * old + 0.5 * branch
+    out[...] = 0.5 * old[...].astype(F32) + 0.5 * branch
 
 
 def shift(v, k):
@@ -322,24 +303,20 @@
     )
     hidden = call(hidden_body, spread, 3)(got, by_chunk(first_gate_scale), by_chunk(first_up_scale))
     hidden = swap(hidden, "z")
-    part = call(leave_first_body, shape(NX * NY, N // NY, N), 5)(
-        hidden, *downs
-    )
+    part = call(leave_body, shape(NX * NY, N, N), 5)(hidden, *downs)
     got = swap(part, XY)
-    stream = call(stream_body, shape(NX * NY, N // NY, N, dtype=F32), 3)(
-        got, tokens, first_down_scale[None]
-    )
-    stream = swap(stream, XY)
-
-    sums = call(enter_second_body, payload, 9)(stream, *downs, *ups)
+    stream = call(stream_body, shape(N, N, dtype=F32), 3)(got, tokens, first_down_scale[None])
+    streams = around([stream] * NX)
+
+    sums = call(enter_second_body, payload, 12)(*streams, *downs, *ups)
     got = swap(sums, "z")
     hidden = call(hidden_body, spread, 3)(
         got, by_chunk(second_gate_scale), by_chunk(second_up_scale)
     )
     hidden = swap(hidden, "z")
-    part = call(leave_second_body, shape(NX * NY, N, N), 5)(hidden, *last_downs)
+    part = call(leave_body, shape(NX * NY, N, N), 5)(hidden, *last_downs)
     got = swap(part, XY)
-    return call(final_body, shape(N, N, dtype=F32), 3)(got, stream, second_down_scale[None])
+    return call(stream_body, shape(N, N, dtype=F32), 3)(got, stream, second_down_scale[None])
 
 
 def solution(mesh):

time: 151 us -> 159 us (1.053)
  starting transfers between devices: 44.9 us -> 62.6 us
  blocking collectives: 33 us -> 16.8 us
  waiting for transfers between devices: 56.2 us -> 63 us
    all_to_all x2 -> x1, blocking collectives: 33 us -> 16.8 us  [swap(): return lax.all_to_all(v, axis, 0, 0, tiled=True)]
    ppermute x12 -> x15, starting transfers between devices: 17.1 us -> 33.3 us  [shift(): return lax.ppermute(v, 'x', [(i, (i + k) % NX) for i in range(NX)])]
    ppermute x12 -> x15, waiting for transfers between devices: 19.8 us -> 31.2 us  [shift(): return lax.ppermute(v, 'x', [(i, (i + k) % NX) for i in range(NX)])]
    all_to_all x5, waiting for transfers between devices: 34.9 us -> 30.2 us  [swap(): return lax.all_to_all(v, axis, 0, 0, tiled=True)]
  transfers between devices with their start and end apart: 20 -> 23, of which waited for: 12 -> 16; matrix products, arithmetic and copies ran while one was open for 0% -> 0% of each run, Pallas kernels for 5% -> 4%
where the time goes in v6:
time: 159 us; the launch traced here: 157 us
  waiting for transfers between devices  63 us (40%)
  starting transfers between devices  62.6 us (39%)
  blocking collectives  16.8 us (11%)
  Pallas kernels  14.2 us (9%)
    ppermute x15, starting transfers between devices, shift(): return lax.ppermute(v, 'x', [(i, (i + k) % NX) for i in range(NX)])  33.3 us
    ppermute x15, waiting for transfers between devices, shift(): return lax.ppermute(v, 'x', [(i, (i + k) % NX) for i in range(NX)])  31.2 us
    all_to_all x5, waiting for transfers between devices, swap(): return lax.all_to_all(v, axis, 0, 0, tiled=True)  30.2 us
    all_to_all x5, starting transfers between devices, swap(): return lax.all_to_all(v, axis, 0, 0, tiled=True)  29.2 us
    all_to_all x1, blocking collectives, swap(): return lax.all_to_all(v, axis, 0, 0, tiled=True)  16.8 us
    pallas_call x12, Pallas kernels, run(): return kernel(*there, *args[far:])  14.2 us
  transfers between devices with their start and end apart: 23, of which 16 were waited for; matrix products, arithmetic and copies ran while one was open for 0% of the time, Pallas kernels for 4%

profile of v6, /device:TPU:2, one launch (start us, length us, event | category | flops | bytes accessed | tf_op | source)
XLA Modules:
  0.0 156.9 jit_solution(4071641952535835425)
XLA Ops:
  0.0 2.1 %shard_map.145 = (bf16[128,896]{1,0:T(8,128)(2,1)S(1)}, bf16[128,896]{1,0:T(8,128)(2,1)S(1)}, bf16[128,896]{1,0:T(8,128)(2,1)S(1)}, bf16[128,896]{1,0:T(8,128)(2,1)S(1)}, bf16[128,768]{1,0:T(8,128)(2,1)S(1)}) custom-call(f32[128,2816]{1,0:T(8,128)} %gate.2, f32[128,2816]{1,0:T(8,128)} %up.2, bf16[128,128]{1,0:T(8,128)(2,1)} %old.1, f32[1,128]{1,0:T(1,128)} %bitcast.8), custom_call_target="tpu_custom_call" | custom-call | tf_op jit(solution)/shard_map/pallas_call | solution.py:44
  2.2 1.6 collective-permute-start
  3.7 2.8 %collective-permute-start.1 = (bf16[128,896]{1,0:T(8,128)(2,1)S(1)}, bf16[128,896]{1,0:T(8,128)(2,1)S(1)}, u32[]{:S(2)}, u32[]{:S(2)}) collective-permute-start(bf16[128,896]{1,0:T(8,128)(2,1)S(1)} %get-tuple-element.24), channel_id=1, source_target_pairs={{0,16},{8,24},{16,0},{24,8},{1,17},{9,25},{17,1},{25,9},{2,18},{10... | collective-permute-start | bytes 688136 | tf_op jit(solution)/shard_map/ppermute | solution.py:234
  6.5 0.4 collective-permute-start.2
  7.0 3.9 %collective-permute-done.r1 = bf16[128,896]{1,0:T(8,128)(2,1)S(1)} collective-permute-done((bf16[128,896]{1,0:T(8,128)(2,1)S(1)}, bf16[128,896]{1,0:T(8,128)(2,1)S(1)}, u32[]{:S(2)}, u32[]{:S(2)}) %collective-permute-start) | collective-permute-done | bytes 229408 | tf_op jit(solution)/shard_map/ppermute | solution.py:234
  10.9 2.8 %collective-permute-done.1.r2 = bf16[128,896]{1,0:T(8,128)(2,1)S(1)} collective-permute-done((bf16[128,896]{1,0:T(8,128)(2,1)S(1)}, bf16[128,896]{1,0:T(8,128)(2,1)S(1)}, u32[]{:S(2)}, u32[]{:S(2)}) %collective-permute-start.1) | collective-permute-done | bytes 229408 | tf_op jit(solution)/shard_map/ppermute | solution.py:234
  13.7 2.7 %collective-permute-done.2.r3 = bf16[128,896]{1,0:T(8,128)(2,1)S(1)} collective-permute-done((bf16[128,896]{1,0:T(8,128)(2,1)S(1)}, bf16[128,896]{1,0:T(8,128)(2,1)S(1)}, u32[]{:S(2)}, u32[]{:S(2)}) %collective-permute-start.2) | collective-permute-done | bytes 229408 | tf_op jit(solution)/shard_map/ppermute | solution.py:234
  16.5 1.5 collective-permute-done.5.s3
  17.9 1.1 shard_map.146
  19.1 8.7 %all-to-all-start = ((bf16[8,2,16,768]{3,2,1,0:T(8,128)(2,1)}), bf16[8,2,16,768]{3,2,1,0:T(8,128)(2,1)S(1)}, u32[]{:S(2)}, u32[]{:S(2)}) async-start(bf16[8,2,16,768]{3,2,1,0:T(8,128)(2,1)} %shard_map.146), calls=%async_computation | async-start | bytes 786432 | tf_op jit(solution)/shard_map/all_to_all | solution.py:246
  27.9 14.8 %all-to-all-done.got = bf16[8,2,16,768]{3,2,1,0:T(8,128)(2,1)S(1)} async-done(((bf16[8,2,16,768]{3,2,1,0:T(8,128)(2,1)}), bf16[8,2,16,768]{3,2,1,0:T(8,128)(2,1)S(1)}, u32[]{:S(2)}, u32[]{:S(2)}) %all-to-all-start) | async-done | bytes 393248 | tf_op jit(solution)/shard_map/all_to_all | solution.py:246
  42.8 0.8 shard_map.147
  43.6 3.4 %all-to-all-start.1 = ((bf16[8,2,16,384]{3,2,1,0:T(8,128)(2,1)}), bf16[8,2,16,384]{3,2,1,0:T(8,128)(2,1)S(1)}, u32[]{:S(2)}, u32[]{:S(2)}) async-start(bf16[8,2,16,384]{3,2,1,0:T(8,128)(2,1)} %shard_map.147), calls=%async_computation.1 | async-start | bytes 393216 | tf_op jit(solution)/shard_map/all_to_all | solution.py:246
  47.0 1.4 shard_map.148
  48.4 1.4 collective-permute-start.6
  49.8 1.8 %collective-permute-start.7 = (bf16[768,128]{1,0:T(8,128)(2,1)S(1)}, bf16[768,128]{1,0:T(8,128)(2,1)S(1)}, u32[]{:S(2)}, u32[]{:S(2)}) collective-permute-start(bf16[768,128]{1,0:T(8,128)(2,1)S(1)} %get-tuple-element.29), channel_id=1, source_target_pairs={{0,16},{8,24},{16,0},{24,8},{1,17},{9,25},{17,1},{25,9},{2,18},{10... | collective-permute-start | bytes 589832 | tf_op jit(solution)/shard_map/ppermute | solution.py:234
  51.6 1.3 collective-permute-start.8
  52.9 3.4 %collective-permute-done.6.d1 = bf16[768,128]{1,0:T(8,128)(2,1)S(1)} collective-permute-done((bf16[768,128]{1,0:T(8,128)(2,1)S(1)}, bf16[768,128]{1,0:T(8,128)(2,1)S(1)}, u32[]{:S(2)}, u32[]{:S(2)}) %collective-permute-start.6) | collective-permute-done | bytes 196640 | tf_op jit(solution)/shard_map/ppermute | solution.py:234
  56.3 2.8 %collective-permute-done.7.d2 = bf16[768,128]{1,0:T(8,128)(2,1)S(1)} collective-permute-done((bf16[768,128]{1,0:T(8,128)(2,1)S(1)}, bf16[768,128]{1,0:T(8,128)(2,1)S(1)}, u32[]{:S(2)}, u32[]{:S(2)}) %collective-permute-start.7) | collective-permute-done | bytes 196640 | tf_op jit(solution)/shard_map/ppermute | solution.py:234
  59.1 2.9 %collective-permute-done.8.d3 = bf16[768,128]{1,0:T(8,128)(2,1)S(1)} collective-permute-done((bf16[768,128]{1,0:T(8,128)(2,1)S(1)}, bf16[768,128]{1,0:T(8,128)(2,1)S(1)}, u32[]{:S(2)}, u32[]{:S(2)}) %collective-permute-start.8) | collective-permute-done | bytes 196640 | tf_op jit(solution)/shard_map/ppermute | solution.py:234
  62.0 1.1 shard_map.149
  63.2 6.9 %all-to-all-start.2 = ((bf16[16,128,128]{2,1,0:T(8,128)(2,1)}), bf16[16,128,128]{2,1,0:T(8,128)(2,1)S(1)}, u32[]{:S(2)}, u32[]{:S(2)}) async-start(bf16[16,128,128]{2,1,0:T(8,128)(2,1)} %shard_map.149), calls=%async_computation.2 | async-start | bytes 1048576 | tf_op jit(solution)/shard_map/all_to_all | solution.py:246
  70.1 3.0 %shard_map.151 = (bf16[128,1536]{1,0:T(8,128)(2,1)S(1)}, bf16[128,1536]{1,0:T(8,128)(2,1)}, bf16[128,1536]{1,0:T(8,128)(2,1)}, bf16[128,1536]{1,0:T(8,128)(2,1)S(1)}) custom-call(f32[128,2816]{1,0:T(8,128)} %gate.3, f32[128,2816]{1,0:T(8,128)} %up.3), custom_call_target="tpu_custom_call" | custom-call | tf_op jit(solution)/shard_map/pallas_call | solution.py:44
  73.1 1.5 collective-permute-start.12
  74.7 0.7 collective-permute-start.13
  75.4 2.5 %collective-permute-start.14 = (bf16[128,1536]{1,0:T(8,128)(2,1)S(1)}, bf16[128,1536]{1,0:T(8,128)(2,1)S(1)}, u32[]{:S(2)}, u32[]{:S(2)}) collective-permute-start(bf16[128,1536]{1,0:T(8,128)(2,1)S(1)} %get-tuple-element.34), channel_id=1, source_target_pairs={{0,24},{8,0},{16,8},{24,16},{1,25},{9,1},{17,9},{25,17},{2,26},{10... | collective-permute-start | bytes 1179656 | tf_op jit(solution)/shard_map/ppermute | solution.py:234
  77.9 2.6 %all-to-all-done.2.got = bf16[16,128,128]{2,1,0:T(8,128)(2,1)S(1)} async-done(((bf16[16,128,128]{2,1,0:T(8,128)(2,1)}), bf16[16,128,128]{2,1,0:T(8,128)(2,1)S(1)}, u32[]{:S(2)}, u32[]{:S(2)}) %all-to-all-start.2) | async-done | bytes 524320 | tf_op jit(solution)/shard_map/all_to_all | solution.py:246
  80.6 2.4 %collective-permute-start.10 = (f32[128,128]{1,0:T(8,128)S(1)}, f32[128,128]{1,0:T(8,128)S(1)}, u32[]{:S(2)}, u32[]{:S(2)}) collective-permute-start(f32[128,128]{1,0:T(8,128)S(1)} %shard_map.150.s0.old), channel_id=1, source_target_pairs={{0,16},{8,24},{16,0},{24,8},{1,17},{9,25},{17,1},{25,9},{2,18},{10... | collective-permute-start | bytes 196616 | tf_op jit(solution)/shard_map/ppermute | solution.py:234
  83.0 0.6 collective-permute-start.11
  83.5 2.4 %collective-permute-done.12.w1 = bf16[128,1536]{1,0:T(8,128)(2,1)S(1)} collective-permute-done((bf16[128,1536]{1,0:T(8,128)(2,1)}, bf16[128,1536]{1,0:T(8,128)(2,1)S(1)}, u32[]{:S(2)}, u32[]{:S(2)}) %collective-permute-start.12) | collective-permute-done | bytes 393248 | tf_op jit(solution)/shard_map/ppermute | solution.py:234
  85.9 10.2 %collective-permute-start.9 = (f32[128,128]{1,0:T(8,128)S(1)}, f32[128,128]{1,0:T(8,128)S(1)}, u32[]{:S(2)}, u32[]{:S(2)}) collective-permute-start(f32[128,128]{1,0:T(8,128)S(1)} %shard_map.150.s0.old), channel_id=1, source_target_pairs={{0,8},{8,16},{16,24},{24,0},{1,9},{9,17},{17,25},{25,1},{2,10},{10... | collective-permute-start | bytes 196616 | tf_op jit(solution)/shard_map/ppermute | solution.py:234
  96.2 1.2 collective-permute-done.10.s2
  97.4 0.7 collective-permute-done.9.s1
  98.1 1.1 shard_map.152
  99.2 6.8 %all-to-all-start.3 = ((bf16[8,2,16,768]{3,2,1,0:T(8,128)(2,1)}), bf16[8,2,16,768]{3,2,1,0:T(8,128)(2,1)S(1)}, u32[]{:S(2)}, u32[]{:S(2)}) async-start(bf16[8,2,16,768]{3,2,1,0:T(8,128)(2,1)} %shard_map.152), calls=%async_computation.3 | async-start | bytes 786432 | tf_op jit(solution)/shard_map/all_to_all | solution.py:246
  106.2 12.8 %all-to-all-done.3.got = bf16[8,2,16,768]{3,2,1,0:T(8,128)(2,1)S(1)} async-done(((bf16[8,2,16,768]{3,2,1,0:T(8,128)(2,1)}), bf16[8,2,16,768]{3,2,1,0:T(8,128)(2,1)S(1)}, u32[]{:S(2)}, u32[]{:S(2)}) %all-to-all-start.3) | async-done | bytes 393248 | tf_op jit(solution)/shard_map/all_to_all | solution.py:246
  119.0 0.8 shard_map.153
  119.8 3.4 %all-to-all-start.4 = ((bf16[8,2,16,384]{3,2,1,0:T(8,128)(2,1)}), bf16[8,2,16,384]{3,2,1,0:T(8,128)(2,1)S(1)}, u32[]{:S(2)}, u32[]{:S(2)}) async-start(bf16[8,2,16,384]{3,2,1,0:T(8,128)(2,1)} %shard_map.153), calls=%async_computation.4 | async-start | bytes 393216 | tf_op jit(solution)/shard_map/all_to_all | solution.py:246
  123.2 1.4 shard_map.154
  124.6 1.3 collective-permute-start.15
  126.0 4.1 %collective-permute-start.16 = (bf16[768,128]{1,0:T(8,128)(2,1)S(1)}, bf16[768,128]{1,0:T(8,128)(2,1)S(1)}, u32[]{:S(2)}, u32[]{:S(2)}) collective-permute-start(bf16[768,128]{1,0:T(8,128)(2,1)S(1)} %get-tuple-element.37), channel_id=1, source_target_pairs={{0,16},{8,24},{16,0},{24,8},{1,17},{9,25},{17,1},{25,9},{2,18},{10... | collective-permute-start | bytes 589832 | tf_op jit(solution)/shard_map/ppermute | solution.py:234
  130.1 0.5 collective-permute-start.17
  130.6 3.2 %collective-permute-done.15.d1 = bf16[768,128]{1,0:T(8,128)(2,1)S(1)} collective-permute-done((bf16[768,128]{1,0:T(8,128)(2,1)S(1)}, bf16[768,128]{1,0:T(8,128)(2,1)S(1)}, u32[]{:S(2)}, u32[]{:S(2)}) %collective-permute-start.15) | collective-permute-done | bytes 196640 | tf_op jit(solution)/shard_map/ppermute | solution.py:234
  133.8 2.1 %collective-permute-done.16.d2 = bf16[768,128]{1,0:T(8,128)(2,1)S(1)} collective-permute-done((bf16[768,128]{1,0:T(8,128)(2,1)S(1)}, bf16[768,128]{1,0:T(8,128)(2,1)S(1)}, u32[]{:S(2)}, u32[]{:S(2)}) %collective-permute-start.16) | collective-permute-done | bytes 196640 | tf_op jit(solution)/shard_map/ppermute | solution.py:234
  135.9 3.2 %collective-permute-done.17.d3 = bf16[768,128]{1,0:T(8,128)(2,1)S(1)} collective-permute-done((bf16[768,128]{1,0:T(8,128)(2,1)S(1)}, bf16[768,128]{1,0:T(8,128)(2,1)S(1)}, u32[]{:S(2)}, u32[]{:S(2)}) %collective-permute-start.17) | collective-permute-done | bytes 196640 | tf_op jit(solution)/shard_map/ppermute | solution.py:234
  139.0 0.4 shard_map.155
  139.4 16.8 %all_to_all.30.got = bf16[16,128,128]{2,1,0:T(8,128)(2,1)S(1)} all-to-all(bf16[16,128,128]{2,1,0:T(8,128)(2,1)S(1)} %shard_map.155), channel_id=1, replica_groups=mesh['z'=8,'x'=4,'y'=4,'c'=2] {'x','y'}, dimensions={0} | all-to-all | bytes 1048576 | tf_op jit(solution)/shard_map/all_to_all | solution.py:246
  156.2 0.7 shard_map.156
  (31 shorter events, 0.4 us)
Async XLA Ops:
  2.2 8.8 %collective-permute-start = (bf16[128,896]{1,0:T(8,128)(2,1)S(1)}, bf16[128,896]{1,0:T(8,128)(2,1)S(1)}, u32[]{:S(2)}, u32[]{:S(2)}) collective-permute-start(bf16[128,896]{1,0:T(8,128)(2,1)S(1)} %get-tuple-element.23), channel_id=1, source_target_pairs={{0,8},{8,16},{16,24},{24,0},{1,9},{9,17},{17,25},{25,1},{2,10},{10... | collective-permute-start | bytes 688136 | tf_op jit(solution)/shard_map/ppermute | solution.py:234
  3.7 10.0 %collective-permute-start.1 = (bf16[128,896]{1,0:T(8,128)(2,1)S(1)}, bf16[128,896]{1,0:T(8,128)(2,1)S(1)}, u32[]{:S(2)}, u32[]{:S(2)}) collective-permute-start(bf16[128,896]{1,0:T(8,128)(2,1)S(1)} %get-tuple-element.24), channel_id=1, source_target_pairs={{0,16},{8,24},{16,0},{24,8},{1,17},{9,25},{17,1},{25,9},{2,18},{10... | collective-permute-start | bytes 688136 | tf_op jit(solution)/shard_map/ppermute | solution.py:234
  6.5 9.9 %collective-permute-start.2 = (bf16[128,896]{1,0:T(8,128)(2,1)S(1)}, bf16[128,896]{1,0:T(8,128)(2,1)S(1)}, u32[]{:S(2)}, u32[]{:S(2)}) collective-permute-start(bf16[128,896]{1,0:T(8,128)(2,1)S(1)} %get-tuple-element.25), channel_id=1, source_target_pairs={{0,24},{8,0},{16,8},{24,16},{1,25},{9,1},{17,9},{25,17},{2,26},{10... | collective-permute-start | bytes 688136 | tf_op jit(solution)/shard_map/ppermute | solution.py:234
  10.9 5.5 %collective-permute-start.3 = (bf16[128,896]{1,0:T(8,128)(2,1)S(1)}, bf16[128,896]{1,0:T(8,128)(2,1)S(1)}, u32[]{:S(2)}, u32[]{:S(2)}) collective-permute-start(bf16[128,896]{1,0:T(8,128)(2,1)S(1)} %collective-permute-done.r1), channel_id=1, source_target_pairs={{0,1},{1,0},{2,3},{3,2},{4,5},{5,4},{6,7},{7,6},{8,9},{9,8},{10,11... | collective-permute-start | bytes 688136 | tf_op jit(solution)/shard_map/ppermute | solution.py:238
  13.7 2.7 %collective-permute-start.4 = (bf16[128,896]{1,0:T(8,128)(2,1)S(1)}, bf16[128,896]{1,0:T(8,128)(2,1)S(1)}, u32[]{:S(2)}, u32[]{:S(2)}) collective-permute-start(bf16[128,896]{1,0:T(8,128)(2,1)S(1)} %collective-permute-done.1.r2), channel_id=1, source_target_pairs={{0,1},{1,0},{2,3},{3,2},{4,5},{5,4},{6,7},{7,6},{8,9},{9,8},{10,11... | collective-permute-start | bytes 688136 | tf_op jit(solution)/shard_map/ppermute | solution.py:238
  16.4 1.5 collective-permute-start.5
  17.9 9.8 %copy-start.4 = (f32[2816]{0:T(1024)S(1)}, f32[2816]{0:T(1024)}, u32[]{:S(2)}) copy-start(f32[2816]{0:T(1024)} %param.18) | copy-start | bytes 33796
  17.9 9.9 %copy-start.5 = (f32[2816]{0:T(1024)S(1)}, f32[2816]{0:T(1024)}, u32[]{:S(2)}) copy-start(f32[2816]{0:T(1024)} %param.20) | copy-start | bytes 33796
  19.1 27.9 %copy-start.1 = (f32[128]{0:T(128)S(1)}, f32[128]{0:T(128)}, u32[]{:S(2)}) copy-start(f32[128]{0:T(128)} %param.23) | copy-start | bytes 1540
  19.1 23.7 %all-to-all-start = ((bf16[8,2,16,768]{3,2,1,0:T(8,128)(2,1)}), bf16[8,2,16,768]{3,2,1,0:T(8,128)(2,1)S(1)}, u32[]{:S(2)}, u32[]{:S(2)}) async-start(bf16[8,2,16,768]{3,2,1,0:T(8,128)(2,1)} %shard_map.146), calls=%async_computation | async-start | bytes 786432 | tf_op jit(solution)/shard_map/all_to_all | solution.py:246
  43.6 18.5 %all-to-all-start.1 = ((bf16[8,2,16,384]{3,2,1,0:T(8,128)(2,1)}), bf16[8,2,16,384]{3,2,1,0:T(8,128)(2,1)S(1)}, u32[]{:S(2)}, u32[]{:S(2)}) async-start(bf16[8,2,16,384]{3,2,1,0:T(8,128)(2,1)} %shard_map.147), calls=%async_computation.1 | async-start | bytes 393216 | tf_op jit(solution)/shard_map/all_to_all | solution.py:246
  48.4 7.8 %collective-permute-start.6 = (bf16[768,128]{1,0:T(8,128)(2,1)S(1)}, bf16[768,128]{1,0:T(8,128)(2,1)S(1)}, u32[]{:S(2)}, u32[]{:S(2)}) collective-permute-start(bf16[768,128]{1,0:T(8,128)(2,1)S(1)} %get-tuple-element.28), channel_id=1, source_target_pairs={{0,8},{8,16},{16,24},{24,0},{1,9},{9,17},{17,25},{25,1},{2,10},{10... | collective-permute-start | bytes 589832 | tf_op jit(solution)/shard_map/ppermute | solution.py:234
  49.8 9.3 %collective-permute-start.7 = (bf16[768,128]{1,0:T(8,128)(2,1)S(1)}, bf16[768,128]{1,0:T(8,128)(2,1)S(1)}, u32[]{:S(2)}, u32[]{:S(2)}) collective-permute-start(bf16[768,128]{1,0:T(8,128)(2,1)S(1)} %get-tuple-element.29), channel_id=1, source_target_pairs={{0,16},{8,24},{16,0},{24,8},{1,17},{9,25},{17,1},{25,9},{2,18},{10... | collective-permute-start | bytes 589832 | tf_op jit(solution)/shard_map/ppermute | solution.py:234
  51.6 10.4 %collective-permute-start.8 = (bf16[768,128]{1,0:T(8,128)(2,1)S(1)}, bf16[768,128]{1,0:T(8,128)(2,1)S(1)}, u32[]{:S(2)}, u32[]{:S(2)}) collective-permute-start(bf16[768,128]{1,0:T(8,128)(2,1)S(1)} %get-tuple-element.30), channel_id=1, source_target_pairs={{0,24},{8,0},{16,8},{24,16},{1,25},{9,1},{17,9},{25,17},{2,26},{10... | collective-permute-start | bytes 589832 | tf_op jit(solution)/shard_map/ppermute | solution.py:234
  63.2 17.3 %all-to-all-start.2 = ((bf16[16,128,128]{2,1,0:T(8,128)(2,1)}), bf16[16,128,128]{2,1,0:T(8,128)(2,1)S(1)}, u32[]{:S(2)}, u32[]{:S(2)}) async-start(bf16[16,128,128]{2,1,0:T(8,128)(2,1)} %shard_map.149), calls=%async_computation.2 | async-start | bytes 1048576 | tf_op jit(solution)/shard_map/all_to_all | solution.py:246
  70.1 10.4 %copy-start = (bf16[128,128]{1,0:T(8,128)(2,1)S(1)}, bf16[128,128]{1,0:T(8,128)(2,1)}, u32[]{:S(2)}) copy-start(bf16[128,128]{1,0:T(8,128)(2,1)} %old.1) | copy-start | bytes 98308
  70.1 10.4 %copy-start.2 = (f32[128]{0:T(128)S(1)}, f32[128]{0:T(128)}, u32[]{:S(2)}) copy-start(f32[128]{0:T(128)} %param.22) | copy-start | bytes 1540
  73.1 12.8 %collective-permute-start.12 = (bf16[128,1536]{1,0:T(8,128)(2,1)}, bf16[128,1536]{1,0:T(8,128)(2,1)S(1)}, u32[]{:S(2)}, u32[]{:S(2)}) collective-permute-start(bf16[128,1536]{1,0:T(8,128)(2,1)} %get-tuple-element.32), channel_id=1, source_target_pairs={{0,8},{8,16},{16,24},{24,0},{1,9},{9,17},{17,25},{25,1},{2,10},{10... | collective-permute-start | bytes 1179656 | tf_op jit(solution)/shard_map/ppermute | solution.py:234
  74.7 21.5 %collective-permute-start.13 = (bf16[128,1536]{1,0:T(8,128)(2,1)}, bf16[128,1536]{1,0:T(8,128)(2,1)S(1)}, u32[]{:S(2)}, u32[]{:S(2)}) collective-permute-start(bf16[128,1536]{1,0:T(8,128)(2,1)} %get-tuple-element.33), channel_id=1, source_target_pairs={{0,16},{8,24},{16,0},{24,8},{1,17},{9,25},{17,1},{25,9},{2,18},{10... | collective-permute-start | bytes 1179656 | tf_op jit(solution)/shard_map/ppermute | solution.py:234
  75.4 20.8 %collective-permute-start.14 = (bf16[128,1536]{1,0:T(8,128)(2,1)S(1)}, bf16[128,1536]{1,0:T(8,128)(2,1)S(1)}, u32[]{:S(2)}, u32[]{:S(2)}) collective-permute-start(bf16[128,1536]{1,0:T(8,128)(2,1)S(1)} %get-tuple-element.34), channel_id=1, source_target_pairs={{0,24},{8,0},{16,8},{24,16},{1,25},{9,1},{17,9},{25,17},{2,26},{10... | collective-permute-start | bytes 1179656 | tf_op jit(solution)/shard_map/ppermute | solution.py:234
  80.6 16.8 %collective-permute-start.10 = (f32[128,128]{1,0:T(8,128)S(1)}, f32[128,128]{1,0:T(8,128)S(1)}, u32[]{:S(2)}, u32[]{:S(2)}) collective-permute-start(f32[128,128]{1,0:T(8,128)S(1)} %shard_map.150.s0.old), channel_id=1, source_target_pairs={{0,16},{8,24},{16,0},{24,8},{1,17},{9,25},{17,1},{25,9},{2,18},{10... | collective-permute-start | bytes 196616 | tf_op jit(solution)/shard_map/ppermute | solution.py:234
  83.0 14.4 %collective-permute-start.11 = (f32[128,128]{1,0:T(8,128)S(1)}, f32[128,128]{1,0:T(8,128)S(1)}, u32[]{:S(2)}, u32[]{:S(2)}) collective-permute-start(f32[128,128]{1,0:T(8,128)S(1)} %shard_map.150.s0.old), channel_id=1, source_target_pairs={{0,24},{8,0},{16,8},{24,16},{1,25},{9,1},{17,9},{25,17},{2,26},{10... | collective-permute-start | bytes 196616 | tf_op jit(solution)/shard_map/ppermute | solution.py:234
  85.9 12.2 %collective-permute-start.9 = (f32[128,128]{1,0:T(8,128)S(1)}, f32[128,128]{1,0:T(8,128)S(1)}, u32[]{:S(2)}, u32[]{:S(2)}) collective-permute-start(f32[128,128]{1,0:T(8,128)S(1)} %shard_map.150.s0.old), channel_id=1, source_target_pairs={{0,8},{8,16},{16,24},{24,0},{1,9},{9,17},{17,25},{25,1},{2,10},{10... | collective-permute-start | bytes 196616 | tf_op jit(solution)/shard_map/ppermute | solution.py:234
  98.1 8.0 %copy-start.6 = (f32[2816]{0:T(1024)S(1)}, f32[2816]{0:T(1024)}, u32[]{:S(2)}) copy-start(f32[2816]{0:T(1024)} %param.25) | copy-start | bytes 33796
  98.1 8.0 %copy-start.7 = (f32[2816]{0:T(1024)S(1)}, f32[2816]{0:T(1024)}, u32[]{:S(2)}) copy-start(f32[2816]{0:T(1024)} %param.27) | copy-start | bytes 33796
  99.2 19.8 %all-to-all-start.3 = ((bf16[8,2,16,768]{3,2,1,0:T(8,128)(2,1)}), bf16[8,2,16,768]{3,2,1,0:T(8,128)(2,1)S(1)}, u32[]{:S(2)}, u32[]{:S(2)}) async-start(bf16[8,2,16,768]{3,2,1,0:T(8,128)(2,1)} %shard_map.152), calls=%async_computation.3 | async-start | bytes 786432 | tf_op jit(solution)/shard_map/all_to_all | solution.py:246
  119.8 19.2 %all-to-all-start.4 = ((bf16[8,2,16,384]{3,2,1,0:T(8,128)(2,1)}), bf16[8,2,16,384]{3,2,1,0:T(8,128)(2,1)S(1)}, u32[]{:S(2)}, u32[]{:S(2)}) async-start(bf16[8,2,16,384]{3,2,1,0:T(8,128)(2,1)} %shard_map.153), calls=%async_computation.4 | async-start | bytes 393216 | tf_op jit(solution)/shard_map/all_to_all | solution.py:246
  124.6 31.6 %copy-start.3 = (f32[128]{0:T(128)S(1)}, f32[128]{0:T(128)}, u32[]{:S(2)}) copy-start(f32[128]{0:T(128)} %param.29) | copy-start | bytes 1540
  124.6 9.2 %collective-permute-start.15 = (bf16[768,128]{1,0:T(8,128)(2,1)S(1)}, bf16[768,128]{1,0:T(8,128)(2,1)S(1)}, u32[]{:S(2)}, u32[]{:S(2)}) collective-permute-start(bf16[768,128]{1,0:T(8,128)(2,1)S(1)} %get-tuple-element.36), channel_id=1, source_target_pairs={{0,8},{8,16},{16,24},{24,0},{1,9},{9,17},{17,25},{25,1},{2,10},{10... | collective-permute-start | bytes 589832 | tf_op jit(solution)/shard_map/ppermute | solution.py:234
  126.0 9.9 %collective-permute-start.16 = (bf16[768,128]{1,0:T(8,128)(2,1)S(1)}, bf16[768,128]{1,0:T(8,128)(2,1)S(1)}, u32[]{:S(2)}, u32[]{:S(2)}) collective-permute-start(bf16[768,128]{1,0:T(8,128)(2,1)S(1)} %get-tuple-element.37), channel_id=1, source_target_pairs={{0,16},{8,24},{16,0},{24,8},{1,17},{9,25},{17,1},{25,9},{2,18},{10... | collective-permute-start | bytes 589832 | tf_op jit(solution)/shard_map/ppermute | solution.py:234
  130.1 8.9 %collective-permute-start.17 = (bf16[768,128]{1,0:T(8,128)(2,1)S(1)}, bf16[768,128]{1,0:T(8,128)(2,1)S(1)}, u32[]{:S(2)}, u32[]{:S(2)}) collective-permute-start(bf16[768,128]{1,0:T(8,128)(2,1)S(1)} %get-tuple-element.38), channel_id=1, source_target_pairs={{0,24},{8,0},{16,8},{24,16},{1,25},{9,1},{17,9},{25,17},{2,26},{10... | collective-permute-start | bytes 589832 | tf_op jit(solution)/shard_map/ppermute | solution.py:234

commit v7 on v6

--- a/solution.py
+++ b/solution.py
@@ -21,7 +21,7 @@
 
 VMEM = pl.BlockSpec(memory_space=pltpu.VMEM)
 HBM = pl.BlockSpec(memory_space=pltpu.HBM)
-BLOCKS = 4
+BLOCKS = 8
 
 
 def shape(*dims, dtype=BF):
@@ -109,13 +109,12 @@
     other[...] = chunks[2 * x + 1 - c]
 
 
-def pack_second_body(gate, up, p0, p1, p2, p3, chunks, gate_here, up_here, sems):
-    x = lax.axis_index("x")
+def pack_second_body(gate, up, p0, p1, p2, p3, other, chunks, gate_here, up_here, sems):
+    x, c = lax.axis_index("x"), lax.axis_index("c")
     cut_chunks(gate, up, gate_here, up_here, sems, chunks)
     for k, out in enumerate((p0, p1, p2, p3)):
-        index = 2 * lax.rem(x + k, NX)
-        out[:, :WIDE] = chunks[index]
-        out[:, WIDE:] = chunks[index + 1]
+        out[...] = chunks[2 * lax.rem(x + k, NX) + c]
+    other[...] = chunks[2 * x + 1 - c]
 
 
 def pack_down_body(far, gain, p0, p1, p2, p3, down, sems):
@@ -167,21 +166,20 @@
         store_payload(out, slot, dot(scaled, weights), high, low)
 
 
-def enter_second_body(s0, s1, s2, s3, d0, d1, d2, d3, w0, w1, w2, w3, out):
-    scaled = []
+def enter_second_body(
+    s0, s1, s2, s3, d0, d1, d2, d3, r0, r1, r2, r3, q0, q1, q2, q3, out
+):
+    c = lax.axis_index("c")
     squares = jnp.zeros((N, N), F32)
-    for stream, d in ((s0, d0), (s1, d1), (s2, d2), (s3, d3)):
-        s = stream[...]
-        squares = squares + s * s
+    for scaled, d in ((s0, d0), (s1, d1), (s2, d2), (s3, d3)):
         tail = d[HALF:PAD, :].astype(F32)
         gain = tail[0:1] + tail[1:2] + tail[2:3]
-        scaled.append((s * gain).astype(BF))
-    squares = jnp.sum(squares, axis=1, keepdims=True)
-    scaled = jnp.concatenate(scaled, axis=1)
-    high, low = high_low(squares)
-    for slot in range(2):
-        cols = slice(slot * WIDE, (slot + 1) * WIDE)
-        weights = jnp.concatenate([w[:, cols] for w in (w0, w1, w2, w3)], axis=0)
+        s = scaled[...].astype(F32) * (1.0 / gain)
+        squares = squares + s * s
+    high, low = high_low(jnp.sum(squares, axis=1, keepdims=True))
+    scaled = jnp.concatenate([v[...] for v in (s0, s1, s2, s3)], axis=1)
+    for slot, group in ((c, (r0, r1, r2, r3)), (1 - c, (q0, q1, q2, q3))):
+        weights = jnp.concatenate([r[...] for r in group], axis=0)
         store_payload(out, slot, dot(scaled, weights), high, low)
 
 
@@ -225,9 +223,19 @@
             out[index * NY + y] = part
 
 
-def stream_body(got, old, scale, out):
+def new_stream(got, old, scale):
     branch = jnp.sum(got[...].astype(F32), axis=0) * scale[...]
-    out[...] = 0.5 * old[...].astype(F32) + 0.5 * branch
+    return 0.5 * old[...].astype(F32) + 0.5 * branch
+
+
+def stream_body(got, old, scale, gain, out, scaled):
+    new = new_stream(got, old, scale)
+    out[...] = new
+    scaled[...] = (new * gain[...]).astype(BF)
+
+
+def final_body(got, old, scale, out):
+    out[...] = new_stream(got, old, scale)
 
 
 def shift(v, k):
@@ -293,9 +301,11 @@
             first_down, second_gain[None]
         ),
     )
-    ups = around(
-        call(pack_second_body, [shape(N, 2 * WIDE)] * NX, 2, cutting, 2)(second_gate, second_up),
-    )
+    *packed, other = call(
+        pack_second_body, [shape(N, WIDE)] * (NX + 1), 2, cutting, 2
+    )(second_gate, second_up)
+    ups = around(packed)
+    ups = ups + [other] + [other_core(v) for v in ups[1:]]
     last_downs = around(
         call(pack_down_body, [shape(2 * PAD, N)] * NX, 2, lowering, 1)(
             second_down, second_gain[None]
@@ -305,10 +315,13 @@
     hidden = swap(hidden, "z")
     part = call(leave_body, shape(NX * NY, N, N), 5)(hidden, *downs)
     got = swap(part, XY)
-    stream = call(stream_body, shape(N, N, dtype=F32), 3)(got, tokens, first_down_scale[None])
-    streams = around([stream] * NX)
-
-    sums = call(enter_second_body, payload, 12)(*streams, *downs, *ups)
+    block = shape(N, N, dtype=F32)
+    stream, scaled = call(stream_body, [block, shape(N, N)], 4)(
+        got, tokens, first_down_scale[None], second_gain[None]
+    )
+    scaled = around([scaled] * NX)
+
+    sums = call(enter_second_body, payload, 16)(*scaled, *downs, *ups)
     got = swap(sums, "z")
     hidden = call(hidden_body, spread, 3)(
         got, by_chunk(second_gate_scale), by_chunk(second_up_scale)
@@ -316,7 +329,7 @@
     hidden = swap(hidden, "z")
     part = call(leave_body, shape(NX * NY, N, N), 5)(hidden, *last_downs)
     got = swap(part, XY)
-    return call(stream_body, shape(N, N, dtype=F32), 3)(got, stream, second_down_scale[None])
+    return call(final_body, block, 3)(got, stream, second_down_scale[None])
 
 
 def solution(mesh):

time: 159 us -> 151 us (0.950)
  starting transfers between devices: 62.6 us -> 52.2 us
  waiting for transfers between devices: 63 us -> 66.7 us
    ppermute x15, starting transfers between devices: 33.3 us -> 22.9 us  [shift(): return lax.ppermute(v, 'x', [(i, (i + k) % NX) for i in range(NX)])]
    ppermute x15, waiting for transfers between devices: 31.2 us -> 36.9 us  [shift(): return lax.ppermute(v, 'x', [(i, (i + k) % NX) for i in range(NX)])]
    all_to_all x5, waiting for transfers between devices: 30.2 us -> 28.3 us  [swap(): return lax.all_to_all(v, axis, 0, 0, tiled=True)]
  transfers between devices with their start and end apart: 23 -> 26, of which waited for: 16 -> 18; matrix products, arithmetic and copies ran while one was open for 0% -> 0% of each run, Pallas kernels for 4% -> 4%
where the time goes in v7:
time: 151 us; the launch traced here: 149 us
  waiting for transfers between devices  66.7 us (44%)
  starting transfers between devices  52.2 us (35%)
  blocking collectives  15.5 us (10%)
  Pallas kernels  13.9 us (9%)
    ppermute x15, waiting for transfers between devices, shift(): return lax.ppermute(v, 'x', [(i, (i + k) % NX) for i in range(NX)])  36.9 us
    all_to_all x5, starting transfers between devices, swap(): return lax.all_to_all(v, axis, 0, 0, tiled=True)  29.2 us
    all_to_all x5, waiting for transfers between devices, swap(): return lax.all_to_all(v, axis, 0, 0, tiled=True)  28.3 us
    ppermute x15, starting transfers between devices, shift(): return lax.ppermute(v, 'x', [(i, (i + k) % NX) for i in range(NX)])  22.9 us
    all_to_all x1, blocking collectives, swap(): return lax.all_to_all(v, axis, 0, 0, tiled=True)  15.5 us
    pallas_call x12, Pallas kernels, run(): return kernel(*there, *args[far:])  13.9 us
  transfers between devices with their start and end apart: 26, of which 18 were waited for; matrix products, arithmetic and copies ran while one was open for 0% of the time, Pallas kernels for 4%

profile of v7, /device:TPU:2, one launch (start us, length us, event | category | flops | bytes accessed | tf_op | source)
XLA Modules:
  0.0 148.8 jit_solution(2327936024943110221)
XLA Ops:
  0.0 2.3 %shard_map.145 = (bf16[128,896]{1,0:T(8,128)(2,1)S(1)}, bf16[128,896]{1,0:T(8,128)(2,1)S(1)}, bf16[128,896]{1,0:T(8,128)(2,1)S(1)}, bf16[128,896]{1,0:T(8,128)(2,1)S(1)}, bf16[128,768]{1,0:T(8,128)(2,1)S(1)}) custom-call(f32[128,2816]{1,0:T(8,128)} %gate.2, f32[128,2816]{1,0:T(8,128)} %up.2, bf16[128,128]{1,0:T(8,128)(2,1)} %old.1, f32[1,128]{1,0:T(1,128)} %bitcast.9), custom_call_target="tpu_custom_call" | custom-call | tf_op jit(solution)/shard_map/pallas_call | solution.py:44
  2.4 1.6 %collective-permute-start = (bf16[128,896]{1,0:T(8,128)(2,1)S(1)}, bf16[128,896]{1,0:T(8,128)(2,1)S(1)}, u32[]{:S(2)}, u32[]{:S(2)}) collective-permute-start(bf16[128,896]{1,0:T(8,128)(2,1)S(1)} %get-tuple-element.26), channel_id=1, source_target_pairs={{0,8},{8,16},{16,24},{24,0},{1,9},{9,17},{17,25},{25,1},{2,10},{10... | collective-permute-start | bytes 688136 | tf_op jit(solution)/shard_map/ppermute | solution.py:242
  3.9 2.8 %collective-permute-start.1 = (bf16[128,896]{1,0:T(8,128)(2,1)S(1)}, bf16[128,896]{1,0:T(8,128)(2,1)S(1)}, u32[]{:S(2)}, u32[]{:S(2)}) collective-permute-start(bf16[128,896]{1,0:T(8,128)(2,1)S(1)} %get-tuple-element.27), channel_id=1, source_target_pairs={{0,16},{8,24},{16,0},{24,8},{1,17},{9,25},{17,1},{25,9},{2,18},{10... | collective-permute-start | bytes 688136 | tf_op jit(solution)/shard_map/ppermute | solution.py:242
  6.7 0.4 collective-permute-start.2
  7.2 3.9 %collective-permute-done.r1 = bf16[128,896]{1,0:T(8,128)(2,1)S(1)} collective-permute-done((bf16[128,896]{1,0:T(8,128)(2,1)S(1)}, bf16[128,896]{1,0:T(8,128)(2,1)S(1)}, u32[]{:S(2)}, u32[]{:S(2)}) %collective-permute-start) | collective-permute-done | bytes 229408 | tf_op jit(solution)/shard_map/ppermute | solution.py:242
  11.1 2.8 %collective-permute-done.1.r2 = bf16[128,896]{1,0:T(8,128)(2,1)S(1)} collective-permute-done((bf16[128,896]{1,0:T(8,128)(2,1)S(1)}, bf16[128,896]{1,0:T(8,128)(2,1)S(1)}, u32[]{:S(2)}, u32[]{:S(2)}) %collective-permute-start.1) | collective-permute-done | bytes 229408 | tf_op jit(solution)/shard_map/ppermute | solution.py:242
  13.9 2.7 %collective-permute-done.2.r3 = bf16[128,896]{1,0:T(8,128)(2,1)S(1)} collective-permute-done((bf16[128,896]{1,0:T(8,128)(2,1)S(1)}, bf16[128,896]{1,0:T(8,128)(2,1)S(1)}, u32[]{:S(2)}, u32[]{:S(2)}) %collective-permute-start.2) | collective-permute-done | bytes 229408 | tf_op jit(solution)/shard_map/ppermute | solution.py:242
  16.6 1.5 collective-permute-done.5.s3
  18.1 1.1 shard_map.146
  19.3 8.7 %all-to-all-start = ((bf16[8,2,16,768]{3,2,1,0:T(8,128)(2,1)}), bf16[8,2,16,768]{3,2,1,0:T(8,128)(2,1)S(1)}, u32[]{:S(2)}, u32[]{:S(2)}) async-start(bf16[8,2,16,768]{3,2,1,0:T(8,128)(2,1)} %shard_map.146), calls=%async_computation | async-start | bytes 786432 | tf_op jit(solution)/shard_map/all_to_all | solution.py:254
  28.1 14.8 %all-to-all-done.got = bf16[8,2,16,768]{3,2,1,0:T(8,128)(2,1)S(1)} async-done(((bf16[8,2,16,768]{3,2,1,0:T(8,128)(2,1)}), bf16[8,2,16,768]{3,2,1,0:T(8,128)(2,1)S(1)}, u32[]{:S(2)}, u32[]{:S(2)}) %all-to-all-start) | async-done | bytes 393248 | tf_op jit(solution)/shard_map/all_to_all | solution.py:254
  42.9 0.8 shard_map.147
  43.7 3.4 %all-to-all-start.1 = ((bf16[8,2,16,384]{3,2,1,0:T(8,128)(2,1)}), bf16[8,2,16,384]{3,2,1,0:T(8,128)(2,1)S(1)}, u32[]{:S(2)}, u32[]{:S(2)}) async-start(bf16[8,2,16,384]{3,2,1,0:T(8,128)(2,1)} %shard_map.147), calls=%async_computation.1 | async-start | bytes 393216 | tf_op jit(solution)/shard_map/all_to_all | solution.py:254
  47.1 1.6 %shard_map.148 = (bf16[768,128]{1,0:T(8,128)(2,1)S(1)}, bf16[768,128]{1,0:T(8,128)(2,1)S(1)}, bf16[768,128]{1,0:T(8,128)(2,1)S(1)}, bf16[768,128]{1,0:T(8,128)(2,1)S(1)}) custom-call(f32[2816,128]{1,0:T(8,128)} %far.2, f32[1,128]{1,0:T(1,128)S(1)} %bitcast.4), custom_call_target="tpu_custom_call" | custom-call | tf_op jit(solution)/shard_map/pallas_call | solution.py:44
  48.7 1.4 collective-permute-start.6
  50.1 1.8 %collective-permute-start.7 = (bf16[768,128]{1,0:T(8,128)(2,1)S(1)}, bf16[768,128]{1,0:T(8,128)(2,1)S(1)}, u32[]{:S(2)}, u32[]{:S(2)}) collective-permute-start(bf16[768,128]{1,0:T(8,128)(2,1)S(1)} %get-tuple-element.32), channel_id=1, source_target_pairs={{0,16},{8,24},{16,0},{24,8},{1,17},{9,25},{17,1},{25,9},{2,18},{10... | collective-permute-start | bytes 589832 | tf_op jit(solution)/shard_map/ppermute | solution.py:242
  51.9 1.3 collective-permute-start.8
  53.2 3.4 %collective-permute-done.6.d1 = bf16[768,128]{1,0:T(8,128)(2,1)S(1)} collective-permute-done((bf16[768,128]{1,0:T(8,128)(2,1)S(1)}, bf16[768,128]{1,0:T(8,128)(2,1)S(1)}, u32[]{:S(2)}, u32[]{:S(2)}) %collective-permute-start.6) | collective-permute-done | bytes 196640 | tf_op jit(solution)/shard_map/ppermute | solution.py:242
  56.6 2.8 %collective-permute-done.7.d2 = bf16[768,128]{1,0:T(8,128)(2,1)S(1)} collective-permute-done((bf16[768,128]{1,0:T(8,128)(2,1)S(1)}, bf16[768,128]{1,0:T(8,128)(2,1)S(1)}, u32[]{:S(2)}, u32[]{:S(2)}) %collective-permute-start.7) | collective-permute-done | bytes 196640 | tf_op jit(solution)/shard_map/ppermute | solution.py:242
  59.4 2.9 %collective-permute-done.8.d3 = bf16[768,128]{1,0:T(8,128)(2,1)S(1)} collective-permute-done((bf16[768,128]{1,0:T(8,128)(2,1)S(1)}, bf16[768,128]{1,0:T(8,128)(2,1)S(1)}, u32[]{:S(2)}, u32[]{:S(2)}) %collective-permute-start.8) | collective-permute-done | bytes 196640 | tf_op jit(solution)/shard_map/ppermute | solution.py:242
  62.3 1.1 shard_map.149
  63.5 6.9 %all-to-all-start.2 = ((bf16[16,128,128]{2,1,0:T(8,128)(2,1)}), bf16[16,128,128]{2,1,0:T(8,128)(2,1)S(1)}, u32[]{:S(2)}, u32[]{:S(2)}) async-start(bf16[16,128,128]{2,1,0:T(8,128)(2,1)} %shard_map.149), calls=%async_computation.2 | async-start | bytes 1048576 | tf_op jit(solution)/shard_map/all_to_all | solution.py:254
  70.4 2.3 %shard_map.151 = (bf16[128,768]{1,0:T(8,128)(2,1)S(1)}, bf16[128,768]{1,0:T(8,128)(2,1)S(1)}, bf16[128,768]{1,0:T(8,128)(2,1)S(1)}, bf16[128,768]{1,0:T(8,128)(2,1)S(1)}, bf16[128,768]{1,0:T(8,128)(2,1)S(1)}) custom-call(f32[128,2816]{1,0:T(8,128)} %gate.3, f32[128,2816]{1,0:T(8,128)} %up.3), custom_call_target="tpu_custom_call" | custom-call | tf_op jit(solution)/shard_map/pallas_call | solution.py:44
  72.7 1.5 %collective-permute-start.12 = (bf16[128,768]{1,0:T(8,128)(2,1)S(1)}, bf16[128,768]{1,0:T(8,128)(2,1)S(1)}, u32[]{:S(2)}, u32[]{:S(2)}) collective-permute-start(bf16[128,768]{1,0:T(8,128)(2,1)S(1)} %get-tuple-element.36), channel_id=1, source_target_pairs={{0,8},{8,16},{16,24},{24,0},{1,9},{9,17},{17,25},{25,1},{2,10},{10... | collective-permute-start | bytes 589832 | tf_op jit(solution)/shard_map/ppermute | solution.py:242
  74.3 0.7 collective-permute-start.13
  75.0 2.5 %collective-permute-start.14 = (bf16[128,768]{1,0:T(8,128)(2,1)S(1)}, bf16[128,768]{1,0:T(8,128)(2,1)S(1)}, u32[]{:S(2)}, u32[]{:S(2)}) collective-permute-start(bf16[128,768]{1,0:T(8,128)(2,1)S(1)} %get-tuple-element.38), channel_id=1, source_target_pairs={{0,24},{8,0},{16,8},{24,16},{1,25},{9,1},{17,9},{25,17},{2,26},{10... | collective-permute-start | bytes 589832 | tf_op jit(solution)/shard_map/ppermute | solution.py:242
  77.5 4.5 %collective-permute-done.12.r1 = bf16[128,768]{1,0:T(8,128)(2,1)S(1)} collective-permute-done((bf16[128,768]{1,0:T(8,128)(2,1)S(1)}, bf16[128,768]{1,0:T(8,128)(2,1)S(1)}, u32[]{:S(2)}, u32[]{:S(2)}) %collective-permute-start.12) | collective-permute-done | bytes 196640 | tf_op jit(solution)/shard_map/ppermute | solution.py:242
  82.0 1.9 %collective-permute-done.13.r2 = bf16[128,768]{1,0:T(8,128)(2,1)S(1)} collective-permute-done((bf16[128,768]{1,0:T(8,128)(2,1)S(1)}, bf16[128,768]{1,0:T(8,128)(2,1)S(1)}, u32[]{:S(2)}, u32[]{:S(2)}) %collective-permute-start.13) | collective-permute-done | bytes 196640 | tf_op jit(solution)/shard_map/ppermute | solution.py:242
  83.9 2.5 %collective-permute-done.14.r3 = bf16[128,768]{1,0:T(8,128)(2,1)S(1)} collective-permute-done((bf16[128,768]{1,0:T(8,128)(2,1)S(1)}, bf16[128,768]{1,0:T(8,128)(2,1)S(1)}, u32[]{:S(2)}, u32[]{:S(2)}) %collective-permute-start.14) | collective-permute-done | bytes 196640 | tf_op jit(solution)/shard_map/ppermute | solution.py:242
  86.6 1.7 %collective-permute-start.10 = (bf16[128,128]{1,0:T(8,128)(2,1)S(1)}, bf16[128,128]{1,0:T(8,128)(2,1)S(1)}, u32[]{:S(2)}, u32[]{:S(2)}) collective-permute-start(bf16[128,128]{1,0:T(8,128)(2,1)S(1)} %get-tuple-element.34.s0), channel_id=1, source_target_pairs={{0,16},{8,24},{16,0},{24,8},{1,17},{9,25},{17,1},{25,9},{2,18},{10... | collective-permute-start | bytes 98312 | tf_op jit(solution)/shard_map/ppermute | solution.py:242
  88.3 1.7 %collective-permute-start.11 = (bf16[128,128]{1,0:T(8,128)(2,1)S(1)}, bf16[128,128]{1,0:T(8,128)(2,1)S(1)}, u32[]{:S(2)}, u32[]{:S(2)}) collective-permute-start(bf16[128,128]{1,0:T(8,128)(2,1)S(1)} %get-tuple-element.34.s0), channel_id=1, source_target_pairs={{0,24},{8,0},{16,8},{24,16},{1,25},{9,1},{17,9},{25,17},{2,26},{10... | collective-permute-start | bytes 98312 | tf_op jit(solution)/shard_map/ppermute | solution.py:242
  90.1 0.7 collective-permute-start.9
  90.7 1.3 collective-permute-done.10.s2
  92.1 0.6 collective-permute-done.11.s3
  92.6 1.3 collective-permute-done.9.s1
  94.0 1.1 shard_map.152
  95.1 6.8 %all-to-all-start.3 = ((bf16[8,2,16,768]{3,2,1,0:T(8,128)(2,1)}), bf16[8,2,16,768]{3,2,1,0:T(8,128)(2,1)S(1)}, u32[]{:S(2)}, u32[]{:S(2)}) async-start(bf16[8,2,16,768]{3,2,1,0:T(8,128)(2,1)} %shard_map.152), calls=%async_computation.3 | async-start | bytes 786432 | tf_op jit(solution)/shard_map/all_to_all | solution.py:254
  102.1 13.5 %all-to-all-done.3.got = bf16[8,2,16,768]{3,2,1,0:T(8,128)(2,1)S(1)} async-done(((bf16[8,2,16,768]{3,2,1,0:T(8,128)(2,1)}), bf16[8,2,16,768]{3,2,1,0:T(8,128)(2,1)S(1)}, u32[]{:S(2)}, u32[]{:S(2)}) %all-to-all-start.3) | async-done | bytes 393248 | tf_op jit(solution)/shard_map/all_to_all | solution.py:254
  115.6 0.8 shard_map.153
  116.4 3.4 %all-to-all-start.4 = ((bf16[8,2,16,384]{3,2,1,0:T(8,128)(2,1)}), bf16[8,2,16,384]{3,2,1,0:T(8,128)(2,1)S(1)}, u32[]{:S(2)}, u32[]{:S(2)}) async-start(bf16[8,2,16,384]{3,2,1,0:T(8,128)(2,1)} %shard_map.153), calls=%async_computation.4 | async-start | bytes 393216 | tf_op jit(solution)/shard_map/all_to_all | solution.py:254
  119.8 1.6 %shard_map.154 = (bf16[768,128]{1,0:T(8,128)(2,1)S(1)}, bf16[768,128]{1,0:T(8,128)(2,1)S(1)}, bf16[768,128]{1,0:T(8,128)(2,1)S(1)}, bf16[768,128]{1,0:T(8,128)(2,1)S(1)}) custom-call(f32[2816,128]{1,0:T(8,128)} %far.3, f32[1,128]{1,0:T(1,128)S(1)} %bitcast.6), custom_call_target="tpu_custom_call" | custom-call | tf_op jit(solution)/shard_map/pallas_call | solution.py:44
  121.3 0.9 collective-permute-start.18
  122.2 3.8 %collective-permute-start.19 = (bf16[768,128]{1,0:T(8,128)(2,1)S(1)}, bf16[768,128]{1,0:T(8,128)(2,1)S(1)}, u32[]{:S(2)}, u32[]{:S(2)}) collective-permute-start(bf16[768,128]{1,0:T(8,128)(2,1)S(1)} %get-tuple-element.42), channel_id=1, source_target_pairs={{0,16},{8,24},{16,0},{24,8},{1,17},{9,25},{17,1},{25,9},{2,18},{10... | collective-permute-start | bytes 589832 | tf_op jit(solution)/shard_map/ppermute | solution.py:242
  126.0 2.3 %collective-permute-done.18.d1 = bf16[768,128]{1,0:T(8,128)(2,1)S(1)} collective-permute-done((bf16[768,128]{1,0:T(8,128)(2,1)S(1)}, bf16[768,128]{1,0:T(8,128)(2,1)S(1)}, u32[]{:S(2)}, u32[]{:S(2)}) %collective-permute-start.18) | collective-permute-done | bytes 196640 | tf_op jit(solution)/shard_map/ppermute | solution.py:242
  128.3 1.8 %collective-permute-done.19.d2 = bf16[768,128]{1,0:T(8,128)(2,1)S(1)} collective-permute-done((bf16[768,128]{1,0:T(8,128)(2,1)S(1)}, bf16[768,128]{1,0:T(8,128)(2,1)S(1)}, u32[]{:S(2)}, u32[]{:S(2)}) %collective-permute-start.19) | collective-permute-done | bytes 196640 | tf_op jit(solution)/shard_map/ppermute | solution.py:242
  130.1 2.1 %collective-permute-done.20.d3 = bf16[768,128]{1,0:T(8,128)(2,1)S(1)} collective-permute-done((bf16[768,128]{1,0:T(8,128)(2,1)S(1)}, bf16[768,128]{1,0:T(8,128)(2,1)S(1)}, u32[]{:S(2)}, u32[]{:S(2)}) %collective-permute-start.20) | collective-permute-done | bytes 196640 | tf_op jit(solution)/shard_map/ppermute | solution.py:242
  132.6 15.5 %all_to_all.30.got = bf16[16,128,128]{2,1,0:T(8,128)(2,1)S(1)} all-to-all(bf16[16,128,128]{2,1,0:T(8,128)(2,1)S(1)} %shard_map.155), channel_id=1, replica_groups=mesh['z'=8,'x'=4,'y'=4,'c'=2] {'x','y'}, dimensions={0} | all-to-all | bytes 1048576 | tf_op jit(solution)/shard_map/all_to_all | solution.py:254
  148.1 0.7 shard_map.156
  (37 shorter events, 0.8 us)
Async XLA Ops:
  2.4 8.8 %collective-permute-start = (bf16[128,896]{1,0:T(8,128)(2,1)S(1)}, bf16[128,896]{1,0:T(8,128)(2,1)S(1)}, u32[]{:S(2)}, u32[]{:S(2)}) collective-permute-start(bf16[128,896]{1,0:T(8,128)(2,1)S(1)} %get-tuple-element.26), channel_id=1, source_target_pairs={{0,8},{8,16},{16,24},{24,0},{1,9},{9,17},{17,25},{25,1},{2,10},{10... | collective-permute-start | bytes 688136 | tf_op jit(solution)/shard_map/ppermute | solution.py:242
  3.9 10.0 %collective-permute-start.1 = (bf16[128,896]{1,0:T(8,128)(2,1)S(1)}, bf16[128,896]{1,0:T(8,128)(2,1)S(1)}, u32[]{:S(2)}, u32[]{:S(2)}) collective-permute-start(bf16[128,896]{1,0:T(8,128)(2,1)S(1)} %get-tuple-element.27), channel_id=1, source_target_pairs={{0,16},{8,24},{16,0},{24,8},{1,17},{9,25},{17,1},{25,9},{2,18},{10... | collective-permute-start | bytes 688136 | tf_op jit(solution)/shard_map/ppermute | solution.py:242
  6.7 9.9 %collective-permute-start.2 = (bf16[128,896]{1,0:T(8,128)(2,1)S(1)}, bf16[128,896]{1,0:T(8,128)(2,1)S(1)}, u32[]{:S(2)}, u32[]{:S(2)}) collective-permute-start(bf16[128,896]{1,0:T(8,128)(2,1)S(1)} %get-tuple-element.28), channel_id=1, source_target_pairs={{0,24},{8,0},{16,8},{24,16},{1,25},{9,1},{17,9},{25,17},{2,26},{10... | collective-permute-start | bytes 688136 | tf_op jit(solution)/shard_map/ppermute | solution.py:242
  11.1 5.5 %collective-permute-start.3 = (bf16[128,896]{1,0:T(8,128)(2,1)S(1)}, bf16[128,896]{1,0:T(8,128)(2,1)S(1)}, u32[]{:S(2)}, u32[]{:S(2)}) collective-permute-start(bf16[128,896]{1,0:T(8,128)(2,1)S(1)} %collective-permute-done.r1), channel_id=1, source_target_pairs={{0,1},{1,0},{2,3},{3,2},{4,5},{5,4},{6,7},{7,6},{8,9},{9,8},{10,11... | collective-permute-start | bytes 688136 | tf_op jit(solution)/shard_map/ppermute | solution.py:246
  13.9 2.7 %collective-permute-start.4 = (bf16[128,896]{1,0:T(8,128)(2,1)S(1)}, bf16[128,896]{1,0:T(8,128)(2,1)S(1)}, u32[]{:S(2)}, u32[]{:S(2)}) collective-permute-start(bf16[128,896]{1,0:T(8,128)(2,1)S(1)} %collective-permute-done.1.r2), channel_id=1, source_target_pairs={{0,1},{1,0},{2,3},{3,2},{4,5},{5,4},{6,7},{7,6},{8,9},{9,8},{10,11... | collective-permute-start | bytes 688136 | tf_op jit(solution)/shard_map/ppermute | solution.py:246
  16.6 1.5 %collective-permute-start.5 = (bf16[128,896]{1,0:T(8,128)(2,1)S(1)}, bf16[128,896]{1,0:T(8,128)(2,1)S(1)}, u32[]{:S(2)}, u32[]{:S(2)}) collective-permute-start(bf16[128,896]{1,0:T(8,128)(2,1)S(1)} %collective-permute-done.2.r3), channel_id=1, source_target_pairs={{0,1},{1,0},{2,3},{3,2},{4,5},{5,4},{6,7},{7,6},{8,9},{9,8},{10,11... | collective-permute-start | bytes 688136 | tf_op jit(solution)/shard_map/ppermute | solution.py:246
  18.1 9.8 %copy-start.4 = (f32[2816]{0:T(1024)S(1)}, f32[2816]{0:T(1024)}, u32[]{:S(2)}) copy-start(f32[2816]{0:T(1024)} %param.18) | copy-start | bytes 33796
  18.1 9.9 %copy-start.5 = (f32[2816]{0:T(1024)S(1)}, f32[2816]{0:T(1024)}, u32[]{:S(2)}) copy-start(f32[2816]{0:T(1024)} %param.20) | copy-start | bytes 33796
  19.3 27.9 %copy-start.1 = (f32[128]{0:T(128)S(1)}, f32[128]{0:T(128)}, u32[]{:S(2)}) copy-start(f32[128]{0:T(128)} %param.23) | copy-start | bytes 1540
  19.3 23.7 %all-to-all-start = ((bf16[8,2,16,768]{3,2,1,0:T(8,128)(2,1)}), bf16[8,2,16,768]{3,2,1,0:T(8,128)(2,1)S(1)}, u32[]{:S(2)}, u32[]{:S(2)}) async-start(bf16[8,2,16,768]{3,2,1,0:T(8,128)(2,1)} %shard_map.146), calls=%async_computation | async-start | bytes 786432 | tf_op jit(solution)/shard_map/all_to_all | solution.py:254
  43.7 18.6 %all-to-all-start.1 = ((bf16[8,2,16,384]{3,2,1,0:T(8,128)(2,1)}), bf16[8,2,16,384]{3,2,1,0:T(8,128)(2,1)S(1)}, u32[]{:S(2)}, u32[]{:S(2)}) async-start(bf16[8,2,16,384]{3,2,1,0:T(8,128)(2,1)} %shard_map.147), calls=%async_computation.1 | async-start | bytes 393216 | tf_op jit(solution)/shard_map/all_to_all | solution.py:254
  48.7 7.8 %collective-permute-start.6 = (bf16[768,128]{1,0:T(8,128)(2,1)S(1)}, bf16[768,128]{1,0:T(8,128)(2,1)S(1)}, u32[]{:S(2)}, u32[]{:S(2)}) collective-permute-start(bf16[768,128]{1,0:T(8,128)(2,1)S(1)} %get-tuple-element.31), channel_id=1, source_target_pairs={{0,8},{8,16},{16,24},{24,0},{1,9},{9,17},{17,25},{25,1},{2,10},{10... | collective-permute-start | bytes 589832 | tf_op jit(solution)/shard_map/ppermute | solution.py:242
  50.1 9.3 %collective-permute-start.7 = (bf16[768,128]{1,0:T(8,128)(2,1)S(1)}, bf16[768,128]{1,0:T(8,128)(2,1)S(1)}, u32[]{:S(2)}, u32[]{:S(2)}) collective-permute-start(bf16[768,128]{1,0:T(8,128)(2,1)S(1)} %get-tuple-element.32), channel_id=1, source_target_pairs={{0,16},{8,24},{16,0},{24,8},{1,17},{9,25},{17,1},{25,9},{2,18},{10... | collective-permute-start | bytes 589832 | tf_op jit(solution)/shard_map/ppermute | solution.py:242
  51.9 10.4 %collective-permute-start.8 = (bf16[768,128]{1,0:T(8,128)(2,1)S(1)}, bf16[768,128]{1,0:T(8,128)(2,1)S(1)}, u32[]{:S(2)}, u32[]{:S(2)}) collective-permute-start(bf16[768,128]{1,0:T(8,128)(2,1)S(1)} %get-tuple-element.33), channel_id=1, source_target_pairs={{0,24},{8,0},{16,8},{24,16},{1,25},{9,1},{17,9},{25,17},{2,26},{10... | collective-permute-start | bytes 589832 | tf_op jit(solution)/shard_map/ppermute | solution.py:242
  63.5 23.0 %all-to-all-start.2 = ((bf16[16,128,128]{2,1,0:T(8,128)(2,1)}), bf16[16,128,128]{2,1,0:T(8,128)(2,1)S(1)}, u32[]{:S(2)}, u32[]{:S(2)}) async-start(bf16[16,128,128]{2,1,0:T(8,128)(2,1)} %shard_map.149), calls=%async_computation.2 | async-start | bytes 1048576 | tf_op jit(solution)/shard_map/all_to_all | solution.py:254
  70.4 16.0 %copy-start = (bf16[128,128]{1,0:T(8,128)(2,1)S(1)}, bf16[128,128]{1,0:T(8,128)(2,1)}, u32[]{:S(2)}) copy-start(bf16[128,128]{1,0:T(8,128)(2,1)} %old.1) | copy-start | bytes 98308
  70.4 16.0 %copy-start.2 = (f32[128]{0:T(128)S(1)}, f32[128]{0:T(128)}, u32[]{:S(2)}) copy-start(f32[128]{0:T(128)} %param.22) | copy-start | bytes 1540
  72.7 9.3 %collective-permute-start.12 = (bf16[128,768]{1,0:T(8,128)(2,1)S(1)}, bf16[128,768]{1,0:T(8,128)(2,1)S(1)}, u32[]{:S(2)}, u32[]{:S(2)}) collective-permute-start(bf16[128,768]{1,0:T(8,128)(2,1)S(1)} %get-tuple-element.36), channel_id=1, source_target_pairs={{0,8},{8,16},{16,24},{24,0},{1,9},{9,17},{17,25},{25,1},{2,10},{10... | collective-permute-start | bytes 589832 | tf_op jit(solution)/shard_map/ppermute | solution.py:242
  74.3 9.6 %collective-permute-start.13 = (bf16[128,768]{1,0:T(8,128)(2,1)S(1)}, bf16[128,768]{1,0:T(8,128)(2,1)S(1)}, u32[]{:S(2)}, u32[]{:S(2)}) collective-permute-start(bf16[128,768]{1,0:T(8,128)(2,1)S(1)} %get-tuple-element.37), channel_id=1, source_target_pairs={{0,16},{8,24},{16,0},{24,8},{1,17},{9,25},{17,1},{25,9},{2,18},{10... | collective-permute-start | bytes 589832 | tf_op jit(solution)/shard_map/ppermute | solution.py:242
  75.0 11.5 %collective-permute-start.14 = (bf16[128,768]{1,0:T(8,128)(2,1)S(1)}, bf16[128,768]{1,0:T(8,128)(2,1)S(1)}, u32[]{:S(2)}, u32[]{:S(2)}) collective-permute-start(bf16[128,768]{1,0:T(8,128)(2,1)S(1)} %get-tuple-element.38), channel_id=1, source_target_pairs={{0,24},{8,0},{16,8},{24,16},{1,25},{9,1},{17,9},{25,17},{2,26},{10... | collective-permute-start | bytes 589832 | tf_op jit(solution)/shard_map/ppermute | solution.py:242
  82.0 8.1 %collective-permute-start.15 = (bf16[128,768]{1,0:T(8,128)(2,1)S(1)}, bf16[128,768]{1,0:T(8,128)(2,1)S(1)}, u32[]{:S(2)}, u32[]{:S(2)}) collective-permute-start(bf16[128,768]{1,0:T(8,128)(2,1)S(1)} %collective-permute-done.12.r1), channel_id=1, source_target_pairs={{0,1},{1,0},{2,3},{3,2},{4,5},{5,4},{6,7},{7,6},{8,9},{9,8},{10,11... | collective-permute-start | bytes 589832 | tf_op jit(solution)/shard_map/ppermute | solution.py:246
  83.9 6.8 %collective-permute-start.16 = (bf16[128,768]{1,0:T(8,128)(2,1)S(1)}, bf16[128,768]{1,0:T(8,128)(2,1)S(1)}, u32[]{:S(2)}, u32[]{:S(2)}) collective-permute-start(bf16[128,768]{1,0:T(8,128)(2,1)S(1)} %collective-permute-done.13.r2), channel_id=1, source_target_pairs={{0,1},{1,0},{2,3},{3,2},{4,5},{5,4},{6,7},{7,6},{8,9},{9,8},{10,11... | collective-permute-start | bytes 589832 | tf_op jit(solution)/shard_map/ppermute | solution.py:246
  86.4 4.3 %collective-permute-start.17 = (bf16[128,768]{1,0:T(8,128)(2,1)S(1)}, bf16[128,768]{1,0:T(8,128)(2,1)S(1)}, u32[]{:S(2)}, u32[]{:S(2)}) collective-permute-start(bf16[128,768]{1,0:T(8,128)(2,1)S(1)} %collective-permute-done.14.r3), channel_id=1, source_target_pairs={{0,1},{1,0},{2,3},{3,2},{4,5},{5,4},{6,7},{7,6},{8,9},{9,8},{10,11... | collective-permute-start | bytes 589832 | tf_op jit(solution)/shard_map/ppermute | solution.py:246
  86.6 5.5 %collective-permute-start.10 = (bf16[128,128]{1,0:T(8,128)(2,1)S(1)}, bf16[128,128]{1,0:T(8,128)(2,1)S(1)}, u32[]{:S(2)}, u32[]{:S(2)}) collective-permute-start(bf16[128,128]{1,0:T(8,128)(2,1)S(1)} %get-tuple-element.34.s0), channel_id=1, source_target_pairs={{0,16},{8,24},{16,0},{24,8},{1,17},{9,25},{17,1},{25,9},{2,18},{10... | collective-permute-start | bytes 98312 | tf_op jit(solution)/shard_map/ppermute | solution.py:242
  88.3 4.3 %collective-permute-start.11 = (bf16[128,128]{1,0:T(8,128)(2,1)S(1)}, bf16[128,128]{1,0:T(8,128)(2,1)S(1)}, u32[]{:S(2)}, u32[]{:S(2)}) collective-permute-start(bf16[128,128]{1,0:T(8,128)(2,1)S(1)} %get-tuple-element.34.s0), channel_id=1, source_target_pairs={{0,24},{8,0},{16,8},{24,16},{1,25},{9,1},{17,9},{25,17},{2,26},{10... | collective-permute-start | bytes 98312 | tf_op jit(solution)/shard_map/ppermute | solution.py:242
  90.1 3.9 %collective-permute-start.9 = (bf16[128,128]{1,0:T(8,128)(2,1)S(1)}, bf16[128,128]{1,0:T(8,128)(2,1)S(1)}, u32[]{:S(2)}, u32[]{:S(2)}) collective-permute-start(bf16[128,128]{1,0:T(8,128)(2,1)S(1)} %get-tuple-element.34.s0), channel_id=1, source_target_pairs={{0,8},{8,16},{16,24},{24,0},{1,9},{9,17},{17,25},{25,1},{2,10},{10... | collective-permute-start | bytes 98312 | tf_op jit(solution)/shard_map/ppermute | solution.py:242
  94.0 7.9 %copy-start.6 = (f32[2816]{0:T(1024)S(1)}, f32[2816]{0:T(1024)}, u32[]{:S(2)}) copy-start(f32[2816]{0:T(1024)} %param.25) | copy-start | bytes 33796
  94.0 8.0 %copy-start.7 = (f32[2816]{0:T(1024)S(1)}, f32[2816]{0:T(1024)}, u32[]{:S(2)}) copy-start(f32[2816]{0:T(1024)} %param.27) | copy-start | bytes 33796
  95.1 20.5 %all-to-all-start.3 = ((bf16[8,2,16,768]{3,2,1,0:T(8,128)(2,1)}), bf16[8,2,16,768]{3,2,1,0:T(8,128)(2,1)S(1)}, u32[]{:S(2)}, u32[]{:S(2)}) async-start(bf16[8,2,16,768]{3,2,1,0:T(8,128)(2,1)} %shard_map.152), calls=%async_computation.3 | async-start | bytes 786432 | tf_op jit(solution)/shard_map/all_to_all | solution.py:254
  116.4 15.8 %all-to-all-start.4 = ((bf16[8,2,16,384]{3,2,1,0:T(8,128)(2,1)}), bf16[8,2,16,384]{3,2,1,0:T(8,128)(2,1)S(1)}, u32[]{:S(2)}, u32[]{:S(2)}) async-start(bf16[8,2,16,384]{3,2,1,0:T(8,128)(2,1)} %shard_map.153), calls=%async_computation.4 | async-start | bytes 393216 | tf_op jit(solution)/shard_map/all_to_all | solution.py:254
  121.3 26.7 %copy-start.3 = (f32[128]{0:T(128)S(1)}, f32[128]{0:T(128)}, u32[]{:S(2)}) copy-start(f32[128]{0:T(128)} %param.29) | copy-start | bytes 1540
  121.3 7.0 %collective-permute-start.18 = (bf16[768,128]{1,0:T(8,128)(2,1)S(1)}, bf16[768,128]{1,0:T(8,128)(2,1)S(1)}, u32[]{:S(2)}, u32[]{:S(2)}) collective-permute-start(bf16[768,128]{1,0:T(8,128)(2,1)S(1)} %get-tuple-element.41), channel_id=1, source_target_pairs={{0,8},{8,16},{16,24},{24,0},{1,9},{9,17},{17,25},{25,1},{2,10},{10... | collective-permute-start | bytes 589832 | tf_op jit(solution)/shard_map/ppermute | solution.py:242
  122.2 7.9 %collective-permute-start.19 = (bf16[768,128]{1,0:T(8,128)(2,1)S(1)}, bf16[768,128]{1,0:T(8,128)(2,1)S(1)}, u32[]{:S(2)}, u32[]{:S(2)}) collective-permute-start(bf16[768,128]{1,0:T(8,128)(2,1)S(1)} %get-tuple-element.42), channel_id=1, source_target_pairs={{0,16},{8,24},{16,0},{24,8},{1,17},{9,25},{17,1},{25,9},{2,18},{10... | collective-permute-start | bytes 589832 | tf_op jit(solution)/shard_map/ppermute | solution.py:242
  126.0 6.2 %collective-permute-start.20 = (bf16[768,128]{1,0:T(8,128)(2,1)S(1)}, bf16[768,128]{1,0:T(8,128)(2,1)S(1)}, u32[]{:S(2)}, u32[]{:S(2)}) collective-permute-start(bf16[768,128]{1,0:T(8,128)(2,1)S(1)} %get-tuple-element.43), channel_id=1, source_target_pairs={{0,24},{8,0},{16,8},{24,16},{1,25},{9,1},{17,9},{25,17},{2,26},{10... | collective-permute-start | bytes 589832 | tf_op jit(solution)/shard_map/ppermute | solution.py:242

commit v8 on v7

--- a/solution.py
+++ b/solution.py
@@ -21,7 +21,7 @@
 
 VMEM = pl.BlockSpec(memory_space=pltpu.VMEM)
 HBM = pl.BlockSpec(memory_space=pltpu.HBM)
-BLOCKS = 8
+BLOCKS = 4
 
 
 def shape(*dims, dtype=BF):
@@ -109,12 +109,13 @@
     other[...] = chunks[2 * x + 1 - c]
 
 
-def pack_second_body(gate, up, p0, p1, p2, p3, other, chunks, gate_here, up_here, sems):
-    x, c = lax.axis_index("x"), lax.axis_index("c")
+def pack_second_body(gate, up, p0, p1, p2, p3, chunks, gate_here, up_here, sems):
+    x = lax.axis_index("x")
     cut_chunks(gate, up, gate_here, up_here, sems, chunks)
     for k, out in enumerate((p0, p1, p2, p3)):
-        out[...] = chunks[2 * lax.rem(x + k, NX) + c]
-    other[...] = chunks[2 * x + 1 - c]
+        index = 2 * lax.rem(x + k, NX)
+        out[:, :WIDE] = chunks[index]
+        out[:, WIDE:] = chunks[index + 1]
 
 
 def pack_down_body(far, gain, p0, p1, p2, p3, down, sems):
@@ -166,10 +167,7 @@
         store_payload(out, slot, dot(scaled, weights), high, low)
 
 
-def enter_second_body(
-    s0, s1, s2, s3, d0, d1, d2, d3, r0, r1, r2, r3, q0, q1, q2, q3, out
-):
-    c = lax.axis_index("c")
+def enter_second_body(s0, s1, s2, s3, d0, d1, d2, d3, w0, w1, w2, w3, out):
     squares = jnp.zeros((N, N), F32)
     for scaled, d in ((s0, d0), (s1, d1), (s2, d2), (s3, d3)):
         tail = d[HALF:PAD, :].astype(F32)
@@ -178,8 +176,9 @@
         squares = squares + s * s
     high, low = high_low(jnp.sum(squares, axis=1, keepdims=True))
     scaled = jnp.concatenate([v[...] for v in (s0, s1, s2, s3)], axis=1)
-    for slot, group in ((c, (r0, r1, r2, r3)), (1 - c, (q0, q1, q2, q3))):
-        weights = jnp.concatenate([r[...] for r in group], axis=0)
+    for slot in range(2):
+        cols = slice(slot * WIDE, (slot + 1) * WIDE)
+        weights = jnp.concatenate([w[:, cols] for w in (w0, w1, w2, w3)], axis=0)
         store_payload(out, slot, dot(scaled, weights), high, low)
 
 
@@ -301,11 +300,9 @@
             first_down, second_gain[None]
         ),
     )
-    *packed, other = call(
-        pack_second_body, [shape(N, WIDE)] * (NX + 1), 2, cutting, 2
-    )(second_gate, second_up)
-    ups = around(packed)
-    ups = ups + [other] + [other_core(v) for v in ups[1:]]
+    ups = around(
+        call(pack_second_body, [shape(N, 2 * WIDE)] * NX, 2, cutting, 2)(second_gate, second_up),
+    )
     last_downs = around(
         call(pack_down_body, [shape(2 * PAD, N)] * NX, 2, lowering, 1)(
             second_down, second_gain[None]
@@ -321,7 +318,7 @@
     )
     scaled = around([scaled] * NX)
 
-    sums = call(enter_second_body, payload, 16)(*scaled, *downs, *ups)
+    sums = call(enter_second_body, payload, 12)(*scaled, *downs, *ups)
     got = swap(sums, "z")
     hidden = call(hidden_body, spread, 3)(
         got, by_chunk(second_gate_scale), by_chunk(second_up_scale)

time: 151 us -> 158 us (1.046)
  starting transfers between devices: 52.2 us -> 62.1 us
  waiting for transfers between devices: 66.7 us -> 62.1 us
    ppermute x15, starting transfers between devices: 22.9 us -> 32.8 us  [shift(): return lax.ppermute(v, 'x', [(i, (i + k) % NX) for i in range(NX)])]
    ppermute x15, waiting for transfers between devices: 36.9 us -> 30.9 us  [shift(): return lax.ppermute(v, 'x', [(i, (i + k) % NX) for i in range(NX)])]
  transfers between devices with their start and end apart: 26 -> 23, of which waited for: 18 -> 16; matrix products, arithmetic and copies ran while one was open for 0% -> 0% of each run, Pallas kernels for 4% -> 4%
where the time goes in v8:
time: 158 us; the launch traced here: 156 us
  starting transfers between devices  62.1 us (39%)
  waiting for transfers between devices  62.1 us (39%)
  blocking collectives  16.8 us (11%)
  Pallas kernels  14.2 us (9%)
    ppermute x15, starting transfers between devices, shift(): return lax.ppermute(v, 'x', [(i, (i + k) % NX) for i in range(NX)])  32.8 us
    ppermute x15, waiting for transfers between devices, shift(): return lax.ppermute(v, 'x', [(i, (i + k) % NX) for i in range(NX)])  30.9 us
    all_to_all x5, waiting for transfers between devices, swap(): return lax.all_to_all(v, axis, 0, 0, tiled=True)  29.6 us
    all_to_all x5, starting transfers between devices, swap(): return lax.all_to_all(v, axis, 0, 0, tiled=True)  29.2 us
    all_to_all x1, blocking collectives, swap(): return lax.all_to_all(v, axis, 0, 0, tiled=True)  16.8 us
    pallas_call x12, Pallas kernels, run(): return kernel(*there, *args[far:])  14.2 us
  transfers between devices with their start and end apart: 23, of which 16 were waited for; matrix products, arithmetic and copies ran while one was open for 0% of the time, Pallas kernels for 4%

profile of v8, /device:TPU:2, one launch (start us, length us, event | category | flops | bytes accessed | tf_op | source)
XLA Modules:
  0.0 155.5 jit_solution(1244053673331699127)
XLA Ops:
  0.0 2.1 %shard_map.145 = (bf16[128,896]{1,0:T(8,128)(2,1)S(1)}, bf16[128,896]{1,0:T(8,128)(2,1)S(1)}, bf16[128,896]{1,0:T(8,128)(2,1)S(1)}, bf16[128,896]{1,0:T(8,128)(2,1)S(1)}, bf16[128,768]{1,0:T(8,128)(2,1)S(1)}) custom-call(f32[128,2816]{1,0:T(8,128)} %gate.2, f32[128,2816]{1,0:T(8,128)} %up.2, bf16[128,128]{1,0:T(8,128)(2,1)} %old.1, f32[1,128]{1,0:T(1,128)} %bitcast.9), custom_call_target="tpu_custom_call" | custom-call | tf_op jit(solution)/shard_map/pallas_call | solution.py:44
  2.2 1.6 %collective-permute-start = (bf16[128,896]{1,0:T(8,128)(2,1)S(1)}, bf16[128,896]{1,0:T(8,128)(2,1)S(1)}, u32[]{:S(2)}, u32[]{:S(2)}) collective-permute-start(bf16[128,896]{1,0:T(8,128)(2,1)S(1)} %get-tuple-element.25), channel_id=1, source_target_pairs={{0,8},{8,16},{16,24},{24,0},{1,9},{9,17},{17,25},{25,1},{2,10},{10... | collective-permute-start | bytes 688136 | tf_op jit(solution)/shard_map/ppermute | solution.py:241
  3.7 2.8 %collective-permute-start.1 = (bf16[128,896]{1,0:T(8,128)(2,1)S(1)}, bf16[128,896]{1,0:T(8,128)(2,1)S(1)}, u32[]{:S(2)}, u32[]{:S(2)}) collective-permute-start(bf16[128,896]{1,0:T(8,128)(2,1)S(1)} %get-tuple-element.26), channel_id=1, source_target_pairs={{0,16},{8,24},{16,0},{24,8},{1,17},{9,25},{17,1},{25,9},{2,18},{10... | collective-permute-start | bytes 688136 | tf_op jit(solution)/shard_map/ppermute | solution.py:241
  6.5 0.4 collective-permute-start.2
  7.0 3.9 %collective-permute-done.r1 = bf16[128,896]{1,0:T(8,128)(2,1)S(1)} collective-permute-done((bf16[128,896]{1,0:T(8,128)(2,1)S(1)}, bf16[128,896]{1,0:T(8,128)(2,1)S(1)}, u32[]{:S(2)}, u32[]{:S(2)}) %collective-permute-start) | collective-permute-done | bytes 229408 | tf_op jit(solution)/shard_map/ppermute | solution.py:241
  10.9 2.8 %collective-permute-done.1.r2 = bf16[128,896]{1,0:T(8,128)(2,1)S(1)} collective-permute-done((bf16[128,896]{1,0:T(8,128)(2,1)S(1)}, bf16[128,896]{1,0:T(8,128)(2,1)S(1)}, u32[]{:S(2)}, u32[]{:S(2)}) %collective-permute-start.1) | collective-permute-done | bytes 229408 | tf_op jit(solution)/shard_map/ppermute | solution.py:241
  13.7 2.7 %collective-permute-done.2.r3 = bf16[128,896]{1,0:T(8,128)(2,1)S(1)} collective-permute-done((bf16[128,896]{1,0:T(8,128)(2,1)S(1)}, bf16[128,896]{1,0:T(8,128)(2,1)S(1)}, u32[]{:S(2)}, u32[]{:S(2)}) %collective-permute-start.2) | collective-permute-done | bytes 229408 | tf_op jit(solution)/shard_map/ppermute | solution.py:241
  16.5 1.5 collective-permute-done.5.s3
  17.9 1.1 shard_map.146
  19.1 8.7 %all-to-all-start = ((bf16[8,2,16,768]{3,2,1,0:T(8,128)(2,1)}), bf16[8,2,16,768]{3,2,1,0:T(8,128)(2,1)S(1)}, u32[]{:S(2)}, u32[]{:S(2)}) async-start(bf16[8,2,16,768]{3,2,1,0:T(8,128)(2,1)} %shard_map.146), calls=%async_computation | async-start | bytes 786432 | tf_op jit(solution)/shard_map/all_to_all | solution.py:253
  27.9 14.8 %all-to-all-done.got = bf16[8,2,16,768]{3,2,1,0:T(8,128)(2,1)S(1)} async-done(((bf16[8,2,16,768]{3,2,1,0:T(8,128)(2,1)}), bf16[8,2,16,768]{3,2,1,0:T(8,128)(2,1)S(1)}, u32[]{:S(2)}, u32[]{:S(2)}) %all-to-all-start) | async-done | bytes 393248 | tf_op jit(solution)/shard_map/all_to_all | solution.py:253
  42.8 0.8 shard_map.147
  43.6 3.4 %all-to-all-start.1 = ((bf16[8,2,16,384]{3,2,1,0:T(8,128)(2,1)}), bf16[8,2,16,384]{3,2,1,0:T(8,128)(2,1)S(1)}, u32[]{:S(2)}, u32[]{:S(2)}) async-start(bf16[8,2,16,384]{3,2,1,0:T(8,128)(2,1)} %shard_map.147), calls=%async_computation.1 | async-start | bytes 393216 | tf_op jit(solution)/shard_map/all_to_all | solution.py:253
  47.0 1.4 shard_map.148
  48.4 1.4 collective-permute-start.6
  49.8 1.8 %collective-permute-start.7 = (bf16[768,128]{1,0:T(8,128)(2,1)S(1)}, bf16[768,128]{1,0:T(8,128)(2,1)S(1)}, u32[]{:S(2)}, u32[]{:S(2)}) collective-permute-start(bf16[768,128]{1,0:T(8,128)(2,1)S(1)} %get-tuple-element.31), channel_id=1, source_target_pairs={{0,16},{8,24},{16,0},{24,8},{1,17},{9,25},{17,1},{25,9},{2,18},{10... | collective-permute-start | bytes 589832 | tf_op jit(solution)/shard_map/ppermute | solution.py:241
  51.6 1.3 collective-permute-start.8
  52.9 3.4 %collective-permute-done.6.d1 = bf16[768,128]{1,0:T(8,128)(2,1)S(1)} collective-permute-done((bf16[768,128]{1,0:T(8,128)(2,1)S(1)}, bf16[768,128]{1,0:T(8,128)(2,1)S(1)}, u32[]{:S(2)}, u32[]{:S(2)}) %collective-permute-start.6) | collective-permute-done | bytes 196640 | tf_op jit(solution)/shard_map/ppermute | solution.py:241
  56.3 2.8 %collective-permute-done.7.d2 = bf16[768,128]{1,0:T(8,128)(2,1)S(1)} collective-permute-done((bf16[768,128]{1,0:T(8,128)(2,1)S(1)}, bf16[768,128]{1,0:T(8,128)(2,1)S(1)}, u32[]{:S(2)}, u32[]{:S(2)}) %collective-permute-start.7) | collective-permute-done | bytes 196640 | tf_op jit(solution)/shard_map/ppermute | solution.py:241
  59.1 2.9 %collective-permute-done.8.d3 = bf16[768,128]{1,0:T(8,128)(2,1)S(1)} collective-permute-done((bf16[768,128]{1,0:T(8,128)(2,1)S(1)}, bf16[768,128]{1,0:T(8,128)(2,1)S(1)}, u32[]{:S(2)}, u32[]{:S(2)}) %collective-permute-start.8) | collective-permute-done | bytes 196640 | tf_op jit(solution)/shard_map/ppermute | solution.py:241
  62.0 1.2 shard_map.149
  63.2 6.9 %all-to-all-start.2 = ((bf16[16,128,128]{2,1,0:T(8,128)(2,1)}), bf16[16,128,128]{2,1,0:T(8,128)(2,1)S(1)}, u32[]{:S(2)}, u32[]{:S(2)}) async-start(bf16[16,128,128]{2,1,0:T(8,128)(2,1)} %shard_map.149), calls=%async_computation.2 | async-start | bytes 1048576 | tf_op jit(solution)/shard_map/all_to_all | solution.py:253
  70.1 3.0 %shard_map.151 = (bf16[128,1536]{1,0:T(8,128)(2,1)S(1)}, bf16[128,1536]{1,0:T(8,128)(2,1)}, bf16[128,1536]{1,0:T(8,128)(2,1)}, bf16[128,1536]{1,0:T(8,128)(2,1)S(1)}) custom-call(f32[128,2816]{1,0:T(8,128)} %gate.3, f32[128,2816]{1,0:T(8,128)} %up.3), custom_call_target="tpu_custom_call" | custom-call | tf_op jit(solution)/shard_map/pallas_call | solution.py:44
  73.1 1.5 collective-permute-start.12
  74.7 0.7 collective-permute-start.13
  75.4 2.5 %collective-permute-start.14 = (bf16[128,1536]{1,0:T(8,128)(2,1)S(1)}, bf16[128,1536]{1,0:T(8,128)(2,1)S(1)}, u32[]{:S(2)}, u32[]{:S(2)}) collective-permute-start(bf16[128,1536]{1,0:T(8,128)(2,1)S(1)} %get-tuple-element.37), channel_id=1, source_target_pairs={{0,24},{8,0},{16,8},{24,16},{1,25},{9,1},{17,9},{25,17},{2,26},{10... | collective-permute-start | bytes 1179656 | tf_op jit(solution)/shard_map/ppermute | solution.py:241
  77.9 2.6 %all-to-all-done.2.got = bf16[16,128,128]{2,1,0:T(8,128)(2,1)S(1)} async-done(((bf16[16,128,128]{2,1,0:T(8,128)(2,1)}), bf16[16,128,128]{2,1,0:T(8,128)(2,1)S(1)}, u32[]{:S(2)}, u32[]{:S(2)}) %all-to-all-start.2) | async-done | bytes 524320 | tf_op jit(solution)/shard_map/all_to_all | solution.py:253
  80.6 2.4 %collective-permute-start.10 = (bf16[128,128]{1,0:T(8,128)(2,1)S(1)}, bf16[128,128]{1,0:T(8,128)(2,1)S(1)}, u32[]{:S(2)}, u32[]{:S(2)}) collective-permute-start(bf16[128,128]{1,0:T(8,128)(2,1)S(1)} %get-tuple-element.33.s0), channel_id=1, source_target_pairs={{0,16},{8,24},{16,0},{24,8},{1,17},{9,25},{17,1},{25,9},{2,18},{10... | collective-permute-start | bytes 98312 | tf_op jit(solution)/shard_map/ppermute | solution.py:241
  83.0 0.6 collective-permute-start.11
  83.6 2.4 %collective-permute-done.12.w1 = bf16[128,1536]{1,0:T(8,128)(2,1)S(1)} collective-permute-done((bf16[128,1536]{1,0:T(8,128)(2,1)}, bf16[128,1536]{1,0:T(8,128)(2,1)S(1)}, u32[]{:S(2)}, u32[]{:S(2)}) %collective-permute-start.12) | collective-permute-done | bytes 393248 | tf_op jit(solution)/shard_map/ppermute | solution.py:241
  85.9 10.1 %collective-permute-start.9 = (bf16[128,128]{1,0:T(8,128)(2,1)S(1)}, bf16[128,128]{1,0:T(8,128)(2,1)S(1)}, u32[]{:S(2)}, u32[]{:S(2)}) collective-permute-start(bf16[128,128]{1,0:T(8,128)(2,1)S(1)} %get-tuple-element.33.s0), channel_id=1, source_target_pairs={{0,8},{8,16},{16,24},{24,0},{1,9},{9,17},{17,25},{25,1},{2,10},{10... | collective-permute-start | bytes 98312 | tf_op jit(solution)/shard_map/ppermute | solution.py:241
  96.0 0.2 collective-permute-done.10.s2
  96.2 1.4 collective-permute-done.9.s1
  97.6 1.1 shard_map.152
  98.7 6.8 %all-to-all-start.3 = ((bf16[8,2,16,768]{3,2,1,0:T(8,128)(2,1)}), bf16[8,2,16,768]{3,2,1,0:T(8,128)(2,1)S(1)}, u32[]{:S(2)}, u32[]{:S(2)}) async-start(bf16[8,2,16,768]{3,2,1,0:T(8,128)(2,1)} %shard_map.152), calls=%async_computation.3 | async-start | bytes 786432 | tf_op jit(solution)/shard_map/all_to_all | solution.py:253
  105.7 12.2 %all-to-all-done.3.got = bf16[8,2,16,768]{3,2,1,0:T(8,128)(2,1)S(1)} async-done(((bf16[8,2,16,768]{3,2,1,0:T(8,128)(2,1)}), bf16[8,2,16,768]{3,2,1,0:T(8,128)(2,1)S(1)}, u32[]{:S(2)}, u32[]{:S(2)}) %all-to-all-start.3) | async-done | bytes 393248 | tf_op jit(solution)/shard_map/all_to_all | solution.py:253
  118.0 0.8 shard_map.153
  118.8 3.4 %all-to-all-start.4 = ((bf16[8,2,16,384]{3,2,1,0:T(8,128)(2,1)}), bf16[8,2,16,384]{3,2,1,0:T(8,128)(2,1)S(1)}, u32[]{:S(2)}, u32[]{:S(2)}) async-start(bf16[8,2,16,384]{3,2,1,0:T(8,128)(2,1)} %shard_map.153), calls=%async_computation.4 | async-start | bytes 393216 | tf_op jit(solution)/shard_map/all_to_all | solution.py:253
  122.2 1.4 shard_map.154
  123.6 1.9 %collective-permute-start.15 = (bf16[768,128]{1,0:T(8,128)(2,1)S(1)}, bf16[768,128]{1,0:T(8,128)(2,1)S(1)}, u32[]{:S(2)}, u32[]{:S(2)}) collective-permute-start(bf16[768,128]{1,0:T(8,128)(2,1)S(1)} %get-tuple-element.39), channel_id=1, source_target_pairs={{0,8},{8,16},{16,24},{24,0},{1,9},{9,17},{17,25},{25,1},{2,10},{10... | collective-permute-start | bytes 589832 | tf_op jit(solution)/shard_map/ppermute | solution.py:241
  125.5 3.2 %collective-permute-start.16 = (bf16[768,128]{1,0:T(8,128)(2,1)S(1)}, bf16[768,128]{1,0:T(8,128)(2,1)S(1)}, u32[]{:S(2)}, u32[]{:S(2)}) collective-permute-start(bf16[768,128]{1,0:T(8,128)(2,1)S(1)} %get-tuple-element.40), channel_id=1, source_target_pairs={{0,16},{8,24},{16,0},{24,8},{1,17},{9,25},{17,1},{25,9},{2,18},{10... | collective-permute-start | bytes 589832 | tf_op jit(solution)/shard_map/ppermute | solution.py:241
  128.7 0.5 collective-permute-start.17
  129.2 3.2 %collective-permute-done.15.d1 = bf16[768,128]{1,0:T(8,128)(2,1)S(1)} collective-permute-done((bf16[768,128]{1,0:T(8,128)(2,1)S(1)}, bf16[768,128]{1,0:T(8,128)(2,1)S(1)}, u32[]{:S(2)}, u32[]{:S(2)}) %collective-permute-start.15) | collective-permute-done | bytes 196640 | tf_op jit(solution)/shard_map/ppermute | solution.py:241
  132.4 2.4 %collective-permute-done.16.d2 = bf16[768,128]{1,0:T(8,128)(2,1)S(1)} collective-permute-done((bf16[768,128]{1,0:T(8,128)(2,1)S(1)}, bf16[768,128]{1,0:T(8,128)(2,1)S(1)}, u32[]{:S(2)}, u32[]{:S(2)}) %collective-permute-start.16) | collective-permute-done | bytes 196640 | tf_op jit(solution)/shard_map/ppermute | solution.py:241
  134.8 2.9 %collective-permute-done.17.d3 = bf16[768,128]{1,0:T(8,128)(2,1)S(1)} collective-permute-done((bf16[768,128]{1,0:T(8,128)(2,1)S(1)}, bf16[768,128]{1,0:T(8,128)(2,1)S(1)}, u32[]{:S(2)}, u32[]{:S(2)}) %collective-permute-start.17) | collective-permute-done | bytes 196640 | tf_op jit(solution)/shard_map/ppermute | solution.py:241
  137.7 0.4 shard_map.155
  138.0 16.8 %all_to_all.30.got = bf16[16,128,128]{2,1,0:T(8,128)(2,1)S(1)} all-to-all(bf16[16,128,128]{2,1,0:T(8,128)(2,1)S(1)} %shard_map.155), channel_id=1, replica_groups=mesh['z'=8,'x'=4,'y'=4,'c'=2] {'x','y'}, dimensions={0} | all-to-all | bytes 1048576 | tf_op jit(solution)/shard_map/all_to_all | solution.py:253
  154.8 0.7 shard_map.156
  (31 shorter events, 0.4 us)
Async XLA Ops:
  2.2 8.8 %collective-permute-start = (bf16[128,896]{1,0:T(8,128)(2,1)S(1)}, bf16[128,896]{1,0:T(8,128)(2,1)S(1)}, u32[]{:S(2)}, u32[]{:S(2)}) collective-permute-start(bf16[128,896]{1,0:T(8,128)(2,1)S(1)} %get-tuple-element.25), channel_id=1, source_target_pairs={{0,8},{8,16},{16,24},{24,0},{1,9},{9,17},{17,25},{25,1},{2,10},{10... | collective-permute-start | bytes 688136 | tf_op jit(solution)/shard_map/ppermute | solution.py:241
  3.7 10.0 %collective-permute-start.1 = (bf16[128,896]{1,0:T(8,128)(2,1)S(1)}, bf16[128,896]{1,0:T(8,128)(2,1)S(1)}, u32[]{:S(2)}, u32[]{:S(2)}) collective-permute-start(bf16[128,896]{1,0:T(8,128)(2,1)S(1)} %get-tuple-element.26), channel_id=1, source_target_pairs={{0,16},{8,24},{16,0},{24,8},{1,17},{9,25},{17,1},{25,9},{2,18},{10... | collective-permute-start | bytes 688136 | tf_op jit(solution)/shard_map/ppermute | solution.py:241
  6.5 9.9 %collective-permute-start.2 = (bf16[128,896]{1,0:T(8,128)(2,1)S(1)}, bf16[128,896]{1,0:T(8,128)(2,1)S(1)}, u32[]{:S(2)}, u32[]{:S(2)}) collective-permute-start(bf16[128,896]{1,0:T(8,128)(2,1)S(1)} %get-tuple-element.27), channel_id=1, source_target_pairs={{0,24},{8,0},{16,8},{24,16},{1,25},{9,1},{17,9},{25,17},{2,26},{10... | collective-permute-start | bytes 688136 | tf_op jit(solution)/shard_map/ppermute | solution.py:241
  10.9 5.5 %collective-permute-start.3 = (bf16[128,896]{1,0:T(8,128)(2,1)S(1)}, bf16[128,896]{1,0:T(8,128)(2,1)S(1)}, u32[]{:S(2)}, u32[]{:S(2)}) collective-permute-start(bf16[128,896]{1,0:T(8,128)(2,1)S(1)} %collective-permute-done.r1), channel_id=1, source_target_pairs={{0,1},{1,0},{2,3},{3,2},{4,5},{5,4},{6,7},{7,6},{8,9},{9,8},{10,11... | collective-permute-start | bytes 688136 | tf_op jit(solution)/shard_map/ppermute | solution.py:245
  13.7 2.7 %collective-permute-start.4 = (bf16[128,896]{1,0:T(8,128)(2,1)S(1)}, bf16[128,896]{1,0:T(8,128)(2,1)S(1)}, u32[]{:S(2)}, u32[]{:S(2)}) collective-permute-start(bf16[128,896]{1,0:T(8,128)(2,1)S(1)} %collective-permute-done.1.r2), channel_id=1, source_target_pairs={{0,1},{1,0},{2,3},{3,2},{4,5},{5,4},{6,7},{7,6},{8,9},{9,8},{10,11... | collective-permute-start | bytes 688136 | tf_op jit(solution)/shard_map/ppermute | solution.py:245
  16.4 1.5 collective-permute-start.5
  17.9 9.8 %copy-start.4 = (f32[2816]{0:T(1024)S(1)}, f32[2816]{0:T(1024)}, u32[]{:S(2)}) copy-start(f32[2816]{0:T(1024)} %param.18) | copy-start | bytes 33796
  17.9 9.9 %copy-start.5 = (f32[2816]{0:T(1024)S(1)}, f32[2816]{0:T(1024)}, u32[]{:S(2)}) copy-start(f32[2816]{0:T(1024)} %param.20) | copy-start | bytes 33796
  19.1 27.9 %copy-start.1 = (f32[128]{0:T(128)S(1)}, f32[128]{0:T(128)}, u32[]{:S(2)}) copy-start(f32[128]{0:T(128)} %param.23) | copy-start | bytes 1540
  19.1 23.7 %all-to-all-start = ((bf16[8,2,16,768]{3,2,1,0:T(8,128)(2,1)}), bf16[8,2,16,768]{3,2,1,0:T(8,128)(2,1)S(1)}, u32[]{:S(2)}, u32[]{:S(2)}) async-start(bf16[8,2,16,768]{3,2,1,0:T(8,128)(2,1)} %shard_map.146), calls=%async_computation | async-start | bytes 786432 | tf_op jit(solution)/shard_map/all_to_all | solution.py:253
  43.6 18.5 %all-to-all-start.1 = ((bf16[8,2,16,384]{3,2,1,0:T(8,128)(2,1)}), bf16[8,2,16,384]{3,2,1,0:T(8,128)(2,1)S(1)}, u32[]{:S(2)}, u32[]{:S(2)}) async-start(bf16[8,2,16,384]{3,2,1,0:T(8,128)(2,1)} %shard_map.147), calls=%async_computation.1 | async-start | bytes 393216 | tf_op jit(solution)/shard_map/all_to_all | solution.py:253
  48.4 7.8 %collective-permute-start.6 = (bf16[768,128]{1,0:T(8,128)(2,1)S(1)}, bf16[768,128]{1,0:T(8,128)(2,1)S(1)}, u32[]{:S(2)}, u32[]{:S(2)}) collective-permute-start(bf16[768,128]{1,0:T(8,128)(2,1)S(1)} %get-tuple-element.30), channel_id=1, source_target_pairs={{0,8},{8,16},{16,24},{24,0},{1,9},{9,17},{17,25},{25,1},{2,10},{10... | collective-permute-start | bytes 589832 | tf_op jit(solution)/shard_map/ppermute | solution.py:241
  49.8 9.3 %collective-permute-start.7 = (bf16[768,128]{1,0:T(8,128)(2,1)S(1)}, bf16[768,128]{1,0:T(8,128)(2,1)S(1)}, u32[]{:S(2)}, u32[]{:S(2)}) collective-permute-start(bf16[768,128]{1,0:T(8,128)(2,1)S(1)} %get-tuple-element.31), channel_id=1, source_target_pairs={{0,16},{8,24},{16,0},{24,8},{1,17},{9,25},{17,1},{25,9},{2,18},{10... | collective-permute-start | bytes 589832 | tf_op jit(solution)/shard_map/ppermute | solution.py:241
  51.6 10.4 %collective-permute-start.8 = (bf16[768,128]{1,0:T(8,128)(2,1)S(1)}, bf16[768,128]{1,0:T(8,128)(2,1)S(1)}, u32[]{:S(2)}, u32[]{:S(2)}) collective-permute-start(bf16[768,128]{1,0:T(8,128)(2,1)S(1)} %get-tuple-element.32), channel_id=1, source_target_pairs={{0,24},{8,0},{16,8},{24,16},{1,25},{9,1},{17,9},{25,17},{2,26},{10... | collective-permute-start | bytes 589832 | tf_op jit(solution)/shard_map/ppermute | solution.py:241
  63.2 17.3 %all-to-all-start.2 = ((bf16[16,128,128]{2,1,0:T(8,128)(2,1)}), bf16[16,128,128]{2,1,0:T(8,128)(2,1)S(1)}, u32[]{:S(2)}, u32[]{:S(2)}) async-start(bf16[16,128,128]{2,1,0:T(8,128)(2,1)} %shard_map.149), calls=%async_computation.2 | async-start | bytes 1048576 | tf_op jit(solution)/shard_map/all_to_all | solution.py:253
  70.1 10.4 %copy-start = (bf16[128,128]{1,0:T(8,128)(2,1)S(1)}, bf16[128,128]{1,0:T(8,128)(2,1)}, u32[]{:S(2)}) copy-start(bf16[128,128]{1,0:T(8,128)(2,1)} %old.1) | copy-start | bytes 98308
  70.1 10.4 %copy-start.2 = (f32[128]{0:T(128)S(1)}, f32[128]{0:T(128)}, u32[]{:S(2)}) copy-start(f32[128]{0:T(128)} %param.22) | copy-start | bytes 1540
  73.1 12.8 %collective-permute-start.12 = (bf16[128,1536]{1,0:T(8,128)(2,1)}, bf16[128,1536]{1,0:T(8,128)(2,1)S(1)}, u32[]{:S(2)}, u32[]{:S(2)}) collective-permute-start(bf16[128,1536]{1,0:T(8,128)(2,1)} %get-tuple-element.35), channel_id=1, source_target_pairs={{0,8},{8,16},{16,24},{24,0},{1,9},{9,17},{17,25},{25,1},{2,10},{10... | collective-permute-start | bytes 1179656 | tf_op jit(solution)/shard_map/ppermute | solution.py:241
  74.7 21.3 %collective-permute-start.13 = (bf16[128,1536]{1,0:T(8,128)(2,1)}, bf16[128,1536]{1,0:T(8,128)(2,1)S(1)}, u32[]{:S(2)}, u32[]{:S(2)}) collective-permute-start(bf16[128,1536]{1,0:T(8,128)(2,1)} %get-tuple-element.36), channel_id=1, source_target_pairs={{0,16},{8,24},{16,0},{24,8},{1,17},{9,25},{17,1},{25,9},{2,18},{10... | collective-permute-start | bytes 1179656 | tf_op jit(solution)/shard_map/ppermute | solution.py:241
  75.4 20.6 %collective-permute-start.14 = (bf16[128,1536]{1,0:T(8,128)(2,1)S(1)}, bf16[128,1536]{1,0:T(8,128)(2,1)S(1)}, u32[]{:S(2)}, u32[]{:S(2)}) collective-permute-start(bf16[128,1536]{1,0:T(8,128)(2,1)S(1)} %get-tuple-element.37), channel_id=1, source_target_pairs={{0,24},{8,0},{16,8},{24,16},{1,25},{9,1},{17,9},{25,17},{2,26},{10... | collective-permute-start | bytes 1179656 | tf_op jit(solution)/shard_map/ppermute | solution.py:241
  80.6 15.6 %collective-permute-start.10 = (bf16[128,128]{1,0:T(8,128)(2,1)S(1)}, bf16[128,128]{1,0:T(8,128)(2,1)S(1)}, u32[]{:S(2)}, u32[]{:S(2)}) collective-permute-start(bf16[128,128]{1,0:T(8,128)(2,1)S(1)} %get-tuple-element.33.s0), channel_id=1, source_target_pairs={{0,16},{8,24},{16,0},{24,8},{1,17},{9,25},{17,1},{25,9},{2,18},{10... | collective-permute-start | bytes 98312 | tf_op jit(solution)/shard_map/ppermute | solution.py:241
  83.0 13.2 %collective-permute-start.11 = (bf16[128,128]{1,0:T(8,128)(2,1)S(1)}, bf16[128,128]{1,0:T(8,128)(2,1)S(1)}, u32[]{:S(2)}, u32[]{:S(2)}) collective-permute-start(bf16[128,128]{1,0:T(8,128)(2,1)S(1)} %get-tuple-element.33.s0), channel_id=1, source_target_pairs={{0,24},{8,0},{16,8},{24,16},{1,25},{9,1},{17,9},{25,17},{2,26},{10... | collective-permute-start | bytes 98312 | tf_op jit(solution)/shard_map/ppermute | solution.py:241
  85.9 11.7 %collective-permute-start.9 = (bf16[128,128]{1,0:T(8,128)(2,1)S(1)}, bf16[128,128]{1,0:T(8,128)(2,1)S(1)}, u32[]{:S(2)}, u32[]{:S(2)}) collective-permute-start(bf16[128,128]{1,0:T(8,128)(2,1)S(1)} %get-tuple-element.33.s0), channel_id=1, source_target_pairs={{0,8},{8,16},{16,24},{24,0},{1,9},{9,17},{17,25},{25,1},{2,10},{10... | collective-permute-start | bytes 98312 | tf_op jit(solution)/shard_map/ppermute | solution.py:241
  97.6 8.0 %copy-start.6 = (f32[2816]{0:T(1024)S(1)}, f32[2816]{0:T(1024)}, u32[]{:S(2)}) copy-start(f32[2816]{0:T(1024)} %param.25) | copy-start | bytes 33796
  97.6 8.1 %copy-start.7 = (f32[2816]{0:T(1024)S(1)}, f32[2816]{0:T(1024)}, u32[]{:S(2)}) copy-start(f32[2816]{0:T(1024)} %param.27) | copy-start | bytes 33796
  98.7 19.2 %all-to-all-start.3 = ((bf16[8,2,16,768]{3,2,1,0:T(8,128)(2,1)}), bf16[8,2,16,768]{3,2,1,0:T(8,128)(2,1)S(1)}, u32[]{:S(2)}, u32[]{:S(2)}) async-start(bf16[8,2,16,768]{3,2,1,0:T(8,128)(2,1)} %shard_map.152), calls=%async_computation.3 | async-start | bytes 786432 | tf_op jit(solution)/shard_map/all_to_all | solution.py:253
  118.8 18.9 %all-to-all-start.4 = ((bf16[8,2,16,384]{3,2,1,0:T(8,128)(2,1)}), bf16[8,2,16,384]{3,2,1,0:T(8,128)(2,1)S(1)}, u32[]{:S(2)}, u32[]{:S(2)}) async-start(bf16[8,2,16,384]{3,2,1,0:T(8,128)(2,1)} %shard_map.153), calls=%async_computation.4 | async-start | bytes 393216 | tf_op jit(solution)/shard_map/all_to_all | solution.py:253
  123.6 31.2 %copy-start.3 = (f32[128]{0:T(128)S(1)}, f32[128]{0:T(128)}, u32[]{:S(2)}) copy-start(f32[128]{0:T(128)} %param.29) | copy-start | bytes 1540
  123.6 8.8 %collective-permute-start.15 = (bf16[768,128]{1,0:T(8,128)(2,1)S(1)}, bf16[768,128]{1,0:T(8,128)(2,1)S(1)}, u32[]{:S(2)}, u32[]{:S(2)}) collective-permute-start(bf16[768,128]{1,0:T(8,128)(2,1)S(1)} %get-tuple-element.39), channel_id=1, source_target_pairs={{0,8},{8,16},{16,24},{24,0},{1,9},{9,17},{17,25},{25,1},{2,10},{10... | collective-permute-start | bytes 589832 | tf_op jit(solution)/shard_map/ppermute | solution.py:241
  125.5 9.3 %collective-permute-start.16 = (bf16[768,128]{1,0:T(8,128)(2,1)S(1)}, bf16[768,128]{1,0:T(8,128)(2,1)S(1)}, u32[]{:S(2)}, u32[]{:S(2)}) collective-permute-start(bf16[768,128]{1,0:T(8,128)(2,1)S(1)} %get-tuple-element.40), channel_id=1, source_target_pairs={{0,16},{8,24},{16,0},{24,8},{1,17},{9,25},{17,1},{25,9},{2,18},{10... | collective-permute-start | bytes 589832 | tf_op jit(solution)/shard_map/ppermute | solution.py:241
  128.7 8.9 %collective-permute-start.17 = (bf16[768,128]{1,0:T(8,128)(2,1)S(1)}, bf16[768,128]{1,0:T(8,128)(2,1)S(1)}, u32[]{:S(2)}, u32[]{:S(2)}) collective-permute-start(bf16[768,128]{1,0:T(8,128)(2,1)S(1)} %get-tuple-element.41), channel_id=1, source_target_pairs={{0,24},{8,0},{16,8},{24,16},{1,25},{9,1},{17,9},{25,17},{2,26},{10... | collective-permute-start | bytes 589832 | tf_op jit(solution)/shard_map/ppermute | solution.py:241
